TPU v7x, 32 devices: a whole 2x2x4 slice. The times are simulated.
32 devices in a mesh: ep: 8 (over z, x), tp: 4 (over y, core).
Axes of the slice: x: 2, y: 2, z: 4, core: 2. Of those that a mesh axis runs over, the one named last changes fastest.
Arguments:
- mix_query: bfloat16 [2048, 2048], P('ep', 'tp'), may hold values from -6 to 6
- forget_input: bfloat16 [2048, 2048], P('ep', 'tp'), may hold values from -6 to 6
- mix_value: bfloat16 [2048, 2048], P('ep', 'tp'), may hold values from -6 to 6
- out_gate_input: bfloat16 [2048, 2048], P('ep', 'tp'), may hold values from -6 to 6
- decay_shift: float32 [2048, 16], P('ep', 'tp'), may hold values from -1.5 to 0
- forget_floor: float32 [2048], P('tp'), may hold values from 0.9 to 1
- head_gain: float32 [128], replicated, may hold values from 0.1 to 1.9
- w_mix_out: bfloat16 [2048, 2048], P(None, 'tp'), may hold values from -0.125 to 0.125
- moe_input: bfloat16 [2048, 2048], P('ep'), may hold values from -6 to 6
- moe_gain: float32 [2048], replicated, may hold values from 0.1 to 1.9
- routes: int32 [2048, 2], P('ep'), may hold values from 0 to 7, all different within a row; in each aligned block of 256 rows (0 to 255, 256 to 511, ...) at most 80 rows name the same one
- route_weight: float32 [2048, 2], P('ep'), may hold values from 0.1 to 1
- w_exp_gate: bfloat16 [8, 2048, 4096], P('ep', None, 'tp'), may hold values from -0.125 to 0.125
- w_exp_up: bfloat16 [8, 2048, 4096], P('ep', None, 'tp'), may hold values from -0.125 to 0.125
- w_exp_down: bfloat16 [8, 4096, 2048], P('ep', 'tp'), may hold values from -0.125 to 0.125
Outputs:
- mixed: bfloat16 [2048, 2048], P('ep', 'tp')
- moe_out: bfloat16 [2048, 2048], P('ep', 'tp')
Inputs may be any that keep to these rules, and one draw needn't show every extreme that they name: `routes`: at most 80 of the rows of one index of ep name one expert, and in every draw some device's rows name one expert exactly 80 times; the experts of a row differ.
All inputs are finite; a program needn't handle non-finite values.
Results may differ from a plain program's by a relative error of at most 0.02.
Values may be sent and summed in bfloat16 or wider, within the bound.
No kernel may reach another device: no remote copies, remote signals or barrier semaphores. Data moves between devices by JAX's collectives and lax.ppermute only.
A program may use at most 64 MiB of HBM per device.

v0:
```python
import functools

import jax
import jax.numpy as jnp
from jax import lax
from jax.experimental import pallas as pl
from jax.experimental.pallas import tpu as pltpu
from jax.sharding import PartitionSpec as P


TOP_K = 2
ROWS = 16
EPS = 1e-06
F32 = jnp.float32
BF16 = jnp.bfloat16

VMEM = pl.BlockSpec(memory_space=pltpu.VMEM)
GRANT = 16 << 20
WEIGH = 4e9
NN = (((1,), (0,)), ((), ()))
NT = (((1,), (1,)), ((), ()))
TN = (((0,), (0,)), ((), ()))


def mm(a, b, dims=NN):
    return lax.dot_general(a, b, dims, preferred_element_type=F32)


def split_mm(a, b, dims, left):
    wide = a if left else b
    high = wide.astype(BF16)
    low = (wide - high.astype(F32)).astype(BF16)
    if left:
        return mm(high, b, dims) + mm(low, b, dims)
    return mm(a, high, dims) + mm(a, low, dims)


def call(body, outs, args, flops, scratch=()):
    return pl.pallas_call(
        body,
        out_shape=tuple(jax.ShapeDtypeStruct(s, d) for s, d in outs),
        in_specs=[VMEM] * len(args),
        out_specs=tuple(VMEM for _ in outs),
        scratch_shapes=list(scratch),
        compiler_params=pltpu.CompilerParams(vmem_limit_bytes=GRANT),
        cost_estimate=pl.CostEstimate(
            flops=int(max(flops, WEIGH)), transcendentals=0, bytes_accessed=1 << 20
        ),
    )(*args)


def swap(array, axis, size, bit):
    return lax.ppermute(array, axis, [(i, i ^ bit) for i in range(size)])


def in_hbm(*arrays):
    return [pltpu.with_memory_space_constraint(a, pltpu.HBM) for a in arrays]


def local_body(q_ref, x_ref, v_ref, shift_ref, floor_ref, sd_ref, qd_ref, within_ref):
    length, width = q_ref.shape
    heads = shift_ref.shape[0]
    size = width // heads
    low = floor_ref[...]
    x = x_ref[...].astype(F32)
    g = jnp.log(low + (1.0 - low) * jax.nn.sigmoid(x))
    key = (1.0 - low) * jax.nn.sigmoid(-x)
    row = lax.broadcasted_iota(jnp.int32, (length, length), 0)
    col = lax.broadcasted_iota(jnp.int32, (length, length), 1)
    lower = jnp.where(row >= col, 1.0, 0.0).astype(BF16)
    upper = jnp.where(row <= col, 1.0, 0.0).astype(BF16)
    total = split_mm(lower, g, NN, False)
    shift = shift_ref[...]
    if heads == 1:
        shift = jnp.broadcast_to(shift, (8, length))
    down = split_mm(lower, shift, NT, False)
    across = split_mm(shift, upper, NN, True)
    for h in range(heads):
        cut = slice(h * size, (h + 1) * size)
        q = q_ref[:, cut].astype(F32)
        v = v_ref[:, cut]
        k = key[:, cut]
        run = total[:, cut]
        last = run[length - 1 : length, :]
        fall = down[:, h : h + 1]
        final = fall[length - 1 : length, :]
        grow = jnp.exp(run)
        scores = mm((q * grow).astype(BF16), (k * jnp.exp(-run)).astype(BF16), NT)
        mask = jnp.exp(jnp.minimum(fall - across[h : h + 1, :], 0.0))
        scores = jnp.where(row >= col, scores * mask, 0.0)
        within_ref[:, cut] = mm(scores.astype(BF16), v)
        qd_ref[:, cut] = (q * jnp.exp(run + fall)).astype(BF16)
        kept = (k * jnp.exp((last - run) + (final - fall))).astype(BF16)
        sd_ref[0:size, cut] = mm(v, kept, TN).astype(BF16)
        sd_ref[size : size + ROWS, cut] = jnp.broadcast_to(
            jnp.exp(last + final), (ROWS, size)
        ).astype(BF16)


def after(early, late):
    return (late[1] * early[0] + late[0], late[1] * early[1])


def pair(ref):
    rows = ref.shape[0] - ROWS
    return (ref[0:rows, :].astype(F32), ref[rows : rows + 1, :].astype(F32))


def put(ref, value):
    rows = ref.shape[0] - ROWS
    ref[0:rows, :] = value[0].astype(BF16)
    ref[rows : rows + ROWS, :] = jnp.broadcast_to(value[1], (ROWS, ref.shape[1])).astype(BF16)


def choose(flag, a, b):
    return tuple(jnp.where(flag, x, y) for x, y in zip(a, b))


def scan_body(bit, first, tot_ref, *refs):
    if first:
        rec_ref, new_tot_ref, new_pre_ref = refs
    else:
        pre_ref, rec_ref, new_tot_ref, new_pre_ref = refs
    late = (lax.axis_index("ep") & bit) != 0
    tot = pair(tot_ref)
    rec = pair(rec_ref)
    pre = (jnp.zeros_like(tot[0]), jnp.ones_like(tot[1])) if first else pair(pre_ref)
    put(new_tot_ref, choose(late, after(rec, tot), after(tot, rec)))
    put(new_pre_ref, choose(late, after(rec, pre), pre))


def finish_body(bit, within_ref, qd_ref, pre_ref, rec_ref, gate_ref, gain_ref, out_ref):
    width = qd_ref.shape[1]
    size = gain_ref.shape[1]
    late = (lax.axis_index("ep") & bit) != 0
    pre = pair(pre_ref)
    state = choose(late, after(pair(rec_ref), pre), pre)[0].astype(BF16)
    for h in range(width // size):
        cut = slice(h * size, (h + 1) * size)
        got = within_ref[:, cut] + mm(qd_ref[:, cut], state[:, cut], NT)
        scale = lax.rsqrt(jnp.mean(got * got, axis=1, keepdims=True) + EPS)
        gate = gate_ref[:, cut].astype(F32)
        gate = gate * jax.nn.sigmoid(gate)
        out_ref[:, cut] = (got * scale * gain_ref[...] * gate).astype(BF16)


def mixed_body(masks, w_ref, *refs):
    out_ref = refs[-1]
    at = lax.axis_index("tp")
    acc = None
    for mask, ref in zip(masks, refs[:-1]):
        part = mm(ref[...], w_ref[at ^ mask])
        acc = part if acc is None else acc + part
    out_ref[...] = acc.astype(BF16)


def named(routes, experts):
    seat = lax.broadcasted_iota(jnp.int32, (experts, routes.shape[1]), 0)
    return [routes[j : j + 1, :] == seat for j in range(TOP_K)]


def ranked(hits):
    hit = jnp.where(functools.reduce(jnp.logical_or, hits), 1.0, 0.0)
    count = hit.shape[1]
    row = lax.broadcasted_iota(jnp.int32, (count, count), 0)
    col = lax.broadcasted_iota(jnp.int32, (count, count), 1)
    return mm(hit.astype(BF16), jnp.where(row < col, 1.0, 0.0).astype(BF16)), hit


def spread_body(near, far, routes_ref, x_ref, gain_ref, *refs):
    normed_ref, rank_ref, mark_ref = refs[-3:]
    outs = refs[:-3]
    me = lax.axis_index("ep")
    at = lax.axis_index("tp")
    groups, count, width = normed_ref.shape
    x = x_ref[...].astype(F32)
    scale = lax.rsqrt(jnp.mean(x * x, axis=1, keepdims=True) + EPS)
    normed = (x * scale * gain_ref[...]).astype(BF16)
    for q in range(groups):
        normed_ref[q] = normed[:, q * width : (q + 1) * width]
    rank_ref[...], mark_ref[...] = ranked(named(routes_ref[...], rank_ref.shape[0]))
    slot = lax.broadcasted_iota(jnp.int32, (outs[0].shape[0], count), 0).astype(F32)

    def chosen(k):
        e = me ^ k
        good = (rank_ref[pl.ds(e, 1), :] == slot) & (mark_ref[pl.ds(e, 1), :] > 0.5)
        return jnp.where(good, 1.0, 0.0).astype(BF16)

    for ref, k in zip(outs, far + near + (0,)):
        pick = chosen(k)
        if k in far:
            ref[...] = mm(pick, normed_ref[at]).astype(BF16)
        elif k in near:
            for j in range(groups // 2):
                ref[:, j * width : (j + 1) * width] = mm(
                    pick, normed_ref[2 * j + (at & 1)]
                ).astype(BF16)
        else:
            for q in range(groups):
                ref[:, q * width : (q + 1) * width] = mm(pick, normed_ref[q]).astype(BF16)


def places_body(order, experts, routes_ref, weight_ref, first_ref, second_ref, column_ref, row_ref):
    me = lax.axis_index("ep")
    cap = first_ref.shape[1] // len(order)
    routes = routes_ref[...]
    hits = named(routes, experts)
    rank, _ = ranked(hits)
    row_ref[...] = jnp.zeros_like(row_ref)
    for j in range(TOP_K):
        turn = routes[j : j + 1, :] ^ me
        base = jnp.zeros_like(turn)
        for i, k in enumerate(order):
            base = jnp.where(turn == k, i * cap, base)
        mine = jnp.sum(jnp.where(hits[j], rank, 0.0), axis=0, keepdims=True)
        row_ref[j : j + 1, :] = base.astype(F32) + mine
        row_ref[TOP_K + j : TOP_K + j + 1, :] = weight_ref[j : j + 1, :]
    column = row_ref[...].T
    column_ref[...] = column
    seat = lax.broadcasted_iota(jnp.int32, first_ref.shape, 1)
    for j, ref in enumerate((first_ref, second_ref)):
        place = column[:, j : j + 1].astype(jnp.int32)
        ref[...] = jnp.where(seat == place, 1.0, 0.0).astype(BF16)


def expert_body(plan, cap, wg_ref, wu_ref, wd_ref, *refs):
    mine_ref, other_ref, x_ref, acc_ref = refs[-4:]
    at = lax.axis_index("tp")
    width = mine_ref.shape[1] // 2
    for (block, piece), ref in zip(plan, refs[:-4]):
        rows = slice(block * cap, (block + 1) * cap)
        for j, quarter in enumerate(piece(at)):
            lane = pl.multiple_of(quarter * width, width)
            x_ref[rows, pl.ds(lane, width)] = ref[:, j * width : (j + 1) * width]
    x = x_ref[...]
    hidden = wg_ref.shape[2]
    chunk = min(hidden, 512)
    parts = []
    for c in range(0, hidden, chunk):
        gate = mm(x, wg_ref[0, :, c : c + chunk])
        up = mm(x, wu_ref[0, :, c : c + chunk])
        parts.append((gate * jax.nn.sigmoid(gate) * up).astype(BF16))
    acc_ref[...] = mm(jnp.concatenate(parts, axis=1), wd_ref[0]).astype(BF16)
    for j in range(2):
        cut = slice(j * width, (j + 1) * width)
        lane = pl.multiple_of((2 * j + (at & 1)) * width, width)
        mine_ref[:, cut] = acc_ref[:, pl.ds(lane, width)]
        lane = pl.multiple_of((2 * j + 1 - (at & 1)) * width, width)
        other_ref[:, cut] = acc_ref[:, pl.ds(lane, width)]


def expert_call(wg, wu, wd, pieces, plan, blocks, cap):
    depth, hidden = wg.shape[1:]
    width = wd.shape[2]
    rows = blocks * cap
    half = ((rows, width // 2), BF16)
    return call(
        functools.partial(expert_body, plan, cap),
        [half, half],
        [wg, wu, wd, *pieces],
        6 * rows * depth * hidden,
        scratch=[pltpu.VMEM((rows, depth), BF16), pltpu.VMEM((rows, width), BF16)],
    )


def halve_body(parts, mine_ref, got_ref, keep_ref, *sends):
    width = keep_ref.shape[1]
    side = lax.axis_index("tp") // 2
    rows = keep_ref.shape[0] // parts

    def added(j):
        lane = pl.multiple_of(j * width, width)
        cut = pl.ds(lane, width)
        return (mine_ref[:, cut].astype(F32) + got_ref[:, cut].astype(F32)).astype(BF16)

    keep_ref[...] = added(side)
    send = added(1 - side)
    for i, ref in enumerate(sends):
        ref[...] = send[i * rows : (i + 1) * rows, :]


def add_body(first, keep_ref, got_ref, *outs):
    rows = outs[0].shape[0]
    for i, ref in enumerate(outs):
        cut = slice((first + i) * rows, (first + i + 1) * rows)
        here = slice(i * rows, (i + 1) * rows)
        ref[...] = (keep_ref[cut, :].astype(F32) + got_ref[here, :].astype(F32)).astype(BF16)


def combine_body(column_ref, first_ref, second_ref, *refs):
    out_ref, all_ref = refs[-2:]
    cap = refs[0].shape[0]
    for i, ref in enumerate(refs[:-2]):
        all_ref[i * cap : (i + 1) * cap, :] = ref[...]
    weight = column_ref[:, TOP_K : 2 * TOP_K]
    back = all_ref[...]
    out_ref[...] = (
        weight[:, 0:1] * mm(first_ref[...], back) + weight[:, 1:2] * mm(second_ref[...], back)
    ).astype(BF16)


def carried_in(own, place):
    gathered = lax.all_gather(own, "ep")
    rows = own.shape[0] - ROWS

    def one(turn, state):
        block = lax.dynamic_index_in_dim(gathered, turn, 0, False).astype(F32)
        return after(state, (block[:rows], block[rows : rows + 1]))

    width = own.shape[1]
    start = (jnp.zeros((rows, width), F32), jnp.ones((1, width), F32))
    state, decay = lax.fori_loop(0, place, one, start)
    return jnp.concatenate([state, jnp.broadcast_to(decay, (ROWS, width))], 0).astype(BF16)


def experts_grouped(moe_input, moe_gain, routes, route_weight, w_gate, w_up, w_down):
    count = moe_input.shape[0]
    experts = lax.axis_size("ep")
    cap = 5 * count * TOP_K // (4 * experts)
    x = moe_input.astype(F32)
    scale = lax.rsqrt(jnp.mean(x * x, axis=1, keepdims=True) + EPS)
    normed = (x * scale * moe_gain).astype(BF16)
    flat = routes.reshape(-1)
    one_hot = (flat[:, None] == jnp.arange(experts, dtype=jnp.int32)[None, :]).astype(jnp.int32)
    rank = jnp.sum((jnp.cumsum(one_hot, axis=0) - one_hot) * one_hot, axis=1)
    slot = flat * cap + rank
    owner = jnp.zeros((experts * cap,), jnp.int32).at[slot].set(
        jnp.arange(flat.shape[0], dtype=jnp.int32) // TOP_K
    )
    width = normed.shape[1] // lax.axis_size("tp")
    own = lax.dynamic_slice_in_dim(normed, lax.axis_index("tp") * width, width, 1)[owner]
    arrived = lax.all_to_all(own, "ep", split_axis=0, concat_axis=0, tiled=True)
    rows = lax.all_gather(arrived, "tp", axis=1, tiled=True)
    gate = jnp.dot(rows, w_gate[0], preferred_element_type=F32)
    up = jnp.dot(rows, w_up[0], preferred_element_type=F32)
    hidden = (jax.nn.silu(gate) * up).astype(BF16)
    part = jnp.dot(hidden, w_down[0], preferred_element_type=F32).astype(BF16)
    summed = lax.psum_scatter(part, "tp", scatter_dimension=1, tiled=True)
    back = lax.all_to_all(summed, "ep", split_axis=0, concat_axis=0, tiled=True)
    picked = back[slot].astype(F32).reshape(count, TOP_K, width)
    return jnp.sum(picked * route_weight[:, :, None], axis=1).astype(BF16)


def body(
    direct,
    mix_query,
    forget_input,
    mix_value,
    out_gate_input,
    decay_shift,
    forget_floor,
    head_gain,
    w_mix_out,
    moe_input,
    moe_gain,
    routes,
    route_weight,
    w_exp_gate,
    w_exp_up,
    w_exp_down,
):
    experts = lax.axis_size("ep")
    groups = lax.axis_size("tp")
    me = lax.axis_index("ep").astype(jnp.int32)
    length, width = mix_query.shape
    size = head_gain.shape[0]
    count, depth = moe_input.shape
    slice_width = depth // groups
    cap = -(-5 * count * TOP_K // (4 * experts) // ROWS) * ROWS
    floor = forget_floor.reshape(1, -1)
    head_gain = head_gain.reshape(1, -1)
    half = experts // 2
    near = tuple(range(1, half))
    far = tuple(range(half, experts))
    block = lambda n: ((cap, n), BF16)
    padded = -(-experts // ROWS) * ROWS

    if direct:
        sent = call(
            functools.partial(spread_body, near, far),
            [block(slice_width)] * len(far) + [block(depth // 2)] * len(near) + [block(depth)],
            in_hbm(routes.T, moe_input, moe_gain.reshape(1, -1)),
            2 * experts * cap * count * depth,
            scratch=[
                pltpu.VMEM((groups, count, slice_width), BF16),
                pltpu.VMEM((padded, count), F32),
                pltpu.VMEM((padded, count), F32),
            ],
        )
        own_rows = sent[-1]
        far_in = {k: swap(a, "ep", experts, k) for k, a in zip(far, sent)}
        near_in = {k: swap(a, "ep", experts, k) for k, a in zip(near, sent[len(far) :])}

    state_shape = ((size + ROWS, width), BF16)
    sd, qd, within = call(
        local_body,
        [state_shape, ((length, width), BF16), ((length, width), F32)],
        in_hbm(mix_query, forget_input, mix_value, decay_shift.T, floor),
        8 * length * length * width,
    )
    if direct:
        total, before = sd, None
        bit = 1
        while bit < half:
            got = swap(total, "ep", experts, bit)
            args = [total] + ([] if before is None else [before]) + [got]
            total, before = call(
                functools.partial(scan_body, bit, before is None),
                [state_shape, state_shape],
                args,
                8 * size * width,
            )
            bit *= 2
        got = lax.ppermute(total, "ep", [(i, i ^ bit) for i in range(experts) if not i & bit])
    else:
        bit = 0
        before = carried_in(sd, me)
        got = before
    head_out = call(
        functools.partial(finish_body, bit),
        [((length, width), BF16)],
        [within, qd, before, got, out_gate_input, head_gain],
        2 * length * size * width,
    )[0]
    if direct:
        across = swap(head_out, "tp", groups, 2)
        pieces = [head_out, across]
        pieces += [swap(head_out, "tp", groups, 1), swap(across, "tp", groups, 1)]
        mixed = call(
            functools.partial(mixed_body, (0, 2, 1, 3)),
            [((length, w_mix_out.shape[1]), BF16)],
            [w_mix_out.reshape(groups, width, -1)] + pieces,
            2 * length * groups * width * w_mix_out.shape[1],
        )[0]
    else:
        mixed = jnp.dot(
            lax.all_gather(head_out, "tp", axis=1, tiled=True),
            w_mix_out,
            preferred_element_type=F32,
        ).astype(BF16)
        moe_out = experts_grouped(
            moe_input, moe_gain, routes, route_weight, w_exp_gate, w_exp_up, w_exp_down
        )
        return (mixed, moe_out)

    own_half = lambda at: (at & 1, 2 + (at & 1))
    other_half = lambda at: (1 - (at & 1), 3 - (at & 1))
    only = lambda mask: (lambda at: (at ^ mask,))
    everything = lambda at: tuple(range(groups))

    near_pieces = [own_rows]
    near_plan = [(0, everything)]
    for i, k in enumerate(near):
        near_pieces += [near_in[k], swap(near_in[k], "tp", groups, 1)]
        near_plan += [(i + 1, own_half), (i + 1, other_half)]
    far_pieces = []
    far_plan = []
    for i, k in enumerate(far):
        here = far_in[k]
        there = swap(here, "tp", groups, 2)
        far_pieces += [here, there]
        far_pieces += [swap(here, "tp", groups, 1), swap(there, "tp", groups, 1)]
        far_plan += [(i, only(0)), (i, only(2)), (i, only(1)), (i, only(3))]

    weights = (w_exp_gate, w_exp_up, w_exp_down)
    returned = {}
    for keys, pieces, plan, parts in (
        ((0,) + near, near_pieces, near_plan, 1), (far, far_pieces, far_plan, 2)
    ):
        rows = len(keys) * cap
        mine, other = expert_call(*weights, pieces, plan, len(keys), cap)
        got = swap(other, "tp", groups, 1)
        keep, *sends = call(
            functools.partial(halve_body, parts),
            [((rows, slice_width), BF16)] + [((rows // parts, slice_width), BF16)] * parts,
            [mine, got],
            rows * slice_width * 4,
        )
        per = len(keys) // parts
        for i, send in enumerate(sends):
            back = swap(send, "tp", groups, 2)
            done = call(
                functools.partial(add_body, i * per),
                [block(slice_width)] * per,
                [keep, back],
                rows * slice_width,
            )
            for k, a in zip(keys[i * per : (i + 1) * per], done):
                returned[k] = swap(a, "ep", experts, k) if k else a

    order = (0,) + near + far
    first, second, column = call(
        functools.partial(places_body, order, padded),
        [((count, experts * cap), BF16)] * TOP_K + [((count, 8), F32)],
        [routes.T, route_weight.T],
        2 * count * count * padded,
        scratch=[pltpu.VMEM((8, count), F32)],
    )
    moe_out = call(
        combine_body,
        [((count, slice_width), BF16)],
        [column, first, second] + [returned[k] for k in order],
        4 * count * experts * cap * slice_width,
        scratch=[pltpu.VMEM((experts * cap, slice_width), BF16)],
    )[0]
    return (mixed, moe_out)


def solution(mesh):
    placed = (
        P("ep", "tp"),
        P("ep", "tp"),
        P("ep", "tp"),
        P("ep", "tp"),
        P("ep", "tp"),
        P("tp"),
        P(),
        P(None, "tp"),
        P("ep", None),
        P(),
        P("ep", None),
        P("ep", None),
        P("ep", None, "tp"),
        P("ep", None, "tp"),
        P("ep", "tp", None),
    )
    groups = mesh.shape["tp"]
    experts = mesh.shape["ep"]
    direct = groups == 4 and experts <= 8 and experts & (experts - 1) == 0 and experts >= 4

    def whole(*args):
        return body(direct, *args)

    return jax.shard_map(
        whole,
        mesh=mesh,
        in_specs=placed,
        out_specs=(P("ep", "tp"), P("ep", "tp")),
        check_vma=False,
    )
```

profile of v0, /device:TPU:0, one launch (start us, length us, event | category | flops | bytes accessed | tf_op | source)
XLA Modules:
  0.0 91.4 jit_solution(8451270190890697196)
XLA Ops:
  0.6 2.4 %shard_map.164 = (bf16[80,512]{1,0:T(8,128)(2,1)S(1)}, bf16[80,512]{1,0:T(8,128)(2,1)S(1)}, bf16[80,512]{1,0:T(8,128)(2,1)S(1)}, bf16[80,512]{1,0:T(8,128)(2,1)S...) custom-call(s32[2,256]{1,0:T(2,128)} %bitcast.8, ...), custom_call_target="tpu_custom_call" | custom-call | flops 4000000000 | bytes 1048576 | tf_op jit(solution)/shard_map/pallas_call | solution.py:39
  3.0 4.1 %collective-permute-start.17 = (bf16[80,512]{1,0:T(8,128)(2,1)S(1)}, bf16[80,512]{1,0:T(8,128)(2,1)S(1)}, u32[]{:S(2)}, u32[]{:S(2)}) collective-permute-start(bf16[80,512]{1,0:T(8,128)(2,1)S(1)} %get-tuple-element.59), channel_id=1, source_target_pairs={{0,16},{4,20},{8,24},{12,28},{16,0},{20,4},{24,8},{28,12},{1,17},{... | collective-permute-start | bytes 245768 | tf_op jit(solution)/shard_map/ppermute | solution.py:53
  7.2 1.3 %collective-permute-start.21 = (bf16[80,512]{1,0:T(8,128)(2,1)S(1)}, bf16[80,512]{1,0:T(8,128)(2,1)S(1)}, u32[]{:S(2)}, u32[]{:S(2)}) collective-permute-start(bf16[80,512]{1,0:T(8,128)(2,1)S(1)} %get-tuple-element.60), channel_id=1, source_target_pairs={{0,20},{4,16},{8,28},{12,24},{16,4},{20,0},{24,12},{28,8},{1,21},{... | collective-permute-start | bytes 245768 | tf_op jit(solution)/shard_map/ppermute | solution.py:53
  8.4 2.6 %shard_map.158 = (bf16[144,512]{1,0:T(8,128)(2,1)S(1)}, bf16[256,512]{1,0:T(8,128)(2,1)S(1)}, f32[256,512]{1,0:T(8,128)S(1)}) custom-call(bf16[256,512]{1,0:T(8,128)(2,1)} %q_ref.1, bf16[256,512]{1,0:T(8,128)(2,1)} %x_ref.2, bf16[256,512]{1,0:T(8,128)(2,1)} %v_ref.1, f32[4,256]{1,0:T(4,128)} %bitcast.13, f32[1,512]{1,0:T(1,128)} %bitcast.14), custom_call_target="tpu_custom_call" | custom-call | flops 4000000000 | bytes 1048576 | tf_op jit(solution)/shard_map/pallas_call | solution.py:39
  11.0 0.3 collective-permute-start
  11.3 3.9 %collective-permute-start.25 = (bf16[80,512]{1,0:T(8,128)(2,1)S(1)}, bf16[80,512]{1,0:T(8,128)(2,1)S(1)}, u32[]{:S(2)}, u32[]{:S(2)}) collective-permute-start(bf16[80,512]{1,0:T(8,128)(2,1)S(1)} %get-tuple-element.61), channel_id=1, source_target_pairs={{0,24},{4,28},{8,16},{12,20},{16,8},{20,12},{24,0},{28,4},{1,25},{... | collective-permute-start | bytes 245768 | tf_op jit(solution)/shard_map/ppermute | solution.py:53
  15.2 1.1 %collective-permute-start.29 = (bf16[80,512]{1,0:T(8,128)(2,1)S(1)}, bf16[80,512]{1,0:T(8,128)(2,1)S(1)}, u32[]{:S(2)}, u32[]{:S(2)}) collective-permute-start(bf16[80,512]{1,0:T(8,128)(2,1)S(1)} %get-tuple-element.62), channel_id=1, source_target_pairs={{0,28},{4,24},{8,20},{12,16},{16,12},{20,8},{24,4},{28,0},{1,29},{... | collective-permute-start | bytes 245768 | tf_op jit(solution)/shard_map/ppermute | solution.py:53
  16.3 0.0 collective-permute-done.17.refs_0_
  16.3 1.6 %collective-permute-start.18 = (bf16[80,512]{1,0:T(8,128)(2,1)S(1)}, bf16[80,512]{1,0:T(8,128)(2,1)S(1)}, u32[]{:S(2)}, u32[]{:S(2)}) collective-permute-start(bf16[80,512]{1,0:T(8,128)(2,1)S(1)} %collective-permute-done.17.refs_0_), channel_id=1, source_target_pairs={{0,2},{1,3},{2,0},{3,1},{4,6},{5,7},{6,4},{7,5},{8,10},{9,11},{10,... | collective-permute-start | bytes 245768 | tf_op jit(solution)/shard_map/ppermute | solution.py:53
  17.9 0.0 collective-permute-done.21.refs_4_
  17.9 1.2 %collective-permute-start.22 = (bf16[80,512]{1,0:T(8,128)(2,1)S(1)}, bf16[80,512]{1,0:T(8,128)(2,1)S(1)}, u32[]{:S(2)}, u32[]{:S(2)}) collective-permute-start(bf16[80,512]{1,0:T(8,128)(2,1)S(1)} %collective-permute-done.21.refs_4_), channel_id=1, source_target_pairs={{0,2},{1,3},{2,0},{3,1},{4,6},{5,7},{6,4},{7,5},{8,10},{9,11},{10,... | collective-permute-start | bytes 245768 | tf_op jit(solution)/shard_map/ppermute | solution.py:53
  19.1 0.0 collective-permute-done.25.refs_8_
  19.1 0.9 collective-permute-start.26
  19.9 2.5 %collective-permute-done.29.refs_12_ = bf16[80,512]{1,0:T(8,128)(2,1)S(1)} collective-permute-done((bf16[80,512]{1,0:T(8,128)(2,1)S(1)}, bf16[80,512]{1,0:T(8,128)(2,1)S(1)}, u32[]{:S(2)}, u32[]{:S(2)}) %collective-permute-start.29) | collective-permute-done | bytes 81952 | tf_op jit(solution)/shard_map/ppermute | solution.py:53
  22.4 1.6 %collective-permute-start.30 = (bf16[80,512]{1,0:T(8,128)(2,1)S(1)}, bf16[80,512]{1,0:T(8,128)(2,1)S(1)}, u32[]{:S(2)}, u32[]{:S(2)}) collective-permute-start(bf16[80,512]{1,0:T(8,128)(2,1)S(1)} %collective-permute-done.29.refs_12_), channel_id=1, source_target_pairs={{0,2},{1,3},{2,0},{3,1},{4,6},{5,7},{6,4},{7,5},{8,10},{9,11},{10,... | collective-permute-start | bytes 245768 | tf_op jit(solution)/shard_map/ppermute | solution.py:53
  24.0 1.2 %collective-permute-start.10 = (bf16[80,1024]{1,0:T(8,128)(2,1)S(1)}, bf16[80,1024]{1,0:T(8,128)(2,1)S(1)}, u32[]{:S(2)}, u32[]{:S(2)}) collective-permute-start(bf16[80,1024]{1,0:T(8,128)(2,1)S(1)} %get-tuple-element.50), channel_id=1, source_target_pairs={{0,12},{4,8},{8,4},{12,0},{16,28},{20,24},{24,20},{28,16},{1,13},{... | collective-permute-start | bytes 491528 | tf_op jit(solution)/shard_map/ppermute | solution.py:53
  25.2 1.5 %collective-permute-start.6 = (bf16[80,1024]{1,0:T(8,128)(2,1)S(1)}, bf16[80,1024]{1,0:T(8,128)(2,1)S(1)}, u32[]{:S(2)}, u32[]{:S(2)}) collective-permute-start(bf16[80,1024]{1,0:T(8,128)(2,1)S(1)} %get-tuple-element.48), channel_id=1, source_target_pairs={{0,4},{4,0},{8,12},{12,8},{16,20},{20,16},{24,28},{28,24},{1,5},{5... | collective-permute-start | bytes 491528 | tf_op jit(solution)/shard_map/ppermute | solution.py:53
  26.7 0.2 collective-permute-done.30.refs_13_
  26.9 0.3 collective-permute-start.27
  27.2 0.2 collective-permute-start.31
  27.4 0.6 collective-permute-done.23.refs_6_
  28.0 0.9 collective-permute-start.8
  28.9 0.5 collective-permute-start.24
  29.4 2.7 %collective-permute-done.10.refs_5_ = bf16[80,1024]{1,0:T(8,128)(2,1)S(1)} collective-permute-done((bf16[80,1024]{1,0:T(8,128)(2,1)S(1)}, bf16[80,1024]{1,0:T(8,128)(2,1)S(1)}, u32[]{:S(2)}, u32[]{:S(2)}) %collective-permute-start.10) | collective-permute-done | bytes 163872 | tf_op jit(solution)/shard_map/ppermute | solution.py:53
  32.1 2.9 %collective-permute-done.6.refs_1_ = bf16[80,1024]{1,0:T(8,128)(2,1)S(1)} collective-permute-done((bf16[80,1024]{1,0:T(8,128)(2,1)S(1)}, bf16[80,1024]{1,0:T(8,128)(2,1)S(1)}, u32[]{:S(2)}, u32[]{:S(2)}) %collective-permute-start.6) | collective-permute-done | bytes 163872 | tf_op jit(solution)/shard_map/ppermute | solution.py:53
  35.0 0.1 shard_map.159
  35.1 1.3 %collective-permute-start.1 = (bf16[144,512]{1,0:T(8,128)(2,1)S(1)}, bf16[144,512]{1,0:T(8,128)(2,1)S(1)}, u32[]{:S(2)}, u32[]{:S(2)}) collective-permute-start(bf16[144,512]{1,0:T(8,128)(2,1)S(1)} %get-tuple-element.40.tot_ref), channel_id=1, source_target_pairs={{0,8},{4,12},{8,0},{12,4},{16,24},{20,28},{24,16},{28,20},{1,9},{5... | collective-permute-start | bytes 442376 | tf_op jit(solution)/shard_map/ppermute | solution.py:53
  36.4 0.2 collective-permute-start.11
  36.6 0.3 collective-permute-start.7
  36.9 0.2 collective-permute-start.9
  37.1 4.4 %shard_map.168 = (bf16[320,1024]{1,0:T(8,128)(2,1)S(1)}, bf16[320,1024]{1,0:T(8,128)(2,1)S(1)}) custom-call(bf16[1,2048,1024]{2,1,0:T(8,128)(2,1)S(1)} %copy-done, bf16[1,2048,1024]{2,1,0:T(8,128)(2,1)S(1)} %copy-done.1, bf16[1,1024,2048]{2,1,0:T(8,128)(2,1)S(1)} %copy-done.2, bf16[80,512]{1,0:T(8,128)(2,1)S(1)} %collective-permute-done.17.refs_0_, ...), custom_call_target="tpu_custom_call" | custom-call | flops 4026531840 | bytes 1048576 | tf_op jit(solution)/shard_map/pallas_call | solution.py:39
  41.5 0.4 collective-permute-start.33
  41.9 0.1 shard_map.160
  42.0 3.9 %collective-permute-start.2 = (bf16[144,512]{1,0:T(8,128)(2,1)S(1)}, bf16[144,512]{1,0:T(8,128)(2,1)S(1)}, u32[]{:S(2)}, u32[]{:S(2)}) collective-permute-start(bf16[144,512]{1,0:T(8,128)(2,1)S(1)} %get-tuple-element.43), channel_id=1, source_target_pairs={{0,16},{4,20},{8,24},{12,28},{1,17},{5,21},{9,25},{13,29},{2,18},{... | collective-permute-start | bytes 442376 | tf_op jit(solution)/shard_map/ppermute | solution.py:414
  46.0 0.0 copy-start.4
  46.0 0.0 copy-start.7
  46.0 4.4 %shard_map.165 = (bf16[320,1024]{1,0:T(8,128)(2,1)S(1)}, bf16[320,1024]{1,0:T(8,128)(2,1)S(1)}) custom-call(bf16[1,2048,1024]{2,1,0:T(8,128)(2,1)S(1)} %copy-done, bf16[1,2048,1024]{2,1,0:T(8,128)(2,1)S(1)} %copy-done.1, bf16[1,1024,2048]{2,1,0:T(8,128)(2,1)S(1)} %copy-done.2, bf16[80,2048]{1,0:T(8,128)(2,1)S(1)} %get-tuple-element.47.refs_0_, ...), custom_call_target="tpu_custom_call" | custom-call | flops 4026531840 | bytes 1048576 | tf_op jit(solution)/shard_map/pallas_call | solution.py:39
  50.4 0.1 collective-permute-start.12
  50.5 0.0 copy-start.5
  50.5 0.0 copy-start.6
  50.5 0.4 shard_map.161.refs_0_
  51.0 0.5 collective-permute-start.3
  51.5 0.5 shard_map.163
  52.0 0.3 collective-permute-start.4
  52.3 7.4 %collective-permute-done.3.refs_1_ = bf16[256,512]{1,0:T(8,128)(2,1)S(1)} collective-permute-done((bf16[256,512]{1,0:T(8,128)(2,1)S(1)}, bf16[256,512]{1,0:T(8,128)(2,1)S(1)}, u32[]{:S(2)}, u32[]{:S(2)}) %collective-permute-start.3) | collective-permute-done | bytes 262176 | tf_op jit(solution)/shard_map/ppermute | solution.py:53
  59.7 0.2 shard_map.169
  59.9 0.5 collective-permute-start.37
  60.4 1.5 %collective-permute-start.34 = (bf16[160,512]{1,0:T(8,128)(2,1)S(1)}, bf16[160,512]{1,0:T(8,128)(2,1)S(1)}, u32[]{:S(2)}, u32[]{:S(2)}) collective-permute-start(bf16[160,512]{1,0:T(8,128)(2,1)S(1)} %get-tuple-element.66), channel_id=1, source_target_pairs={{0,2},{1,3},{2,0},{3,1},{4,6},{5,7},{6,4},{7,5},{8,10},{9,11},{10,... | collective-permute-start | bytes 491528 | tf_op jit(solution)/shard_map/ppermute | solution.py:53
  62.0 0.2 shard_map.166
  62.2 0.5 collective-permute-start.13
  62.7 4.3 %collective-permute-done.37.got_ref = bf16[160,512]{1,0:T(8,128)(2,1)S(1)} collective-permute-done((bf16[160,512]{1,0:T(8,128)(2,1)S(1)}, bf16[160,512]{1,0:T(8,128)(2,1)S(1)}, u32[]{:S(2)}, u32[]{:S(2)}) %collective-permute-start.37) | collective-permute-done | bytes 163872 | tf_op jit(solution)/shard_map/ppermute | solution.py:53
  67.1 5.5 %collective-permute-start.38 = (bf16[80,512]{1,0:T(8,128)(2,1)S(1)}, bf16[80,512]{1,0:T(8,128)(2,1)S(1)}, u32[]{:S(2)}, u32[]{:S(2)}) collective-permute-start(bf16[80,512]{1,0:T(8,128)(2,1)S(1)} %get-tuple-element.70), channel_id=1, source_target_pairs={{0,24},{4,28},{8,16},{12,20},{16,8},{20,12},{24,0},{28,4},{1,25},{... | collective-permute-start | bytes 245768 | tf_op jit(solution)/shard_map/ppermute | solution.py:53
  72.6 4.0 %collective-permute-start.39 = (bf16[80,512]{1,0:T(8,128)(2,1)S(1)}, bf16[80,512]{1,0:T(8,128)(2,1)S(1)}, u32[]{:S(2)}, u32[]{:S(2)}) collective-permute-start(bf16[80,512]{1,0:T(8,128)(2,1)S(1)} %get-tuple-element.71), channel_id=1, source_target_pairs={{0,28},{4,24},{8,20},{12,16},{16,12},{20,8},{24,4},{28,0},{1,29},{... | collective-permute-start | bytes 245768 | tf_op jit(solution)/shard_map/ppermute | solution.py:53
  76.6 0.5 collective-permute-done.13.got_ref
  77.1 0.7 collective-permute-start.35
  77.8 0.1 shard_map.167
  77.9 2.7 %collective-permute-start.36 = (bf16[80,512]{1,0:T(8,128)(2,1)S(1)}, bf16[80,512]{1,0:T(8,128)(2,1)S(1)}, u32[]{:S(2)}, u32[]{:S(2)}) collective-permute-start(bf16[80,512]{1,0:T(8,128)(2,1)S(1)} %get-tuple-element.68), channel_id=1, source_target_pairs={{0,20},{4,16},{8,28},{12,24},{16,4},{20,0},{24,12},{28,8},{1,21},{... | collective-permute-start | bytes 245768 | tf_op jit(solution)/shard_map/ppermute | solution.py:53
  80.6 1.1 %collective-permute-start.14 = (bf16[80,512]{1,0:T(8,128)(2,1)S(1)}, bf16[80,512]{1,0:T(8,128)(2,1)S(1)}, u32[]{:S(2)}, u32[]{:S(2)}) collective-permute-start(bf16[80,512]{1,0:T(8,128)(2,1)S(1)} %get-tuple-element.56), channel_id=1, source_target_pairs={{0,4},{4,0},{8,12},{12,8},{16,20},{20,16},{24,28},{28,24},{1,5},{5... | collective-permute-start | bytes 245768 | tf_op jit(solution)/shard_map/ppermute | solution.py:53
  81.7 3.1 %collective-permute-start.15 = (bf16[80,512]{1,0:T(8,128)(2,1)S(1)}, bf16[80,512]{1,0:T(8,128)(2,1)S(1)}, u32[]{:S(2)}, u32[]{:S(2)}) collective-permute-start(bf16[80,512]{1,0:T(8,128)(2,1)S(1)} %get-tuple-element.57), channel_id=1, source_target_pairs={{0,8},{4,12},{8,0},{12,4},{16,24},{20,28},{24,16},{28,20},{1,9},{5... | collective-permute-start | bytes 245768 | tf_op jit(solution)/shard_map/ppermute | solution.py:53
  84.8 0.6 collective-permute-start.16
  85.4 1.4 %shard_map.162 = bf16[256,512]{1,0:T(8,128)(2,1)} custom-call(bf16[4,512,512]{2,1,0:T(8,128)(2,1)S(1)} %bitcast.7, bf16[256,512]{1,0:T(8,128)(2,1)S(1)} %shard_map.161.refs_0_, bf16[256,512]{1,0:T(8,128)(2,1)S(1)} %collective-permute-done.3.refs_1_, bf16[256,512]{1,0:T(8,128)(2,1)S(1)} %collective-permute-done.4.refs_2_, ...), custom_call_target="tpu_custom_call" | custom-call | flops 4000000000 | bytes 1048576 | tf_op jit(solution)/shard_map/pallas_call | solution.py:39
  86.8 1.1 %collective-permute-done.15.refs_2_ = bf16[80,512]{1,0:T(8,128)(2,1)S(1)} collective-permute-done((bf16[80,512]{1,0:T(8,128)(2,1)S(1)}, bf16[80,512]{1,0:T(8,128)(2,1)S(1)}, u32[]{:S(2)}, u32[]{:S(2)}) %collective-permute-start.15) | collective-permute-done | bytes 81952 | tf_op jit(solution)/shard_map/ppermute | solution.py:53
  87.9 2.2 %collective-permute-done.16.refs_3_ = bf16[80,512]{1,0:T(8,128)(2,1)S(1)} collective-permute-done((bf16[80,512]{1,0:T(8,128)(2,1)S(1)}, bf16[80,512]{1,0:T(8,128)(2,1)S(1)}, u32[]{:S(2)}, u32[]{:S(2)}) %collective-permute-start.16) | collective-permute-done | bytes 81952 | tf_op jit(solution)/shard_map/ppermute | solution.py:53
  90.1 1.3 %shard_map.172 = bf16[256,512]{1,0:T(8,128)(2,1)} custom-call(f32[256,8]{1,0:T(8,128)S(1)} %get-tuple-element.44.column_ref, bf16[256,640]{1,0:T(8,128)(2,1)S(1)} %get-tuple-element.45.first_ref, bf16[256,640]{1,0:T(8,128)(2,1)S(1)} %get-tuple-element.46.second_ref, bf16[80,512]{1,0:T(8,128)(2,1)S(1)} %get-tuple-element.55.refs_0_, ...), custom_call_target="tpu_custom_call" | custom-call | flops 4000000000 | bytes 1048576 | tf_op jit(solution)/shard_map/pallas_call | solution.py:39
  (47 shorter events, 0.2 us)
Async XLA Ops:
  3.0 13.3 %collective-permute-start.17 = (bf16[80,512]{1,0:T(8,128)(2,1)S(1)}, bf16[80,512]{1,0:T(8,128)(2,1)S(1)}, u32[]{:S(2)}, u32[]{:S(2)}) collective-permute-start(bf16[80,512]{1,0:T(8,128)(2,1)S(1)} %get-tuple-element.59), channel_id=1, source_target_pairs={{0,16},{4,20},{8,24},{12,28},{16,0},{20,4},{24,8},{28,12},{1,17},{... | collective-permute-start | bytes 245768 | tf_op jit(solution)/shard_map/ppermute | solution.py:53
  7.2 10.8 %collective-permute-start.21 = (bf16[80,512]{1,0:T(8,128)(2,1)S(1)}, bf16[80,512]{1,0:T(8,128)(2,1)S(1)}, u32[]{:S(2)}, u32[]{:S(2)}) collective-permute-start(bf16[80,512]{1,0:T(8,128)(2,1)S(1)} %get-tuple-element.60), channel_id=1, source_target_pairs={{0,20},{4,16},{8,28},{12,24},{16,4},{20,0},{24,12},{28,8},{1,21},{... | collective-permute-start | bytes 245768 | tf_op jit(solution)/shard_map/ppermute | solution.py:53
  11.0 13.0 %collective-permute-start = (bf16[144,512]{1,0:T(8,128)(2,1)S(1)}, bf16[144,512]{1,0:T(8,128)(2,1)S(1)}, u32[]{:S(2)}, u32[]{:S(2)}) collective-permute-start(bf16[144,512]{1,0:T(8,128)(2,1)S(1)} %get-tuple-element.39.tot_ref), channel_id=1, source_target_pairs={{0,4},{4,0},{8,12},{12,8},{16,20},{20,16},{24,28},{28,24},{1,5},{5... | collective-permute-start | bytes 442376 | tf_op jit(solution)/shard_map/ppermute | solution.py:53
  11.3 7.7 %collective-permute-start.25 = (bf16[80,512]{1,0:T(8,128)(2,1)S(1)}, bf16[80,512]{1,0:T(8,128)(2,1)S(1)}, u32[]{:S(2)}, u32[]{:S(2)}) collective-permute-start(bf16[80,512]{1,0:T(8,128)(2,1)S(1)} %get-tuple-element.61), channel_id=1, source_target_pairs={{0,24},{4,28},{8,16},{12,20},{16,8},{20,12},{24,0},{28,4},{1,25},{... | collective-permute-start | bytes 245768 | tf_op jit(solution)/shard_map/ppermute | solution.py:53
  15.2 7.2 %collective-permute-start.29 = (bf16[80,512]{1,0:T(8,128)(2,1)S(1)}, bf16[80,512]{1,0:T(8,128)(2,1)S(1)}, u32[]{:S(2)}, u32[]{:S(2)}) collective-permute-start(bf16[80,512]{1,0:T(8,128)(2,1)S(1)} %get-tuple-element.62), channel_id=1, source_target_pairs={{0,28},{4,24},{8,20},{12,16},{16,12},{20,8},{24,4},{28,0},{1,29},{... | collective-permute-start | bytes 245768 | tf_op jit(solution)/shard_map/ppermute | solution.py:53
  16.3 7.7 %collective-permute-start.18 = (bf16[80,512]{1,0:T(8,128)(2,1)S(1)}, bf16[80,512]{1,0:T(8,128)(2,1)S(1)}, u32[]{:S(2)}, u32[]{:S(2)}) collective-permute-start(bf16[80,512]{1,0:T(8,128)(2,1)S(1)} %collective-permute-done.17.refs_0_), channel_id=1, source_target_pairs={{0,2},{1,3},{2,0},{3,1},{4,6},{5,7},{6,4},{7,5},{8,10},{9,11},{10,... | collective-permute-start | bytes 245768 | tf_op jit(solution)/shard_map/ppermute | solution.py:53
  17.9 7.3 %collective-permute-start.22 = (bf16[80,512]{1,0:T(8,128)(2,1)S(1)}, bf16[80,512]{1,0:T(8,128)(2,1)S(1)}, u32[]{:S(2)}, u32[]{:S(2)}) collective-permute-start(bf16[80,512]{1,0:T(8,128)(2,1)S(1)} %collective-permute-done.21.refs_4_), channel_id=1, source_target_pairs={{0,2},{1,3},{2,0},{3,1},{4,6},{5,7},{6,4},{7,5},{8,10},{9,11},{10,... | collective-permute-start | bytes 245768 | tf_op jit(solution)/shard_map/ppermute | solution.py:53
  19.1 7.6 %collective-permute-start.26 = (bf16[80,512]{1,0:T(8,128)(2,1)S(1)}, bf16[80,512]{1,0:T(8,128)(2,1)S(1)}, u32[]{:S(2)}, u32[]{:S(2)}) collective-permute-start(bf16[80,512]{1,0:T(8,128)(2,1)S(1)} %collective-permute-done.25.refs_8_), channel_id=1, source_target_pairs={{0,2},{1,3},{2,0},{3,1},{4,6},{5,7},{6,4},{7,5},{8,10},{9,11},{10,... | collective-permute-start | bytes 245768 | tf_op jit(solution)/shard_map/ppermute | solution.py:53
  22.4 4.4 %collective-permute-start.30 = (bf16[80,512]{1,0:T(8,128)(2,1)S(1)}, bf16[80,512]{1,0:T(8,128)(2,1)S(1)}, u32[]{:S(2)}, u32[]{:S(2)}) collective-permute-start(bf16[80,512]{1,0:T(8,128)(2,1)S(1)} %collective-permute-done.29.refs_12_), channel_id=1, source_target_pairs={{0,2},{1,3},{2,0},{3,1},{4,6},{5,7},{6,4},{7,5},{8,10},{9,11},{10,... | collective-permute-start | bytes 245768 | tf_op jit(solution)/shard_map/ppermute | solution.py:53
  24.0 3.2 %collective-permute-start.19 = (bf16[80,512]{1,0:T(8,128)(2,1)S(1)}, bf16[80,512]{1,0:T(8,128)(2,1)S(1)}, u32[]{:S(2)}, u32[]{:S(2)}) collective-permute-start(bf16[80,512]{1,0:T(8,128)(2,1)S(1)} %collective-permute-done.17.refs_0_), channel_id=1, source_target_pairs={{0,1},{1,0},{2,3},{3,2},{4,5},{5,4},{6,7},{7,6},{8,9},{9,8},{10,11... | collective-permute-start | bytes 245768 | tf_op jit(solution)/shard_map/ppermute | solution.py:53
  24.0 8.1 %collective-permute-start.10 = (bf16[80,1024]{1,0:T(8,128)(2,1)S(1)}, bf16[80,1024]{1,0:T(8,128)(2,1)S(1)}, u32[]{:S(2)}, u32[]{:S(2)}) collective-permute-start(bf16[80,1024]{1,0:T(8,128)(2,1)S(1)} %get-tuple-element.50), channel_id=1, source_target_pairs={{0,12},{4,8},{8,4},{12,0},{16,28},{20,24},{24,20},{28,16},{1,13},{... | collective-permute-start | bytes 491528 | tf_op jit(solution)/shard_map/ppermute | solution.py:53
  25.2 9.8 %collective-permute-start.6 = (bf16[80,1024]{1,0:T(8,128)(2,1)S(1)}, bf16[80,1024]{1,0:T(8,128)(2,1)S(1)}, u32[]{:S(2)}, u32[]{:S(2)}) collective-permute-start(bf16[80,1024]{1,0:T(8,128)(2,1)S(1)} %get-tuple-element.48), channel_id=1, source_target_pairs={{0,4},{4,0},{8,12},{12,8},{16,20},{20,16},{24,28},{28,24},{1,5},{5... | collective-permute-start | bytes 491528 | tf_op jit(solution)/shard_map/ppermute | solution.py:53
  26.7 1.3 %collective-permute-start.23 = (bf16[80,512]{1,0:T(8,128)(2,1)S(1)}, bf16[80,512]{1,0:T(8,128)(2,1)S(1)}, u32[]{:S(2)}, u32[]{:S(2)}) collective-permute-start(bf16[80,512]{1,0:T(8,128)(2,1)S(1)} %collective-permute-done.21.refs_4_), channel_id=1, source_target_pairs={{0,1},{1,0},{2,3},{3,2},{4,5},{5,4},{6,7},{7,6},{8,9},{9,8},{10,11... | collective-permute-start | bytes 245768 | tf_op jit(solution)/shard_map/ppermute | solution.py:53
  26.9 2.0 %collective-permute-start.27 = (bf16[80,512]{1,0:T(8,128)(2,1)S(1)}, bf16[80,512]{1,0:T(8,128)(2,1)S(1)}, u32[]{:S(2)}, u32[]{:S(2)}) collective-permute-start(bf16[80,512]{1,0:T(8,128)(2,1)S(1)} %collective-permute-done.25.refs_8_), channel_id=1, source_target_pairs={{0,1},{1,0},{2,3},{3,2},{4,5},{5,4},{6,7},{7,6},{8,9},{9,8},{10,11... | collective-permute-start | bytes 245768 | tf_op jit(solution)/shard_map/ppermute | solution.py:53
  27.2 1.7 %collective-permute-start.31 = (bf16[80,512]{1,0:T(8,128)(2,1)S(1)}, bf16[80,512]{1,0:T(8,128)(2,1)S(1)}, u32[]{:S(2)}, u32[]{:S(2)}) collective-permute-start(bf16[80,512]{1,0:T(8,128)(2,1)S(1)} %collective-permute-done.29.refs_12_), channel_id=1, source_target_pairs={{0,1},{1,0},{2,3},{3,2},{4,5},{5,4},{6,7},{7,6},{8,9},{9,8},{10,11... | collective-permute-start | bytes 245768 | tf_op jit(solution)/shard_map/ppermute | solution.py:53
  28.0 9.1 %copy-start = (bf16[1,2048,1024]{2,1,0:T(8,128)(2,1)S(1)}, bf16[1,2048,1024]{2,1,0:T(8,128)(2,1)}, u32[]{:S(2)}) copy-start(bf16[1,2048,1024]{2,1,0:T(8,128)(2,1)} %wg_ref.3) | copy-start | bytes 12582916
  28.0 9.1 %copy-start.1 = (bf16[1,2048,1024]{2,1,0:T(8,128)(2,1)S(1)}, bf16[1,2048,1024]{2,1,0:T(8,128)(2,1)}, u32[]{:S(2)}) copy-start(bf16[1,2048,1024]{2,1,0:T(8,128)(2,1)} %wu_ref.3) | copy-start | bytes 12582916
  28.0 9.1 %copy-start.2 = (bf16[1,1024,2048]{2,1,0:T(8,128)(2,1)S(1)}, bf16[1,1024,2048]{2,1,0:T(8,128)(2,1)}, u32[]{:S(2)}) copy-start(bf16[1,1024,2048]{2,1,0:T(8,128)(2,1)} %wd_ref.3) | copy-start | bytes 12582916
  28.0 7.1 %collective-permute-start.8 = (bf16[80,1024]{1,0:T(8,128)(2,1)S(1)}, bf16[80,1024]{1,0:T(8,128)(2,1)S(1)}, u32[]{:S(2)}, u32[]{:S(2)}) collective-permute-start(bf16[80,1024]{1,0:T(8,128)(2,1)S(1)} %get-tuple-element.49), channel_id=1, source_target_pairs={{0,8},{4,12},{8,0},{12,4},{16,24},{20,28},{24,16},{28,20},{1,9},{5... | collective-permute-start | bytes 491528 | tf_op jit(solution)/shard_map/ppermute | solution.py:53
  28.9 7.5 %collective-permute-start.20 = (bf16[80,512]{1,0:T(8,128)(2,1)S(1)}, bf16[80,512]{1,0:T(8,128)(2,1)S(1)}, u32[]{:S(2)}, u32[]{:S(2)}) collective-permute-start(bf16[80,512]{1,0:T(8,128)(2,1)S(1)} %collective-permute-done.18.refs_1_), channel_id=1, source_target_pairs={{0,1},{1,0},{2,3},{3,2},{4,5},{5,4},{6,7},{7,6},{8,9},{9,8},{10,11... | collective-permute-start | bytes 245768 | tf_op jit(solution)/shard_map/ppermute | solution.py:53
  28.9 7.7 %collective-permute-start.24 = (bf16[80,512]{1,0:T(8,128)(2,1)S(1)}, bf16[80,512]{1,0:T(8,128)(2,1)S(1)}, u32[]{:S(2)}, u32[]{:S(2)}) collective-permute-start(bf16[80,512]{1,0:T(8,128)(2,1)S(1)} %collective-permute-done.22.refs_5_), channel_id=1, source_target_pairs={{0,1},{1,0},{2,3},{3,2},{4,5},{5,4},{6,7},{7,6},{8,9},{9,8},{10,11... | collective-permute-start | bytes 245768 | tf_op jit(solution)/shard_map/ppermute | solution.py:53
  32.1 4.8 %collective-permute-start.28 = (bf16[80,512]{1,0:T(8,128)(2,1)S(1)}, bf16[80,512]{1,0:T(8,128)(2,1)S(1)}, u32[]{:S(2)}, u32[]{:S(2)}) collective-permute-start(bf16[80,512]{1,0:T(8,128)(2,1)S(1)} %collective-permute-done.26.refs_9_), channel_id=1, source_target_pairs={{0,1},{1,0},{2,3},{3,2},{4,5},{5,4},{6,7},{7,6},{8,9},{9,8},{10,11... | collective-permute-start | bytes 245768 | tf_op jit(solution)/shard_map/ppermute | solution.py:53
  35.0 2.1 %collective-permute-start.32 = (bf16[80,512]{1,0:T(8,128)(2,1)S(1)}, bf16[80,512]{1,0:T(8,128)(2,1)S(1)}, u32[]{:S(2)}, u32[]{:S(2)}) collective-permute-start(bf16[80,512]{1,0:T(8,128)(2,1)S(1)} %collective-permute-done.30.refs_13_), channel_id=1, source_target_pairs={{0,1},{1,0},{2,3},{3,2},{4,5},{5,4},{6,7},{7,6},{8,9},{9,8},{10,11... | collective-permute-start | bytes 245768 | tf_op jit(solution)/shard_map/ppermute | solution.py:53
  35.1 6.9 %collective-permute-start.1 = (bf16[144,512]{1,0:T(8,128)(2,1)S(1)}, bf16[144,512]{1,0:T(8,128)(2,1)S(1)}, u32[]{:S(2)}, u32[]{:S(2)}) collective-permute-start(bf16[144,512]{1,0:T(8,128)(2,1)S(1)} %get-tuple-element.40.tot_ref), channel_id=1, source_target_pairs={{0,8},{4,12},{8,0},{12,4},{16,24},{20,28},{24,16},{28,20},{1,9},{5... | collective-permute-start | bytes 442376 | tf_op jit(solution)/shard_map/ppermute | solution.py:53
  36.4 9.5 %collective-permute-start.11 = (bf16[80,1024]{1,0:T(8,128)(2,1)S(1)}, bf16[80,1024]{1,0:T(8,128)(2,1)S(1)}, u32[]{:S(2)}, u32[]{:S(2)}) collective-permute-start(bf16[80,1024]{1,0:T(8,128)(2,1)S(1)} %collective-permute-done.10.refs_5_), channel_id=1, source_target_pairs={{0,1},{1,0},{2,3},{3,2},{4,5},{5,4},{6,7},{7,6},{8,9},{9,8},{10,11... | collective-permute-start | bytes 491528 | tf_op jit(solution)/shard_map/ppermute | solution.py:53
  36.6 9.4 %collective-permute-start.7 = (bf16[80,1024]{1,0:T(8,128)(2,1)S(1)}, bf16[80,1024]{1,0:T(8,128)(2,1)S(1)}, u32[]{:S(2)}, u32[]{:S(2)}) collective-permute-start(bf16[80,1024]{1,0:T(8,128)(2,1)S(1)} %collective-permute-done.6.refs_1_), channel_id=1, source_target_pairs={{0,1},{1,0},{2,3},{3,2},{4,5},{5,4},{6,7},{7,6},{8,9},{9,8},{10,11... | collective-permute-start | bytes 491528 | tf_op jit(solution)/shard_map/ppermute | solution.py:53
  36.9 9.1 %collective-permute-start.9 = (bf16[80,1024]{1,0:T(8,128)(2,1)S(1)}, bf16[80,1024]{1,0:T(8,128)(2,1)S(1)}, u32[]{:S(2)}, u32[]{:S(2)}) collective-permute-start(bf16[80,1024]{1,0:T(8,128)(2,1)S(1)} %collective-permute-done.8.refs_3_), channel_id=1, source_target_pairs={{0,1},{1,0},{2,3},{3,2},{4,5},{5,4},{6,7},{7,6},{8,9},{9,8},{10,11... | collective-permute-start | bytes 491528 | tf_op jit(solution)/shard_map/ppermute | solution.py:53
  41.5 18.2 %collective-permute-start.33 = (bf16[320,1024]{1,0:T(8,128)(2,1)S(1)}, bf16[320,1024]{1,0:T(8,128)(2,1)S(1)}, u32[]{:S(2)}, u32[]{:S(2)}) collective-permute-start(bf16[320,1024]{1,0:T(8,128)(2,1)S(1)} %get-tuple-element.64), channel_id=1, source_target_pairs={{0,1},{1,0},{2,3},{3,2},{4,5},{5,4},{6,7},{7,6},{8,9},{9,8},{10,11... | collective-permute-start | bytes 1966088 | tf_op jit(solution)/shard_map/ppermute | solution.py:53
  42.0 8.4 %collective-permute-start.2 = (bf16[144,512]{1,0:T(8,128)(2,1)S(1)}, bf16[144,512]{1,0:T(8,128)(2,1)S(1)}, u32[]{:S(2)}, u32[]{:S(2)}) collective-permute-start(bf16[144,512]{1,0:T(8,128)(2,1)S(1)} %get-tuple-element.43), channel_id=1, source_target_pairs={{0,16},{4,20},{8,24},{12,28},{1,17},{5,21},{9,25},{13,29},{2,18},{... | collective-permute-start | bytes 442376 | tf_op jit(solution)/shard_map/ppermute | solution.py:414
  46.0 4.5 %copy-start.4 = (bf16[256,512]{1,0:T(8,128)(2,1)S(1)}, bf16[256,512]{1,0:T(8,128)(2,1)}, u32[]{:S(2)}) copy-start(bf16[256,512]{1,0:T(8,128)(2,1)} %gate_ref.1) | copy-start | bytes 786436
  46.0 4.5 %copy-start.7 = (f32[128]{0:T(128)S(1)}, f32[128]{0:T(128)}, u32[]{:S(2)}) copy-start(f32[128]{0:T(128)} %param.21) | copy-start | bytes 1540
  50.4 11.6 %collective-permute-start.12 = (bf16[320,1024]{1,0:T(8,128)(2,1)S(1)}, bf16[320,1024]{1,0:T(8,128)(2,1)S(1)}, u32[]{:S(2)}, u32[]{:S(2)}) collective-permute-start(bf16[320,1024]{1,0:T(8,128)(2,1)S(1)} %get-tuple-element.52), channel_id=1, source_target_pairs={{0,1},{1,0},{2,3},{3,2},{4,5},{5,4},{6,7},{7,6},{8,9},{9,8},{10,11... | collective-permute-start | bytes 1966088 | tf_op jit(solution)/shard_map/ppermute | solution.py:53
  50.5 1.0 %copy-start.5 = (s32[256,2]{0,1:T(2,128)S(1)}, s32[256,2]{0,1:T(2,128)}, u32[]{:S(2)}) copy-start(s32[256,2]{0,1:T(2,128)} %param.25) | copy-start | bytes 6148
  50.5 1.0 %copy-start.6 = (f32[256,2]{0,1:T(2,128)S(1)}, f32[256,2]{0,1:T(2,128)}, u32[]{:S(2)}) copy-start(f32[256,2]{0,1:T(2,128)} %param.26) | copy-start | bytes 6148
  51.0 8.8 %collective-permute-start.3 = (bf16[256,512]{1,0:T(8,128)(2,1)S(1)}, bf16[256,512]{1,0:T(8,128)(2,1)S(1)}, u32[]{:S(2)}, u32[]{:S(2)}) collective-permute-start(bf16[256,512]{1,0:T(8,128)(2,1)S(1)} %shard_map.161.refs_0_), channel_id=1, source_target_pairs={{0,2},{1,3},{2,0},{3,1},{4,6},{5,7},{6,4},{7,5},{8,10},{9,11},{10,... | collective-permute-start | bytes 786440 | tf_op jit(solution)/shard_map/ppermute | solution.py:53
  52.0 25.9 %collective-permute-start.4 = (bf16[256,512]{1,0:T(8,128)(2,1)S(1)}, bf16[256,512]{1,0:T(8,128)(2,1)S(1)}, u32[]{:S(2)}, u32[]{:S(2)}) collective-permute-start(bf16[256,512]{1,0:T(8,128)(2,1)S(1)} %shard_map.161.refs_0_), channel_id=1, source_target_pairs={{0,1},{1,0},{2,3},{3,2},{4,5},{5,4},{6,7},{7,6},{8,9},{9,8},{10,11... | collective-permute-start | bytes 786440 | tf_op jit(solution)/shard_map/ppermute | solution.py:53
  59.7 20.9 %collective-permute-start.5 = (bf16[256,512]{1,0:T(8,128)(2,1)S(1)}, bf16[256,512]{1,0:T(8,128)(2,1)S(1)}, u32[]{:S(2)}, u32[]{:S(2)}) collective-permute-start(bf16[256,512]{1,0:T(8,128)(2,1)S(1)} %collective-permute-done.3.refs_1_), channel_id=1, source_target_pairs={{0,1},{1,0},{2,3},{3,2},{4,5},{5,4},{6,7},{7,6},{8,9},{9,8},{10,11... | collective-permute-start | bytes 786440 | tf_op jit(solution)/shard_map/ppermute | solution.py:53
  59.9 7.1 %collective-permute-start.37 = (bf16[160,512]{1,0:T(8,128)(2,1)S(1)}, bf16[160,512]{1,0:T(8,128)(2,1)S(1)}, u32[]{:S(2)}, u32[]{:S(2)}) collective-permute-start(bf16[160,512]{1,0:T(8,128)(2,1)S(1)} %get-tuple-element.69), channel_id=1, source_target_pairs={{0,2},{1,3},{2,0},{3,1},{4,6},{5,7},{6,4},{7,5},{8,10},{9,11},{10,... | collective-permute-start | bytes 491528 | tf_op jit(solution)/shard_map/ppermute | solution.py:53
  60.4 12.2 %collective-permute-start.34 = (bf16[160,512]{1,0:T(8,128)(2,1)S(1)}, bf16[160,512]{1,0:T(8,128)(2,1)S(1)}, u32[]{:S(2)}, u32[]{:S(2)}) collective-permute-start(bf16[160,512]{1,0:T(8,128)(2,1)S(1)} %get-tuple-element.66), channel_id=1, source_target_pairs={{0,2},{1,3},{2,0},{3,1},{4,6},{5,7},{6,4},{7,5},{8,10},{9,11},{10,... | collective-permute-start | bytes 491528 | tf_op jit(solution)/shard_map/ppermute | solution.py:53
  62.2 14.9 %collective-permute-start.13 = (bf16[320,512]{1,0:T(8,128)(2,1)S(1)}, bf16[320,512]{1,0:T(8,128)(2,1)S(1)}, u32[]{:S(2)}, u32[]{:S(2)}) collective-permute-start(bf16[320,512]{1,0:T(8,128)(2,1)S(1)} %get-tuple-element.54), channel_id=1, source_target_pairs={{0,2},{1,3},{2,0},{3,1},{4,6},{5,7},{6,4},{7,5},{8,10},{9,11},{10,... | collective-permute-start | bytes 983048 | tf_op jit(solution)/shard_map/ppermute | solution.py:53
  67.1 14.6 %collective-permute-start.38 = (bf16[80,512]{1,0:T(8,128)(2,1)S(1)}, bf16[80,512]{1,0:T(8,128)(2,1)S(1)}, u32[]{:S(2)}, u32[]{:S(2)}) collective-permute-start(bf16[80,512]{1,0:T(8,128)(2,1)S(1)} %get-tuple-element.70), channel_id=1, source_target_pairs={{0,24},{4,28},{8,16},{12,20},{16,8},{20,12},{24,0},{28,4},{1,25},{... | collective-permute-start | bytes 245768 | tf_op jit(solution)/shard_map/ppermute | solution.py:53
  72.6 12.2 %collective-permute-start.39 = (bf16[80,512]{1,0:T(8,128)(2,1)S(1)}, bf16[80,512]{1,0:T(8,128)(2,1)S(1)}, u32[]{:S(2)}, u32[]{:S(2)}) collective-permute-start(bf16[80,512]{1,0:T(8,128)(2,1)S(1)} %get-tuple-element.71), channel_id=1, source_target_pairs={{0,28},{4,24},{8,20},{12,16},{16,12},{20,8},{24,4},{28,0},{1,29},{... | collective-permute-start | bytes 245768 | tf_op jit(solution)/shard_map/ppermute | solution.py:53
  77.1 9.7 %collective-permute-start.35 = (bf16[80,512]{1,0:T(8,128)(2,1)S(1)}, bf16[80,512]{1,0:T(8,128)(2,1)S(1)}, u32[]{:S(2)}, u32[]{:S(2)}) collective-permute-start(bf16[80,512]{1,0:T(8,128)(2,1)S(1)} %get-tuple-element.67), channel_id=1, source_target_pairs={{0,16},{4,20},{8,24},{12,28},{16,0},{20,4},{24,8},{28,12},{1,17},{... | collective-permute-start | bytes 245768 | tf_op jit(solution)/shard_map/ppermute | solution.py:53
  77.8 7.6 %copy-start.3 = (bf16[2048,512]{1,0:T(8,128)(2,1)S(1)}, bf16[2048,512]{1,0:T(8,128)(2,1)}, u32[]{:S(2)}) copy-start(bf16[2048,512]{1,0:T(8,128)(2,1)} %param.22) | copy-start | bytes 6291460
  77.9 8.9 %collective-permute-start.36 = (bf16[80,512]{1,0:T(8,128)(2,1)S(1)}, bf16[80,512]{1,0:T(8,128)(2,1)S(1)}, u32[]{:S(2)}, u32[]{:S(2)}) collective-permute-start(bf16[80,512]{1,0:T(8,128)(2,1)S(1)} %get-tuple-element.68), channel_id=1, source_target_pairs={{0,20},{4,16},{8,28},{12,24},{16,4},{20,0},{24,12},{28,8},{1,21},{... | collective-permute-start | bytes 245768 | tf_op jit(solution)/shard_map/ppermute | solution.py:53
  80.6 6.2 %collective-permute-start.14 = (bf16[80,512]{1,0:T(8,128)(2,1)S(1)}, bf16[80,512]{1,0:T(8,128)(2,1)S(1)}, u32[]{:S(2)}, u32[]{:S(2)}) collective-permute-start(bf16[80,512]{1,0:T(8,128)(2,1)S(1)} %get-tuple-element.56), channel_id=1, source_target_pairs={{0,4},{4,0},{8,12},{12,8},{16,20},{20,16},{24,28},{28,24},{1,5},{5... | collective-permute-start | bytes 245768 | tf_op jit(solution)/shard_map/ppermute | solution.py:53
  81.7 6.2 %collective-permute-start.15 = (bf16[80,512]{1,0:T(8,128)(2,1)S(1)}, bf16[80,512]{1,0:T(8,128)(2,1)S(1)}, u32[]{:S(2)}, u32[]{:S(2)}) collective-permute-start(bf16[80,512]{1,0:T(8,128)(2,1)S(1)} %get-tuple-element.57), channel_id=1, source_target_pairs={{0,8},{4,12},{8,0},{12,4},{16,24},{20,28},{24,16},{28,20},{1,9},{5... | collective-permute-start | bytes 245768 | tf_op jit(solution)/shard_map/ppermute | solution.py:53
  84.8 5.3 %collective-permute-start.16 = (bf16[80,512]{1,0:T(8,128)(2,1)S(1)}, bf16[80,512]{1,0:T(8,128)(2,1)S(1)}, u32[]{:S(2)}, u32[]{:S(2)}) collective-permute-start(bf16[80,512]{1,0:T(8,128)(2,1)S(1)} %get-tuple-element.58), channel_id=1, source_target_pairs={{0,12},{4,8},{8,4},{12,0},{16,28},{20,24},{24,20},{28,16},{1,13},{... | collective-permute-start | bytes 245768 | tf_op jit(solution)/shard_map/ppermute | solution.py:53
where the time goes:
time: 91.6 us; the launch traced here: 91.4 us
  starting transfers between devices  48 us (52%)
  waiting for transfers between devices  24.4 us (27%)
  Pallas kernels  18.1 us (20%)
    ppermute x39, starting transfers between devices, swap(): return lax.ppermute(array, axis, [(i, i ^ bit) for i in range(size)])  44.1 us
    ppermute x39, waiting for transfers between devices, swap(): return lax.ppermute(array, axis, [(i, i ^ bit) for i in range(size)])  24.4 us
    pallas_call x15, Pallas kernels, call(): pl.pallas_call(body, out_shape=tuple((jax.ShapeDtypeStruct(s, d) for s, d...  18.1 us
    ppermute x1, starting transfers between devices, body(): lax.ppermute(total, 'ep', [(i, i ^ bit) for i in range(experts) if not i...  3.87 us
  transfers between devices with their start and end apart: 40, of which 10 were waited for; matrix products, arithmetic and copies ran while one was open for 0% of the time, Pallas kernels for 16%

commit v1 on v0

--- a/solution.py
+++ b/solution.py
@@ -16,7 +16,7 @@
 
 VMEM = pl.BlockSpec(memory_space=pltpu.VMEM)
 GRANT = 16 << 20
-WEIGH = 4e9
+LONG = 2e10
 NN = (((1,), (0,)), ((), ()))
 NT = (((1,), (1,)), ((), ()))
 TN = (((0,), (0,)), ((), ()))
@@ -43,9 +43,7 @@
         out_specs=tuple(VMEM for _ in outs),
         scratch_shapes=list(scratch),
         compiler_params=pltpu.CompilerParams(vmem_limit_bytes=GRANT),
-        cost_estimate=pl.CostEstimate(
-            flops=int(max(flops, WEIGH)), transcendentals=0, bytes_accessed=1 << 20
-        ),
+        cost_estimate=pl.CostEstimate(flops=int(flops), transcendentals=0, bytes_accessed=1 << 20),
     )(*args)
 
 
@@ -57,7 +55,8 @@
     return [pltpu.with_memory_space_constraint(a, pltpu.HBM) for a in arrays]
 
 
-def local_body(q_ref, x_ref, v_ref, shift_ref, floor_ref, sd_ref, qd_ref, within_ref):
+def local_body(q_ref, x_ref, v_ref, shift_ref, floor_ref, *refs):
+    sd_ref, qd_ref, within_ref = refs[-3:]
     length, width = q_ref.shape
     heads = shift_ref.shape[0]
     size = width // heads
@@ -75,6 +74,7 @@
         shift = jnp.broadcast_to(shift, (8, length))
     down = split_mm(lower, shift, NT, False)
     across = split_mm(shift, upper, NN, True)
+    states, decays = [], []
     for h in range(heads):
         cut = slice(h * size, (h + 1) * size)
         q = q_ref[:, cut].astype(F32)
@@ -91,41 +91,67 @@
         within_ref[:, cut] = mm(scores.astype(BF16), v)
         qd_ref[:, cut] = (q * jnp.exp(run + fall)).astype(BF16)
         kept = (k * jnp.exp((last - run) + (final - fall))).astype(BF16)
-        sd_ref[0:size, cut] = mm(v, kept, TN).astype(BF16)
-        sd_ref[size : size + ROWS, cut] = jnp.broadcast_to(
-            jnp.exp(last + final), (ROWS, size)
-        ).astype(BF16)
+        states.append(mm(v, kept, TN))
+        decays.append(jnp.exp(last + final))
+    value = (jnp.concatenate(states, axis=1), jnp.concatenate(decays, axis=1))
+    if len(refs) == 3:
+        put(sd_ref, value)
+    else:
+        put_wide(sd_ref, value, refs[0])
 
 
 def after(early, late):
     return (late[1] * early[0] + late[0], late[1] * early[1])
 
 
-def pair(ref):
+def pair(ref, first=0):
     rows = ref.shape[0] - ROWS
-    return (ref[0:rows, :].astype(F32), ref[rows : rows + 1, :].astype(F32))
-
-
-def put(ref, value):
+    return (ref[first:rows, :].astype(F32), ref[rows : rows + 1, :].astype(F32))
+
+
+def put(ref, value, first=0):
     rows = ref.shape[0] - ROWS
-    ref[0:rows, :] = value[0].astype(BF16)
+    ref[first:rows, :] = value[0].astype(BF16)
     ref[rows : rows + ROWS, :] = jnp.broadcast_to(value[1], (ROWS, ref.shape[1])).astype(BF16)
+
+
+def pair_wide(ref, first):
+    rows = ref.shape[0] - ROWS
+    width = ref.shape[1] // 2
+    state = jnp.concatenate([ref[first:rows, 0:width], ref[first:rows, width : 2 * width]], axis=0)
+    return (state.astype(F32), ref[rows : rows + 1, 0:width].astype(F32))
+
+
+def put_wide(ref, value, rows_ref):
+    first = rows_ref.shape[0]
+    ref[0:first, :] = rows_ref[...]
+    rows = ref.shape[0] - ROWS
+    half = rows - first
+    width = ref.shape[1] // 2
+    state = value[0].astype(BF16)
+    decay = jnp.broadcast_to(value[1], (ROWS, width)).astype(BF16)
+    for j in range(2):
+        cut = slice(j * width, (j + 1) * width)
+        ref[first:rows, cut] = state[j * half : (j + 1) * half, :]
+        ref[rows : rows + ROWS, cut] = decay
 
 
 def choose(flag, a, b):
     return tuple(jnp.where(flag, x, y) for x, y in zip(a, b))
 
 
-def scan_body(bit, first, tot_ref, *refs):
-    if first:
-        rec_ref, new_tot_ref, new_pre_ref = refs
+def scan_body(bit, first, cap, *refs):
+    new_tot_ref, new_pre_ref = refs[-2:]
+    tot_ref, rec_ref = refs[:2]
+    late = (lax.axis_index("ep") & bit) != 0
+    tot = pair_wide(tot_ref, cap)
+    rec = pair_wide(rec_ref, cap)
+    pre = (jnp.zeros_like(tot[0]), jnp.ones_like(tot[1])) if first else pair(refs[2])
+    new = choose(late, after(rec, tot), after(tot, rec))
+    if new_tot_ref.shape[0] == new_pre_ref.shape[0]:
+        put(new_tot_ref, new)
     else:
-        pre_ref, rec_ref, new_tot_ref, new_pre_ref = refs
-    late = (lax.axis_index("ep") & bit) != 0
-    tot = pair(tot_ref)
-    rec = pair(rec_ref)
-    pre = (jnp.zeros_like(tot[0]), jnp.ones_like(tot[1])) if first else pair(pre_ref)
-    put(new_tot_ref, choose(late, after(rec, tot), after(tot, rec)))
+        put_wide(new_tot_ref, new, refs[-3])
     put(new_pre_ref, choose(late, after(rec, pre), pre))
 
 
@@ -134,7 +160,8 @@
     size = gain_ref.shape[1]
     late = (lax.axis_index("ep") & bit) != 0
     pre = pair(pre_ref)
-    state = choose(late, after(pair(rec_ref), pre), pre)[0].astype(BF16)
+    rec = pair(rec_ref, rec_ref.shape[0] - pre_ref.shape[0])
+    state = choose(late, after(rec, pre), pre)[0].astype(BF16)
     for h in range(width // size):
         cut = slice(h * size, (h + 1) * size)
         got = within_ref[:, cut] + mm(qd_ref[:, cut], state[:, cut], NT)
@@ -227,11 +254,11 @@
     mine_ref, other_ref, x_ref, acc_ref = refs[-4:]
     at = lax.axis_index("tp")
     width = mine_ref.shape[1] // 2
-    for (block, piece), ref in zip(plan, refs[:-4]):
-        rows = slice(block * cap, (block + 1) * cap)
+    for (block, count, piece), ref in zip(plan, refs[:-4]):
+        rows = slice(block * cap, (block + count) * cap)
         for j, quarter in enumerate(piece(at)):
             lane = pl.multiple_of(quarter * width, width)
-            x_ref[rows, pl.ds(lane, width)] = ref[:, j * width : (j + 1) * width]
+            x_ref[rows, pl.ds(lane, width)] = ref[0 : count * cap, j * width : (j + 1) * width]
     x = x_ref[...]
     hidden = wg_ref.shape[2]
     chunk = min(hidden, 512)
@@ -263,35 +290,36 @@
     )
 
 
-def halve_body(parts, mine_ref, got_ref, keep_ref, *sends):
+def halve_body(mine_ref, got_ref, keep_ref, send_ref):
     width = keep_ref.shape[1]
     side = lax.axis_index("tp") // 2
-    rows = keep_ref.shape[0] // parts
-
-    def added(j):
-        lane = pl.multiple_of(j * width, width)
-        cut = pl.ds(lane, width)
-        return (mine_ref[:, cut].astype(F32) + got_ref[:, cut].astype(F32)).astype(BF16)
-
-    keep_ref[...] = added(side)
-    send = added(1 - side)
-    for i, ref in enumerate(sends):
-        ref[...] = send[i * rows : (i + 1) * rows, :]
-
-
-def add_body(first, keep_ref, got_ref, *outs):
-    rows = outs[0].shape[0]
+    for ref, j in ((keep_ref, side), (send_ref, 1 - side)):
+        cut = pl.ds(pl.multiple_of(j * width, width), width)
+        ref[...] = (mine_ref[:, cut].astype(F32) + got_ref[:, cut].astype(F32)).astype(BF16)
+
+
+def pack_body(*refs):
+    out_ref = refs[-1]
+    rows = out_ref.shape[0] // (len(refs) - 1)
+    for i, ref in enumerate(refs[:-1]):
+        out_ref[i * rows : (i + 1) * rows, :] = ref[0:rows, :]
+
+
+def add_body(keep_ref, got_ref, *refs):
+    outs = refs[-2:]
+    rows = keep_ref.shape[0] // 2
+    if len(refs) == 3:
+        outs[0][rows:, :] = refs[0][...]
     for i, ref in enumerate(outs):
-        cut = slice((first + i) * rows, (first + i + 1) * rows)
-        here = slice(i * rows, (i + 1) * rows)
-        ref[...] = (keep_ref[cut, :].astype(F32) + got_ref[here, :].astype(F32)).astype(BF16)
+        cut = slice(i * rows, (i + 1) * rows)
+        ref[0:rows, :] = (keep_ref[cut, :].astype(F32) + got_ref[cut, :].astype(F32)).astype(BF16)
 
 
 def combine_body(column_ref, first_ref, second_ref, *refs):
     out_ref, all_ref = refs[-2:]
-    cap = refs[0].shape[0]
+    cap = all_ref.shape[0] // (len(refs) - 2)
     for i, ref in enumerate(refs[:-2]):
-        all_ref[i * cap : (i + 1) * cap, :] = ref[...]
+        all_ref[i * cap : (i + 1) * cap, :] = ref[0:cap, :]
     weight = column_ref[:, TOP_K : 2 * TOP_K]
     back = all_ref[...]
     out_ref[...] = (
@@ -380,7 +408,7 @@
             functools.partial(spread_body, near, far),
             [block(slice_width)] * len(far) + [block(depth // 2)] * len(near) + [block(depth)],
             in_hbm(routes.T, moe_input, moe_gain.reshape(1, -1)),
-            2 * experts * cap * count * depth,
+            LONG,
             scratch=[
                 pltpu.VMEM((groups, count, slice_width), BF16),
                 pltpu.VMEM((padded, count), F32),
@@ -389,32 +417,92 @@
         )
         own_rows = sent[-1]
         far_in = {k: swap(a, "ep", experts, k) for k, a in zip(far, sent)}
-        near_in = {k: swap(a, "ep", experts, k) for k, a in zip(near, sent[len(far) :])}
+        near_out = dict(zip(near, sent[len(far) :]))
+        near_in = {}
 
     state_shape = ((size + ROWS, width), BF16)
-    sd, qd, within = call(
+    wide_shape = ((cap + size // 2 + ROWS, 2 * width), BF16)
+    total, qd, within = call(
         local_body,
-        [state_shape, ((length, width), BF16), ((length, width), F32)],
-        in_hbm(mix_query, forget_input, mix_value, decay_shift.T, floor),
-        8 * length * length * width,
+        [
+            wide_shape if direct else state_shape,
+            ((length, width), BF16),
+            ((length, width), F32),
+        ],
+        [mix_query, forget_input, mix_value, decay_shift.T, floor]
+        + ([near_out[1]] if direct else []),
+        LONG,
     )
     if direct:
-        total, before = sd, None
+        before = []
         bit = 1
         while bit < half:
-            got = swap(total, "ep", experts, bit)
-            args = [total] + ([] if before is None else [before]) + [got]
-            total, before = call(
-                functools.partial(scan_body, bit, before is None),
-                [state_shape, state_shape],
-                args,
+            near_in[bit] = swap(total, "ep", experts, bit)
+            last = 2 * bit == half
+            total, *before = call(
+                functools.partial(scan_body, bit, not before, cap),
+                [state_shape if last else wide_shape, state_shape],
+                [total, near_in[bit]] + before + ([] if last else [near_out[2 * bit]]),
                 8 * size * width,
             )
             bit *= 2
-        got = lax.ppermute(total, "ep", [(i, i ^ bit) for i in range(experts) if not i & bit])
+        for k in near:
+            if k not in near_in:
+                near_in[k] = swap(near_out[k], "ep", experts, k)
+
+    def gathered(keys):
+        if 0 in keys:
+            here = near_in[1]
+            pieces = [own_rows, here, swap(here, "tp", groups, 1)]
+            return pieces, [(0, 1, everything), (1, 1, own_half), (1, 1, other_half)]
+        wide = keys[0] in near
+        source = near_in if wide else far_in
+        here = call(
+            pack_body,
+            [((2 * cap, depth // 2 if wide else slice_width), BF16)],
+            [source[k] for k in keys],
+            0,
+        )[0]
+        pieces = [here, swap(here, "tp", groups, 1)]
+        if wide:
+            return pieces, [(0, 2, own_half), (0, 2, other_half)]
+        there = swap(here, "tp", groups, 2)
+        pieces += [there, swap(there, "tp", groups, 1)]
+        return pieces, [(0, 2, only(mask)) for mask in (0, 1, 2, 3)]
+
+    own_half = lambda at: (at & 1, 2 + (at & 1))
+    other_half = lambda at: (1 - (at & 1), 3 - (at & 1))
+    only = lambda mask: (lambda at: (at ^ mask,))
+    everything = lambda at: tuple(range(groups))
+
+    if direct:
+        weights = (w_exp_gate, w_exp_up, w_exp_down)
+        returned = {}
+        for i in range(experts // 2):
+            keys = (2 * i, 2 * i + 1)
+            rows = 2 * cap
+            pieces, plan = gathered(keys)
+            mine, other = expert_call(*weights, pieces, plan, 2, cap)
+            got = swap(other, "tp", groups, 1)
+            quarter = ((rows, slice_width), BF16)
+            keep, send = call(halve_body, [quarter, quarter], [mine, got], 0)
+            back = swap(send, "tp", groups, 2)
+            with_state = half in keys
+            done = call(
+                add_body,
+                [((cap + size + ROWS, width), BF16) if with_state else block(slice_width)]
+                + [block(slice_width)],
+                [keep, back] + ([total] if with_state else []),
+                0,
+            )
+            for k, a in zip(keys, done):
+                returned[k] = swap(a, "ep", experts, k) if k else a
+        got = returned[half]
+        before = before[0]
+        bit = half
     else:
         bit = 0
-        before = carried_in(sd, me)
+        before = carried_in(total, me)
         got = before
     head_out = call(
         functools.partial(finish_body, bit),
@@ -443,51 +531,6 @@
         )
         return (mixed, moe_out)
 
-    own_half = lambda at: (at & 1, 2 + (at & 1))
-    other_half = lambda at: (1 - (at & 1), 3 - (at & 1))
-    only = lambda mask: (lambda at: (at ^ mask,))
-    everything = lambda at: tuple(range(groups))
-
-    near_pieces = [own_rows]
-    near_plan = [(0, everything)]
-    for i, k in enumerate(near):
-        near_pieces += [near_in[k], swap(near_in[k], "tp", groups, 1)]
-        near_plan += [(i + 1, own_half), (i + 1, other_half)]
-    far_pieces = []
-    far_plan = []
-    for i, k in enumerate(far):
-        here = far_in[k]
-        there = swap(here, "tp", groups, 2)
-        far_pieces += [here, there]
-        far_pieces += [swap(here, "tp", groups, 1), swap(there, "tp", groups, 1)]
-        far_plan += [(i, only(0)), (i, only(2)), (i, only(1)), (i, only(3))]
-
-    weights = (w_exp_gate, w_exp_up, w_exp_down)
-    returned = {}
-    for keys, pieces, plan, parts in (
-        ((0,) + near, near_pieces, near_plan, 1), (far, far_pieces, far_plan, 2)
-    ):
-        rows = len(keys) * cap
-        mine, other = expert_call(*weights, pieces, plan, len(keys), cap)
-        got = swap(other, "tp", groups, 1)
-        keep, *sends = call(
-            functools.partial(halve_body, parts),
-            [((rows, slice_width), BF16)] + [((rows // parts, slice_width), BF16)] * parts,
-            [mine, got],
-            rows * slice_width * 4,
-        )
-        per = len(keys) // parts
-        for i, send in enumerate(sends):
-            back = swap(send, "tp", groups, 2)
-            done = call(
-                functools.partial(add_body, i * per),
-                [block(slice_width)] * per,
-                [keep, back],
-                rows * slice_width,
-            )
-            for k, a in zip(keys[i * per : (i + 1) * per], done):
-                returned[k] = swap(a, "ep", experts, k) if k else a
-
     order = (0,) + near + far
     first, second, column = call(
         functools.partial(places_body, order, padded),

time: 91.6 us -> 98.9 us (1.080)
  waiting for transfers between devices: 24.4 us -> 54 us
  starting transfers between devices: 48 us -> 25.7 us
    ppermute x39 -> x33, waiting for transfers between devices: 24.4 us -> 54 us  [swap(): return lax.ppermute(array, axis, [(i, i ^ bit) for i in range(size)])]
    ppermute x39 -> x33, starting transfers between devices: 44.1 us -> 25.7 us  [swap(): return lax.ppermute(array, axis, [(i, i ^ bit) for i in range(size)])]
    ppermute x1 -> x0, starting transfers between devices: 3.87 us -> none  [body(): lax.ppermute(total, 'ep', [(i, i ^ bit) for i in range(experts) if not i...]
    pallas_call x15 -> x23, Pallas kernels: 18.1 us -> 17.9 us  [call(): pl.pallas_call(body, out_shape=tuple((jax.ShapeDtypeStruct(s, d) for s, d...]
  transfers between devices with their start and end apart: 40 -> 33, of which waited for: 10 -> 17; matrix products, arithmetic and copies ran while one was open for 0% -> 0% of each run, Pallas kernels for 16% -> 14%
where the time goes in v1:
time: 98.9 us; the launch traced here: 98.7 us
  waiting for transfers between devices  54 us (55%)
  starting transfers between devices  25.7 us (26%)
  Pallas kernels  17.9 us (18%)
    ppermute x33, waiting for transfers between devices, swap(): return lax.ppermute(array, axis, [(i, i ^ bit) for i in range(size)])  54 us
    ppermute x33, starting transfers between devices, swap(): return lax.ppermute(array, axis, [(i, i ^ bit) for i in range(size)])  25.7 us
    pallas_call x23, Pallas kernels, call(): pl.pallas_call(body, out_shape=tuple((jax.ShapeDtypeStruct(s, d) for s, d...  17.9 us
  transfers between devices with their start and end apart: 33, of which 17 were waited for; matrix products, arithmetic and copies ran while one was open for 0% of the time, Pallas kernels for 14%

profile of v1, /device:TPU:0, one launch (start us, length us, event | category | flops | bytes accessed | tf_op | source)
XLA Modules:
  0.0 98.7 jit_solution(12120487783189289130)
XLA Ops:
  0.7 2.5 %shard_map.158 = (bf16[80,512]{1,0:T(8,128)(2,1)S(1)}, bf16[80,512]{1,0:T(8,128)(2,1)S(1)}, bf16[80,512]{1,0:T(8,128)(2,1)S(1)}, bf16[80,512]{1,0:T(8,128)(2,1)S...) custom-call(s32[2,256]{1,0:T(2,128)} %bitcast.11, ...), custom_call_target="tpu_custom_call" | custom-call | flops 20000000000 | bytes 1048576 | tf_op jit(solution)/shard_map/pallas_call | solution.py:39
  3.1 4.1 %collective-permute-start.2 = (bf16[80,512]{1,0:T(8,128)(2,1)S(1)}, bf16[80,512]{1,0:T(8,128)(2,1)S(1)}, u32[]{:S(2)}, u32[]{:S(2)}) collective-permute-start(bf16[80,512]{1,0:T(8,128)(2,1)S(1)} %get-tuple-element.52), channel_id=1, source_target_pairs={{0,16},{4,20},{8,24},{12,28},{16,0},{20,4},{24,8},{28,12},{1,17},{... | collective-permute-start | bytes 245768 | tf_op jit(solution)/shard_map/ppermute | solution.py:51
  7.3 1.3 %collective-permute-start.3 = (bf16[80,512]{1,0:T(8,128)(2,1)S(1)}, bf16[80,512]{1,0:T(8,128)(2,1)S(1)}, u32[]{:S(2)}, u32[]{:S(2)}) collective-permute-start(bf16[80,512]{1,0:T(8,128)(2,1)S(1)} %get-tuple-element.53), channel_id=1, source_target_pairs={{0,20},{4,16},{8,28},{12,24},{16,4},{20,0},{24,12},{28,8},{1,21},{... | collective-permute-start | bytes 245768 | tf_op jit(solution)/shard_map/ppermute | solution.py:51
  8.6 0.0 copy-start
  8.6 0.0 copy-start.1
  8.6 0.0 copy-start.2
  8.6 1.4 %shard_map.159 = (bf16[160,1024]{1,0:T(8,128)(2,1)S(1)}, bf16[256,512]{1,0:T(8,128)(2,1)S(1)}, f32[256,512]{1,0:T(8,128)S(1)}) custom-call(bf16[256,512]{1,0:T(8,128)(2,1)S(1)} %copy-done.6, bf16[256,512]{1,0:T(8,128)(2,1)S(1)} %copy-done.7, bf16[256,512]{1,0:T(8,128)(2,1)S(1)} %copy-done.8, f32[4,256]{1,0:T(4,128)S(1)} %bitcast.9, f32[1,512]{1,0:T(1,128)S(1)} %bitcast.10, ...), custom_call_target="tpu_custom_call" | custom-call | flops 20000000000 | bytes 1048576 | tf_op jit(solution)/shard_map/pallas_call | solution.py:39
  10.0 0.3 collective-permute-start
  10.4 1.3 %collective-permute-done.2.refs_0_ = bf16[80,512]{1,0:T(8,128)(2,1)S(1)} collective-permute-done((bf16[80,512]{1,0:T(8,128)(2,1)S(1)}, bf16[80,512]{1,0:T(8,128)(2,1)S(1)}, u32[]{:S(2)}, u32[]{:S(2)}) %collective-permute-start.2) | collective-permute-done | bytes 81952 | tf_op jit(solution)/shard_map/ppermute | solution.py:51
  11.7 4.5 %collective-permute-done.3.refs_1_ = bf16[80,512]{1,0:T(8,128)(2,1)S(1)} collective-permute-done((bf16[80,512]{1,0:T(8,128)(2,1)S(1)}, bf16[80,512]{1,0:T(8,128)(2,1)S(1)}, u32[]{:S(2)}, u32[]{:S(2)}) %collective-permute-start.3) | collective-permute-done | bytes 81952 | tf_op jit(solution)/shard_map/ppermute | solution.py:51
  16.2 1.6 %collective-permute-start.5 = (bf16[160,512]{1,0:T(8,128)(2,1)S(1)}, bf16[160,512]{1,0:T(8,128)(2,1)S(1)}, u32[]{:S(2)}, u32[]{:S(2)}) collective-permute-start(bf16[160,512]{1,0:T(8,128)(2,1)S(1)} %shard_map.162.refs_0_), channel_id=1, source_target_pairs={{0,2},{1,3},{2,0},{3,1},{4,6},{5,7},{6,4},{7,5},{8,10},{9,11},{10,... | collective-permute-start | bytes 491528 | tf_op jit(solution)/shard_map/ppermute | solution.py:51
  17.8 3.4 %collective-permute-start.24 = (bf16[80,512]{1,0:T(8,128)(2,1)S(1)}, bf16[80,512]{1,0:T(8,128)(2,1)S(1)}, u32[]{:S(2)}, u32[]{:S(2)}) collective-permute-start(bf16[80,512]{1,0:T(8,128)(2,1)S(1)} %get-tuple-element.78), channel_id=1, source_target_pairs={{0,24},{4,28},{8,16},{12,20},{16,8},{20,12},{24,0},{28,4},{1,25},{... | collective-permute-start | bytes 245768 | tf_op jit(solution)/shard_map/ppermute | solution.py:51
  21.2 0.4 collective-permute-start.25
  21.7 2.5 %collective-permute-done.24.refs_0_ = bf16[80,512]{1,0:T(8,128)(2,1)S(1)} collective-permute-done((bf16[80,512]{1,0:T(8,128)(2,1)S(1)}, bf16[80,512]{1,0:T(8,128)(2,1)S(1)}, u32[]{:S(2)}, u32[]{:S(2)}) %collective-permute-start.24) | collective-permute-done | bytes 81952 | tf_op jit(solution)/shard_map/ppermute | solution.py:51
  24.2 4.2 %collective-permute-done.25.refs_1_ = bf16[80,512]{1,0:T(8,128)(2,1)S(1)} collective-permute-done((bf16[80,512]{1,0:T(8,128)(2,1)S(1)}, bf16[80,512]{1,0:T(8,128)(2,1)S(1)}, u32[]{:S(2)}, u32[]{:S(2)}) %collective-permute-start.25) | collective-permute-done | bytes 81952 | tf_op jit(solution)/shard_map/ppermute | solution.py:51
  28.4 0.5 collective-permute-start.27
  28.9 0.5 collective-permute-start.26
  29.4 0.1 shard_map.160
  29.5 1.8 %collective-permute-start.1 = (bf16[160,1024]{1,0:T(8,128)(2,1)S(1)}, bf16[160,1024]{1,0:T(8,128)(2,1)S(1)}, u32[]{:S(2)}, u32[]{:S(2)}) collective-permute-start(bf16[160,1024]{1,0:T(8,128)(2,1)S(1)} %get-tuple-element.49.refs_0_), channel_id=1, source_target_pairs={{0,8},{4,12},{8,0},{12,4},{16,24},{20,28},{24,16},{28,20},{1,9},{5... | collective-permute-start | bytes 983048 | tf_op jit(solution)/shard_map/ppermute | solution.py:51
  31.3 2.4 %collective-permute-done.27.refs_2_ = bf16[160,512]{1,0:T(8,128)(2,1)S(1)} collective-permute-done((bf16[160,512]{1,0:T(8,128)(2,1)S(1)}, bf16[160,512]{1,0:T(8,128)(2,1)S(1)}, u32[]{:S(2)}, u32[]{:S(2)}) %collective-permute-start.27) | collective-permute-done | bytes 163872 | tf_op jit(solution)/shard_map/ppermute | solution.py:51
  33.8 2.3 %shard_map.163 = (bf16[160,1024]{1,0:T(8,128)(2,1)S(1)}, bf16[160,1024]{1,0:T(8,128)(2,1)S(1)}) custom-call(bf16[1,2048,1024]{2,1,0:T(8,128)(2,1)S(1)} %copy-done, bf16[1,2048,1024]{2,1,0:T(8,128)(2,1)S(1)} %copy-done.1, bf16[1,1024,2048]{2,1,0:T(8,128)(2,1)S(1)} %copy-done.2, bf16[160,512]{1,0:T(8,128)(2,1)S(1)} %shard_map.162.refs_0_, ...), custom_call_target="tpu_custom_call" | custom-call | flops 2013265920 | bytes 1048576 | tf_op jit(solution)/shard_map/pallas_call | solution.py:39
  36.1 0.6 collective-permute-start.7
  36.7 0.2 collective-permute-done.17.refs_1_
  36.9 5.6 %collective-permute-done.1.refs_1_.refs_0_ = bf16[160,1024]{1,0:T(8,128)(2,1)S(1)} collective-permute-done((bf16[160,1024]{1,0:T(8,128)(2,1)S(1)}, bf16[160,1024]{1,0:T(8,128)(2,1)S(1)}, u32[]{:S(2)}, u32[]{:S(2)}) %collective-permute-start.1) | collective-permute-done | bytes 327712 | tf_op jit(solution)/shard_map/ppermute | solution.py:51
  42.5 0.1 collective-permute-start.18
  42.6 2.4 %shard_map.177 = (bf16[160,1024]{1,0:T(8,128)(2,1)S(1)}, bf16[160,1024]{1,0:T(8,128)(2,1)S(1)}) custom-call(bf16[1,2048,1024]{2,1,0:T(8,128)(2,1)S(1)} %copy-done, bf16[1,2048,1024]{2,1,0:T(8,128)(2,1)S(1)} %copy-done.1, bf16[1,1024,2048]{2,1,0:T(8,128)(2,1)S(1)} %copy-done.2, bf16[160,512]{1,0:T(8,128)(2,1)S(1)} %shard_map.176.refs_0_, ...), custom_call_target="tpu_custom_call" | custom-call | flops 2013265920 | bytes 1048576 | tf_op jit(solution)/shard_map/pallas_call | solution.py:39
  45.0 0.5 collective-permute-start.29
  45.5 0.1 shard_map.164
  45.6 1.6 %collective-permute-start.8 = (bf16[160,512]{1,0:T(8,128)(2,1)S(1)}, bf16[160,512]{1,0:T(8,128)(2,1)S(1)}, u32[]{:S(2)}, u32[]{:S(2)}) collective-permute-start(bf16[160,512]{1,0:T(8,128)(2,1)S(1)} %get-tuple-element.57), channel_id=1, source_target_pairs={{0,2},{1,3},{2,0},{3,1},{4,6},{5,7},{6,4},{7,5},{8,10},{9,11},{10,... | collective-permute-start | bytes 491528 | tf_op jit(solution)/shard_map/ppermute | solution.py:51
  47.2 2.4 %shard_map.169 = (bf16[160,1024]{1,0:T(8,128)(2,1)S(1)}, bf16[160,1024]{1,0:T(8,128)(2,1)S(1)}) custom-call(bf16[1,2048,1024]{2,1,0:T(8,128)(2,1)S(1)} %copy-done, bf16[1,2048,1024]{2,1,0:T(8,128)(2,1)S(1)} %copy-done.1, bf16[1,1024,2048]{2,1,0:T(8,128)(2,1)S(1)} %copy-done.2, bf16[80,2048]{1,0:T(8,128)(2,1)S(1)} %get-tuple-element.63.refs_0_, ...), custom_call_target="tpu_custom_call" | custom-call | flops 2013265920 | bytes 1048576 | tf_op jit(solution)/shard_map/pallas_call | solution.py:39
  49.6 0.1 collective-permute-start.14
  49.7 0.1 shard_map.161
  49.8 2.0 %collective-permute-done.8.got_ref = bf16[160,512]{1,0:T(8,128)(2,1)S(1)} collective-permute-done((bf16[160,512]{1,0:T(8,128)(2,1)S(1)}, bf16[160,512]{1,0:T(8,128)(2,1)S(1)}, u32[]{:S(2)}, u32[]{:S(2)}) %collective-permute-start.8) | collective-permute-done | bytes 163872 | tf_op jit(solution)/shard_map/ppermute | solution.py:51
  51.9 0.0 copy-start.4
  51.9 0.0 copy-start.5
  51.9 0.1 collective-permute-start.9
  52.0 2.6 %shard_map.173 = (bf16[160,1024]{1,0:T(8,128)(2,1)S(1)}, bf16[160,1024]{1,0:T(8,128)(2,1)S(1)}) custom-call(bf16[1,2048,1024]{2,1,0:T(8,128)(2,1)S(1)} %copy-done, bf16[1,2048,1024]{2,1,0:T(8,128)(2,1)S(1)} %copy-done.1, bf16[1,1024,2048]{2,1,0:T(8,128)(2,1)S(1)} %copy-done.2, bf16[160,1024]{1,0:T(8,128)(2,1)S(1)} %shard_map.172.refs_0_, ...), custom_call_target="tpu_custom_call" | custom-call | flops 2013265920 | bytes 1048576 | tf_op jit(solution)/shard_map/pallas_call | solution.py:39
  54.6 0.0 copy-start.11
  54.6 0.0 copy-start.12
  54.6 0.0 copy-start.3
  54.6 0.1 collective-permute-start.19
  54.7 9.5 %collective-permute-done.9.rec_ref.refs_4_ = bf16[224,512]{1,0:T(8,128)(2,1)S(1)} collective-permute-done((bf16[224,512]{1,0:T(8,128)(2,1)S(1)}, bf16[224,512]{1,0:T(8,128)(2,1)S(1)}, u32[]{:S(2)}, u32[]{:S(2)}) %collective-permute-start.9) | collective-permute-done | bytes 229408 | tf_op jit(solution)/shard_map/ppermute | solution.py:51
  64.2 0.4 shard_map.166.refs_0_
  64.7 1.6 %collective-permute-start.10 = (bf16[256,512]{1,0:T(8,128)(2,1)S(1)}, bf16[256,512]{1,0:T(8,128)(2,1)S(1)}, u32[]{:S(2)}, u32[]{:S(2)}) collective-permute-start(bf16[256,512]{1,0:T(8,128)(2,1)S(1)} %shard_map.166.refs_0_), channel_id=1, source_target_pairs={{0,2},{1,3},{2,0},{3,1},{4,6},{5,7},{6,4},{7,5},{8,10},{9,11},{10,... | collective-permute-start | bytes 786440 | tf_op jit(solution)/shard_map/ppermute | solution.py:51
  66.3 0.1 shard_map.178
  66.4 0.5 collective-permute-start.30
  66.9 0.1 shard_map.170
  67.0 1.6 %collective-permute-start.15 = (bf16[160,512]{1,0:T(8,128)(2,1)S(1)}, bf16[160,512]{1,0:T(8,128)(2,1)S(1)}, u32[]{:S(2)}, u32[]{:S(2)}) collective-permute-start(bf16[160,512]{1,0:T(8,128)(2,1)S(1)} %get-tuple-element.67), channel_id=1, source_target_pairs={{0,2},{1,3},{2,0},{3,1},{4,6},{5,7},{6,4},{7,5},{8,10},{9,11},{10,... | collective-permute-start | bytes 491528 | tf_op jit(solution)/shard_map/ppermute | solution.py:51
  68.6 0.1 shard_map.174
  68.7 0.5 collective-permute-start.20
  69.2 4.7 %collective-permute-done.10.refs_1_ = bf16[256,512]{1,0:T(8,128)(2,1)S(1)} collective-permute-done((bf16[256,512]{1,0:T(8,128)(2,1)S(1)}, bf16[256,512]{1,0:T(8,128)(2,1)S(1)}, u32[]{:S(2)}, u32[]{:S(2)}) %collective-permute-start.10) | collective-permute-done | bytes 262176 | tf_op jit(solution)/shard_map/ppermute | solution.py:51
  73.9 3.5 %collective-permute-done.30.got_ref = bf16[160,512]{1,0:T(8,128)(2,1)S(1)} collective-permute-done((bf16[160,512]{1,0:T(8,128)(2,1)S(1)}, bf16[160,512]{1,0:T(8,128)(2,1)S(1)}, u32[]{:S(2)}, u32[]{:S(2)}) %collective-permute-start.30) | collective-permute-done | bytes 163872 | tf_op jit(solution)/shard_map/ppermute | solution.py:51
  77.5 3.5 %collective-permute-done.15.got_ref = bf16[160,512]{1,0:T(8,128)(2,1)S(1)} collective-permute-done((bf16[160,512]{1,0:T(8,128)(2,1)S(1)}, bf16[160,512]{1,0:T(8,128)(2,1)S(1)}, u32[]{:S(2)}, u32[]{:S(2)}) %collective-permute-start.15) | collective-permute-done | bytes 163872 | tf_op jit(solution)/shard_map/ppermute | solution.py:51
  80.9 1.4 %collective-permute-start.31 = (bf16[80,512]{1,0:T(8,128)(2,1)S(1)}, bf16[80,512]{1,0:T(8,128)(2,1)S(1)}, u32[]{:S(2)}, u32[]{:S(2)}) collective-permute-start(bf16[80,512]{1,0:T(8,128)(2,1)S(1)} %get-tuple-element.84), channel_id=1, source_target_pairs={{0,24},{4,28},{8,16},{12,20},{16,8},{20,12},{24,0},{28,4},{1,25},{... | collective-permute-start | bytes 245768 | tf_op jit(solution)/shard_map/ppermute | solution.py:51
  82.4 1.1 %collective-permute-done.20.got_ref = bf16[160,512]{1,0:T(8,128)(2,1)S(1)} collective-permute-done((bf16[160,512]{1,0:T(8,128)(2,1)S(1)}, bf16[160,512]{1,0:T(8,128)(2,1)S(1)}, u32[]{:S(2)}, u32[]{:S(2)}) %collective-permute-start.20) | collective-permute-done | bytes 163872 | tf_op jit(solution)/shard_map/ppermute | solution.py:51
  83.5 1.4 %collective-permute-start.32 = (bf16[80,512]{1,0:T(8,128)(2,1)S(1)}, bf16[80,512]{1,0:T(8,128)(2,1)S(1)}, u32[]{:S(2)}, u32[]{:S(2)}) collective-permute-start(bf16[80,512]{1,0:T(8,128)(2,1)S(1)} %get-tuple-element.85), channel_id=1, source_target_pairs={{0,28},{4,24},{8,20},{12,16},{16,12},{20,8},{24,4},{28,0},{1,29},{... | collective-permute-start | bytes 245768 | tf_op jit(solution)/shard_map/ppermute | solution.py:51
  85.0 1.5 %collective-permute-start.16 = (bf16[80,512]{1,0:T(8,128)(2,1)S(1)}, bf16[80,512]{1,0:T(8,128)(2,1)S(1)}, u32[]{:S(2)}, u32[]{:S(2)}) collective-permute-start(bf16[80,512]{1,0:T(8,128)(2,1)S(1)} %get-tuple-element.69), channel_id=1, source_target_pairs={{0,4},{4,0},{8,12},{12,8},{16,20},{20,16},{24,28},{28,24},{1,5},{5... | collective-permute-start | bytes 245768 | tf_op jit(solution)/shard_map/ppermute | solution.py:51
  86.6 0.7 collective-permute-done.31.refs_6_
  87.3 3.4 %collective-permute-done.32.refs_7_ = bf16[80,512]{1,0:T(8,128)(2,1)S(1)} collective-permute-done((bf16[80,512]{1,0:T(8,128)(2,1)S(1)}, bf16[80,512]{1,0:T(8,128)(2,1)S(1)}, u32[]{:S(2)}, u32[]{:S(2)}) %collective-permute-start.32) | collective-permute-done | bytes 81952 | tf_op jit(solution)/shard_map/ppermute | solution.py:51
  90.7 0.5 shard_map.168
  91.2 0.6 collective-permute-done.21.refs_2_
  91.9 4.2 %collective-permute-done.22.refs_3_ = bf16[80,512]{1,0:T(8,128)(2,1)S(1)} collective-permute-done((bf16[80,512]{1,0:T(8,128)(2,1)S(1)}, bf16[80,512]{1,0:T(8,128)(2,1)S(1)}, u32[]{:S(2)}, u32[]{:S(2)}) %collective-permute-start.22) | collective-permute-done | bytes 81952 | tf_op jit(solution)/shard_map/ppermute | solution.py:51
  96.0 1.3 %shard_map.180 = bf16[256,512]{1,0:T(8,128)(2,1)} custom-call(f32[256,8]{1,0:T(8,128)S(1)} %get-tuple-element.60.column_ref, bf16[256,640]{1,0:T(8,128)(2,1)S(1)} %get-tuple-element.61.first_ref, bf16[256,640]{1,0:T(8,128)(2,1)S(1)} %get-tuple-element.62.second_ref, bf16[80,512]{1,0:T(8,128)(2,1)S(1)} %get-tuple-element.68.refs_0_, ...), custom_call_target="tpu_custom_call" | custom-call | flops 335544320 | bytes 1048576 | tf_op jit(solution)/shard_map/pallas_call | solution.py:39
  97.3 1.4 %shard_map.167 = bf16[256,512]{1,0:T(8,128)(2,1)} custom-call(bf16[4,512,512]{2,1,0:T(8,128)(2,1)S(1)} %bitcast.7, bf16[256,512]{1,0:T(8,128)(2,1)S(1)} %shard_map.166.refs_0_, bf16[256,512]{1,0:T(8,128)(2,1)S(1)} %collective-permute-done.10.refs_1_, bf16[256,512]{1,0:T(8,128)(2,1)S(1)} %collective-permute-done.11.refs_2_, ...), custom_call_target="tpu_custom_call" | custom-call | flops 536870912 | bytes 1048576 | tf_op jit(solution)/shard_map/pallas_call | solution.py:39
  (51 shorter events, 0.3 us)
Async XLA Ops:
  0.6 7.9 %copy-start.6 = (bf16[256,512]{1,0:T(8,128)(2,1)S(1)}, bf16[256,512]{1,0:T(8,128)(2,1)}, u32[]{:S(2)}) copy-start(bf16[256,512]{1,0:T(8,128)(2,1)} %q_ref.1) | copy-start | bytes 786436
  0.6 7.9 %copy-start.7 = (bf16[256,512]{1,0:T(8,128)(2,1)S(1)}, bf16[256,512]{1,0:T(8,128)(2,1)}, u32[]{:S(2)}) copy-start(bf16[256,512]{1,0:T(8,128)(2,1)} %x_ref.3) | copy-start | bytes 786436
  0.7 7.9 %copy-start.8 = (bf16[256,512]{1,0:T(8,128)(2,1)S(1)}, bf16[256,512]{1,0:T(8,128)(2,1)}, u32[]{:S(2)}) copy-start(bf16[256,512]{1,0:T(8,128)(2,1)} %v_ref.1) | copy-start | bytes 786436
  0.7 7.9 %copy-start.9 = (f32[256,4]{0,1:T(4,128)S(1)}, f32[256,4]{0,1:T(4,128)}, u32[]{:S(2)}) copy-start(f32[256,4]{0,1:T(4,128)} %param.19) | copy-start | bytes 12292
  0.7 7.9 %copy-start.10 = (f32[512]{0:T(512)S(1)}, f32[512]{0:T(512)}, u32[]{:S(2)}) copy-start(f32[512]{0:T(512)} %param.20) | copy-start | bytes 6148
  3.1 8.6 %collective-permute-start.2 = (bf16[80,512]{1,0:T(8,128)(2,1)S(1)}, bf16[80,512]{1,0:T(8,128)(2,1)S(1)}, u32[]{:S(2)}, u32[]{:S(2)}) collective-permute-start(bf16[80,512]{1,0:T(8,128)(2,1)S(1)} %get-tuple-element.52), channel_id=1, source_target_pairs={{0,16},{4,20},{8,24},{12,28},{16,0},{20,4},{24,8},{28,12},{1,17},{... | collective-permute-start | bytes 245768 | tf_op jit(solution)/shard_map/ppermute | solution.py:51
  7.3 8.9 %collective-permute-start.3 = (bf16[80,512]{1,0:T(8,128)(2,1)S(1)}, bf16[80,512]{1,0:T(8,128)(2,1)S(1)}, u32[]{:S(2)}, u32[]{:S(2)}) collective-permute-start(bf16[80,512]{1,0:T(8,128)(2,1)S(1)} %get-tuple-element.53), channel_id=1, source_target_pairs={{0,20},{4,16},{8,28},{12,24},{16,4},{20,0},{24,12},{28,8},{1,21},{... | collective-permute-start | bytes 245768 | tf_op jit(solution)/shard_map/ppermute | solution.py:51
  8.6 25.2 %copy-start = (bf16[1,2048,1024]{2,1,0:T(8,128)(2,1)S(1)}, bf16[1,2048,1024]{2,1,0:T(8,128)(2,1)}, u32[]{:S(2)}) copy-start(bf16[1,2048,1024]{2,1,0:T(8,128)(2,1)} %wg_ref.7) | copy-start | bytes 12582916
  8.6 25.2 %copy-start.1 = (bf16[1,2048,1024]{2,1,0:T(8,128)(2,1)S(1)}, bf16[1,2048,1024]{2,1,0:T(8,128)(2,1)}, u32[]{:S(2)}) copy-start(bf16[1,2048,1024]{2,1,0:T(8,128)(2,1)} %wu_ref.7) | copy-start | bytes 12582916
  8.6 25.2 %copy-start.2 = (bf16[1,1024,2048]{2,1,0:T(8,128)(2,1)S(1)}, bf16[1,1024,2048]{2,1,0:T(8,128)(2,1)}, u32[]{:S(2)}) copy-start(bf16[1,1024,2048]{2,1,0:T(8,128)(2,1)} %wd_ref.7) | copy-start | bytes 12582916
  10.0 18.9 %collective-permute-start = (bf16[160,1024]{1,0:T(8,128)(2,1)S(1)}, bf16[160,1024]{1,0:T(8,128)(2,1)S(1)}, u32[]{:S(2)}, u32[]{:S(2)}) collective-permute-start(bf16[160,1024]{1,0:T(8,128)(2,1)S(1)} %get-tuple-element.47.refs_0_), channel_id=1, source_target_pairs={{0,4},{4,0},{8,12},{12,8},{16,20},{20,16},{24,28},{28,24},{1,5},{5... | collective-permute-start | bytes 983048 | tf_op jit(solution)/shard_map/ppermute | solution.py:51
  16.2 12.7 %collective-permute-start.5 = (bf16[160,512]{1,0:T(8,128)(2,1)S(1)}, bf16[160,512]{1,0:T(8,128)(2,1)S(1)}, u32[]{:S(2)}, u32[]{:S(2)}) collective-permute-start(bf16[160,512]{1,0:T(8,128)(2,1)S(1)} %shard_map.162.refs_0_), channel_id=1, source_target_pairs={{0,2},{1,3},{2,0},{3,1},{4,6},{5,7},{6,4},{7,5},{8,10},{9,11},{10,... | collective-permute-start | bytes 491528 | tf_op jit(solution)/shard_map/ppermute | solution.py:51
  17.8 6.3 %collective-permute-start.24 = (bf16[80,512]{1,0:T(8,128)(2,1)S(1)}, bf16[80,512]{1,0:T(8,128)(2,1)S(1)}, u32[]{:S(2)}, u32[]{:S(2)}) collective-permute-start(bf16[80,512]{1,0:T(8,128)(2,1)S(1)} %get-tuple-element.78), channel_id=1, source_target_pairs={{0,24},{4,28},{8,16},{12,20},{16,8},{20,12},{24,0},{28,4},{1,25},{... | collective-permute-start | bytes 245768 | tf_op jit(solution)/shard_map/ppermute | solution.py:51
  21.2 7.1 %collective-permute-start.25 = (bf16[80,512]{1,0:T(8,128)(2,1)S(1)}, bf16[80,512]{1,0:T(8,128)(2,1)S(1)}, u32[]{:S(2)}, u32[]{:S(2)}) collective-permute-start(bf16[80,512]{1,0:T(8,128)(2,1)S(1)} %get-tuple-element.79), channel_id=1, source_target_pairs={{0,28},{4,24},{8,20},{12,16},{16,12},{20,8},{24,4},{28,0},{1,29},{... | collective-permute-start | bytes 245768 | tf_op jit(solution)/shard_map/ppermute | solution.py:51
  21.6 7.9 %collective-permute-start.4 = (bf16[160,512]{1,0:T(8,128)(2,1)S(1)}, bf16[160,512]{1,0:T(8,128)(2,1)S(1)}, u32[]{:S(2)}, u32[]{:S(2)}) collective-permute-start(bf16[160,512]{1,0:T(8,128)(2,1)S(1)} %shard_map.162.refs_0_), channel_id=1, source_target_pairs={{0,1},{1,0},{2,3},{3,2},{4,5},{5,4},{6,7},{7,6},{8,9},{9,8},{10,11... | collective-permute-start | bytes 491528 | tf_op jit(solution)/shard_map/ppermute | solution.py:51
  28.4 5.4 %collective-permute-start.27 = (bf16[160,512]{1,0:T(8,128)(2,1)S(1)}, bf16[160,512]{1,0:T(8,128)(2,1)S(1)}, u32[]{:S(2)}, u32[]{:S(2)}) collective-permute-start(bf16[160,512]{1,0:T(8,128)(2,1)S(1)} %shard_map.176.refs_0_), channel_id=1, source_target_pairs={{0,2},{1,3},{2,0},{3,1},{4,6},{5,7},{6,4},{7,5},{8,10},{9,11},{10,... | collective-permute-start | bytes 491528 | tf_op jit(solution)/shard_map/ppermute | solution.py:51
  28.9 4.8 %collective-permute-start.6 = (bf16[160,512]{1,0:T(8,128)(2,1)S(1)}, bf16[160,512]{1,0:T(8,128)(2,1)S(1)}, u32[]{:S(2)}, u32[]{:S(2)}) collective-permute-start(bf16[160,512]{1,0:T(8,128)(2,1)S(1)} %collective-permute-done.5.refs_2_), channel_id=1, source_target_pairs={{0,1},{1,0},{2,3},{3,2},{4,5},{5,4},{6,7},{7,6},{8,9},{9,8},{10,11... | collective-permute-start | bytes 491528 | tf_op jit(solution)/shard_map/ppermute | solution.py:51
  28.9 8.0 %collective-permute-start.17 = (bf16[80,1024]{1,0:T(8,128)(2,1)S(1)}, bf16[80,1024]{1,0:T(8,128)(2,1)S(1)}, u32[]{:S(2)}, u32[]{:S(2)}) collective-permute-start(bf16[80,1024]{1,0:T(8,128)(2,1)S(1)} %get-tuple-element.70), channel_id=1, source_target_pairs={{0,12},{4,8},{8,4},{12,0},{16,28},{20,24},{24,20},{28,16},{1,13},{... | collective-permute-start | bytes 491528 | tf_op jit(solution)/shard_map/ppermute | solution.py:51
  28.9 13.7 %collective-permute-start.26 = (bf16[160,512]{1,0:T(8,128)(2,1)S(1)}, bf16[160,512]{1,0:T(8,128)(2,1)S(1)}, u32[]{:S(2)}, u32[]{:S(2)}) collective-permute-start(bf16[160,512]{1,0:T(8,128)(2,1)S(1)} %shard_map.176.refs_0_), channel_id=1, source_target_pairs={{0,1},{1,0},{2,3},{3,2},{4,5},{5,4},{6,7},{7,6},{8,9},{9,8},{10,11... | collective-permute-start | bytes 491528 | tf_op jit(solution)/shard_map/ppermute | solution.py:51
  29.5 13.0 %collective-permute-start.1 = (bf16[160,1024]{1,0:T(8,128)(2,1)S(1)}, bf16[160,1024]{1,0:T(8,128)(2,1)S(1)}, u32[]{:S(2)}, u32[]{:S(2)}) collective-permute-start(bf16[160,1024]{1,0:T(8,128)(2,1)S(1)} %get-tuple-element.49.refs_0_), channel_id=1, source_target_pairs={{0,8},{4,12},{8,0},{12,4},{16,24},{20,28},{24,16},{28,20},{1,9},{5... | collective-permute-start | bytes 983048 | tf_op jit(solution)/shard_map/ppermute | solution.py:51
  33.7 8.9 %collective-permute-start.28 = (bf16[160,512]{1,0:T(8,128)(2,1)S(1)}, bf16[160,512]{1,0:T(8,128)(2,1)S(1)}, u32[]{:S(2)}, u32[]{:S(2)}) collective-permute-start(bf16[160,512]{1,0:T(8,128)(2,1)S(1)} %collective-permute-done.27.refs_2_), channel_id=1, source_target_pairs={{0,1},{1,0},{2,3},{3,2},{4,5},{5,4},{6,7},{7,6},{8,9},{9,8},{10,11... | collective-permute-start | bytes 491528 | tf_op jit(solution)/shard_map/ppermute | solution.py:51
  36.1 9.4 %collective-permute-start.7 = (bf16[160,1024]{1,0:T(8,128)(2,1)S(1)}, bf16[160,1024]{1,0:T(8,128)(2,1)S(1)}, u32[]{:S(2)}, u32[]{:S(2)}) collective-permute-start(bf16[160,1024]{1,0:T(8,128)(2,1)S(1)} %get-tuple-element.55), channel_id=1, source_target_pairs={{0,1},{1,0},{2,3},{3,2},{4,5},{5,4},{6,7},{7,6},{8,9},{9,8},{10,11... | collective-permute-start | bytes 983048 | tf_op jit(solution)/shard_map/ppermute | solution.py:51
  36.9 10.4 %collective-permute-start.13 = (bf16[160,1024]{1,0:T(8,128)(2,1)S(1)}, bf16[160,1024]{1,0:T(8,128)(2,1)S(1)}, u32[]{:S(2)}, u32[]{:S(2)}) collective-permute-start(bf16[160,1024]{1,0:T(8,128)(2,1)S(1)} %collective-permute-done.refs_1_), channel_id=1, source_target_pairs={{0,1},{1,0},{2,3},{3,2},{4,5},{5,4},{6,7},{7,6},{8,9},{9,8},{10,11... | collective-permute-start | bytes 983048 | tf_op jit(solution)/shard_map/ppermute | solution.py:51
  42.5 9.5 %collective-permute-start.18 = (bf16[160,1024]{1,0:T(8,128)(2,1)S(1)}, bf16[160,1024]{1,0:T(8,128)(2,1)S(1)}, u32[]{:S(2)}, u32[]{:S(2)}) collective-permute-start(bf16[160,1024]{1,0:T(8,128)(2,1)S(1)} %shard_map.172.refs_0_), channel_id=1, source_target_pairs={{0,1},{1,0},{2,3},{3,2},{4,5},{5,4},{6,7},{7,6},{8,9},{9,8},{10,11... | collective-permute-start | bytes 983048 | tf_op jit(solution)/shard_map/ppermute | solution.py:51
  45.0 21.3 %collective-permute-start.29 = (bf16[160,1024]{1,0:T(8,128)(2,1)S(1)}, bf16[160,1024]{1,0:T(8,128)(2,1)S(1)}, u32[]{:S(2)}, u32[]{:S(2)}) collective-permute-start(bf16[160,1024]{1,0:T(8,128)(2,1)S(1)} %get-tuple-element.81), channel_id=1, source_target_pairs={{0,1},{1,0},{2,3},{3,2},{4,5},{5,4},{6,7},{7,6},{8,9},{9,8},{10,11... | collective-permute-start | bytes 983048 | tf_op jit(solution)/shard_map/ppermute | solution.py:51
  45.6 6.2 %collective-permute-start.8 = (bf16[160,512]{1,0:T(8,128)(2,1)S(1)}, bf16[160,512]{1,0:T(8,128)(2,1)S(1)}, u32[]{:S(2)}, u32[]{:S(2)}) collective-permute-start(bf16[160,512]{1,0:T(8,128)(2,1)S(1)} %get-tuple-element.57), channel_id=1, source_target_pairs={{0,2},{1,3},{2,0},{3,1},{4,6},{5,7},{6,4},{7,5},{8,10},{9,11},{10,... | collective-permute-start | bytes 491528 | tf_op jit(solution)/shard_map/ppermute | solution.py:51
  49.6 17.3 %collective-permute-start.14 = (bf16[160,1024]{1,0:T(8,128)(2,1)S(1)}, bf16[160,1024]{1,0:T(8,128)(2,1)S(1)}, u32[]{:S(2)}, u32[]{:S(2)}) collective-permute-start(bf16[160,1024]{1,0:T(8,128)(2,1)S(1)} %get-tuple-element.65), channel_id=1, source_target_pairs={{0,1},{1,0},{2,3},{3,2},{4,5},{5,4},{6,7},{7,6},{8,9},{9,8},{10,11... | collective-permute-start | bytes 983048 | tf_op jit(solution)/shard_map/ppermute | solution.py:51
  51.9 12.3 %copy-start.4 = (bf16[256,512]{1,0:T(8,128)(2,1)S(1)}, bf16[256,512]{1,0:T(8,128)(2,1)}, u32[]{:S(2)}) copy-start(bf16[256,512]{1,0:T(8,128)(2,1)} %gate_ref.1) | copy-start | bytes 786436
  51.9 12.3 %copy-start.5 = (f32[128]{0:T(128)S(1)}, f32[128]{0:T(128)}, u32[]{:S(2)}) copy-start(f32[128]{0:T(128)} %param.21) | copy-start | bytes 1540
  51.9 12.3 %collective-permute-start.9 = (bf16[224,512]{1,0:T(8,128)(2,1)S(1)}, bf16[224,512]{1,0:T(8,128)(2,1)S(1)}, u32[]{:S(2)}, u32[]{:S(2)}) collective-permute-start(bf16[224,512]{1,0:T(8,128)(2,1)S(1)} %get-tuple-element.59), channel_id=1, source_target_pairs={{0,16},{4,20},{8,24},{12,28},{16,0},{20,4},{24,8},{28,12},{1,17},{... | collective-permute-start | bytes 688136 | tf_op jit(solution)/shard_map/ppermute | solution.py:51
  54.6 36.1 %copy-start.11 = (s32[256,2]{0,1:T(2,128)S(1)}, s32[256,2]{0,1:T(2,128)}, u32[]{:S(2)}) copy-start(s32[256,2]{0,1:T(2,128)} %param.25) | copy-start | bytes 6148
  54.6 36.1 %copy-start.12 = (f32[256,2]{0,1:T(2,128)S(1)}, f32[256,2]{0,1:T(2,128)}, u32[]{:S(2)}) copy-start(f32[256,2]{0,1:T(2,128)} %param.26) | copy-start | bytes 6148
  54.6 42.7 %copy-start.3 = (bf16[2048,512]{1,0:T(8,128)(2,1)S(1)}, bf16[2048,512]{1,0:T(8,128)(2,1)}, u32[]{:S(2)}) copy-start(bf16[2048,512]{1,0:T(8,128)(2,1)} %param.22) | copy-start | bytes 6291460
  54.6 14.0 %collective-permute-start.19 = (bf16[160,1024]{1,0:T(8,128)(2,1)S(1)}, bf16[160,1024]{1,0:T(8,128)(2,1)S(1)}, u32[]{:S(2)}, u32[]{:S(2)}) collective-permute-start(bf16[160,1024]{1,0:T(8,128)(2,1)S(1)} %get-tuple-element.72), channel_id=1, source_target_pairs={{0,1},{1,0},{2,3},{3,2},{4,5},{5,4},{6,7},{7,6},{8,9},{9,8},{10,11... | collective-permute-start | bytes 983048 | tf_op jit(solution)/shard_map/ppermute | solution.py:51
  64.7 9.2 %collective-permute-start.10 = (bf16[256,512]{1,0:T(8,128)(2,1)S(1)}, bf16[256,512]{1,0:T(8,128)(2,1)S(1)}, u32[]{:S(2)}, u32[]{:S(2)}) collective-permute-start(bf16[256,512]{1,0:T(8,128)(2,1)S(1)} %shard_map.166.refs_0_), channel_id=1, source_target_pairs={{0,2},{1,3},{2,0},{3,1},{4,6},{5,7},{6,4},{7,5},{8,10},{9,11},{10,... | collective-permute-start | bytes 786440 | tf_op jit(solution)/shard_map/ppermute | solution.py:51
  66.4 11.1 %collective-permute-start.30 = (bf16[160,512]{1,0:T(8,128)(2,1)S(1)}, bf16[160,512]{1,0:T(8,128)(2,1)S(1)}, u32[]{:S(2)}, u32[]{:S(2)}) collective-permute-start(bf16[160,512]{1,0:T(8,128)(2,1)S(1)} %get-tuple-element.83), channel_id=1, source_target_pairs={{0,2},{1,3},{2,0},{3,1},{4,6},{5,7},{6,4},{7,5},{8,10},{9,11},{10,... | collective-permute-start | bytes 491528 | tf_op jit(solution)/shard_map/ppermute | solution.py:51
  67.0 13.9 %collective-permute-start.15 = (bf16[160,512]{1,0:T(8,128)(2,1)S(1)}, bf16[160,512]{1,0:T(8,128)(2,1)S(1)}, u32[]{:S(2)}, u32[]{:S(2)}) collective-permute-start(bf16[160,512]{1,0:T(8,128)(2,1)S(1)} %get-tuple-element.67), channel_id=1, source_target_pairs={{0,2},{1,3},{2,0},{3,1},{4,6},{5,7},{6,4},{7,5},{8,10},{9,11},{10,... | collective-permute-start | bytes 491528 | tf_op jit(solution)/shard_map/ppermute | solution.py:51
  68.7 14.8 %collective-permute-start.20 = (bf16[160,512]{1,0:T(8,128)(2,1)S(1)}, bf16[160,512]{1,0:T(8,128)(2,1)S(1)}, u32[]{:S(2)}, u32[]{:S(2)}) collective-permute-start(bf16[160,512]{1,0:T(8,128)(2,1)S(1)} %get-tuple-element.74), channel_id=1, source_target_pairs={{0,2},{1,3},{2,0},{3,1},{4,6},{5,7},{6,4},{7,5},{8,10},{9,11},{10,... | collective-permute-start | bytes 491528 | tf_op jit(solution)/shard_map/ppermute | solution.py:51
  69.2 28.1 %collective-permute-start.11 = (bf16[256,512]{1,0:T(8,128)(2,1)S(1)}, bf16[256,512]{1,0:T(8,128)(2,1)S(1)}, u32[]{:S(2)}, u32[]{:S(2)}) collective-permute-start(bf16[256,512]{1,0:T(8,128)(2,1)S(1)} %shard_map.166.refs_0_), channel_id=1, source_target_pairs={{0,1},{1,0},{2,3},{3,2},{4,5},{5,4},{6,7},{7,6},{8,9},{9,8},{10,11... | collective-permute-start | bytes 786440 | tf_op jit(solution)/shard_map/ppermute | solution.py:51
  73.9 23.4 %collective-permute-start.12 = (bf16[256,512]{1,0:T(8,128)(2,1)S(1)}, bf16[256,512]{1,0:T(8,128)(2,1)S(1)}, u32[]{:S(2)}, u32[]{:S(2)}) collective-permute-start(bf16[256,512]{1,0:T(8,128)(2,1)S(1)} %collective-permute-done.10.refs_1_), channel_id=1, source_target_pairs={{0,1},{1,0},{2,3},{3,2},{4,5},{5,4},{6,7},{7,6},{8,9},{9,8},{10,11... | collective-permute-start | bytes 786440 | tf_op jit(solution)/shard_map/ppermute | solution.py:51
  77.4 7.6 %collective-permute-start.23 = (bf16[80,512]{1,0:T(8,128)(2,1)S(1)}, bf16[80,512]{1,0:T(8,128)(2,1)S(1)}, u32[]{:S(2)}, u32[]{:S(2)}) collective-permute-start(bf16[80,512]{1,0:T(8,128)(2,1)S(1)} %get-tuple-element.77), channel_id=1, source_target_pairs={{0,20},{4,16},{8,28},{12,24},{16,4},{20,0},{24,12},{28,8},{1,21},{... | collective-permute-start | bytes 245768 | tf_op jit(solution)/shard_map/ppermute | solution.py:51
  80.9 6.3 %collective-permute-start.31 = (bf16[80,512]{1,0:T(8,128)(2,1)S(1)}, bf16[80,512]{1,0:T(8,128)(2,1)S(1)}, u32[]{:S(2)}, u32[]{:S(2)}) collective-permute-start(bf16[80,512]{1,0:T(8,128)(2,1)S(1)} %get-tuple-element.84), channel_id=1, source_target_pairs={{0,24},{4,28},{8,16},{12,20},{16,8},{20,12},{24,0},{28,4},{1,25},{... | collective-permute-start | bytes 245768 | tf_op jit(solution)/shard_map/ppermute | solution.py:51
  83.5 7.2 %collective-permute-start.32 = (bf16[80,512]{1,0:T(8,128)(2,1)S(1)}, bf16[80,512]{1,0:T(8,128)(2,1)S(1)}, u32[]{:S(2)}, u32[]{:S(2)}) collective-permute-start(bf16[80,512]{1,0:T(8,128)(2,1)S(1)} %get-tuple-element.85), channel_id=1, source_target_pairs={{0,28},{4,24},{8,20},{12,16},{16,12},{20,8},{24,4},{28,0},{1,29},{... | collective-permute-start | bytes 245768 | tf_op jit(solution)/shard_map/ppermute | solution.py:51
  85.0 6.2 %collective-permute-start.16 = (bf16[80,512]{1,0:T(8,128)(2,1)S(1)}, bf16[80,512]{1,0:T(8,128)(2,1)S(1)}, u32[]{:S(2)}, u32[]{:S(2)}) collective-permute-start(bf16[80,512]{1,0:T(8,128)(2,1)S(1)} %get-tuple-element.69), channel_id=1, source_target_pairs={{0,4},{4,0},{8,12},{12,8},{16,20},{20,16},{24,28},{28,24},{1,5},{5... | collective-permute-start | bytes 245768 | tf_op jit(solution)/shard_map/ppermute | solution.py:51
  87.3 4.6 %collective-permute-start.21 = (bf16[80,512]{1,0:T(8,128)(2,1)S(1)}, bf16[80,512]{1,0:T(8,128)(2,1)S(1)}, u32[]{:S(2)}, u32[]{:S(2)}) collective-permute-start(bf16[80,512]{1,0:T(8,128)(2,1)S(1)} %get-tuple-element.75), channel_id=1, source_target_pairs={{0,8},{4,12},{8,0},{12,4},{16,24},{20,28},{24,16},{28,20},{1,9},{5... | collective-permute-start | bytes 245768 | tf_op jit(solution)/shard_map/ppermute | solution.py:51
  90.7 5.3 %collective-permute-start.22 = (bf16[80,512]{1,0:T(8,128)(2,1)S(1)}, bf16[80,512]{1,0:T(8,128)(2,1)S(1)}, u32[]{:S(2)}, u32[]{:S(2)}) collective-permute-start(bf16[80,512]{1,0:T(8,128)(2,1)S(1)} %get-tuple-element.76), channel_id=1, source_target_pairs={{0,12},{4,8},{8,4},{12,0},{16,28},{20,24},{24,20},{28,16},{1,13},{... | collective-permute-start | bytes 245768 | tf_op jit(solution)/shard_map/ppermute | solution.py:51

commit v2 on v1

--- a/solution.py
+++ b/solution.py
@@ -9,7 +9,7 @@
 
 
 TOP_K = 2
-ROWS = 16
+ROWS = 8
 EPS = 1e-06
 F32 = jnp.float32
 BF16 = jnp.bfloat16
@@ -35,10 +35,10 @@
     return mm(a, high, dims) + mm(a, low, dims)
 
 
-def call(body, outs, args, flops, scratch=()):
+def call(body, outs, args, flops, scratch=(), near=False):
     return pl.pallas_call(
         body,
-        out_shape=tuple(jax.ShapeDtypeStruct(s, d) for s, d in outs),
+        out_shape=tuple(pltpu.VMEM(s, d) if near else jax.ShapeDtypeStruct(s, d) for s, d in outs),
         in_specs=[VMEM] * len(args),
         out_specs=tuple(VMEM for _ in outs),
         scratch_shapes=list(scratch),
@@ -49,6 +49,17 @@
 
 def swap(array, axis, size, bit):
     return lax.ppermute(array, axis, [(i, i ^ bit) for i in range(size)])
+
+
+def send(array, half, i):
+    peers = [(e, t, peer(half, i, t)) for e in range(2 * half) for t in range(4)]
+    pairs = [(e * 4 + t, (e ^ k) * 4 + t) for e, t, k in peers]
+    return lax.ppermute(array, ("ep", "tp"), pairs)
+
+
+def send_near(array, experts, i):
+    pairs = [(e * 4 + t, (e ^ (2 * i + (t & 1))) * 4 + t) for e in range(experts) for t in range(4)]
+    return lax.ppermute(array, ("ep", "tp"), pairs)
 
 
 def in_hbm(*arrays):
@@ -160,8 +171,7 @@
     size = gain_ref.shape[1]
     late = (lax.axis_index("ep") & bit) != 0
     pre = pair(pre_ref)
-    rec = pair(rec_ref, rec_ref.shape[0] - pre_ref.shape[0])
-    state = choose(late, after(rec, pre), pre)[0].astype(BF16)
+    state = choose(late, after(pair(rec_ref), pre), pre)[0].astype(BF16)
     for h in range(width // size):
         cut = slice(h * size, (h + 1) * size)
         got = within_ref[:, cut] + mm(qd_ref[:, cut], state[:, cut], NT)
@@ -194,37 +204,42 @@
     return mm(hit.astype(BF16), jnp.where(row < col, 1.0, 0.0).astype(BF16)), hit
 
 
-def spread_body(near, far, routes_ref, x_ref, gain_ref, *refs):
+def peer(half, i, at):
+    return half + i + (at & 1) * (half // 2)
+
+
+def spread_body(half, routes_ref, x_ref, gain_ref, *refs):
     normed_ref, rank_ref, mark_ref = refs[-3:]
-    outs = refs[:-3]
-    me = lax.axis_index("ep")
     at = lax.axis_index("tp")
-    groups, count, width = normed_ref.shape
+    groups, _, width = normed_ref.shape
     x = x_ref[...].astype(F32)
     scale = lax.rsqrt(jnp.mean(x * x, axis=1, keepdims=True) + EPS)
     normed = (x * scale * gain_ref[...]).astype(BF16)
     for q in range(groups):
         normed_ref[q] = normed[:, q * width : (q + 1) * width]
     rank_ref[...], mark_ref[...] = ranked(named(routes_ref[...], rank_ref.shape[0]))
-    slot = lax.broadcasted_iota(jnp.int32, (outs[0].shape[0], count), 0).astype(F32)
-
-    def chosen(k):
-        e = me ^ k
-        good = (rank_ref[pl.ds(e, 1), :] == slot) & (mark_ref[pl.ds(e, 1), :] > 0.5)
-        return jnp.where(good, 1.0, 0.0).astype(BF16)
-
-    for ref, k in zip(outs, far + near + (0,)):
-        pick = chosen(k)
-        if k in far:
-            ref[...] = mm(pick, normed_ref[at]).astype(BF16)
-        elif k in near:
-            for j in range(groups // 2):
-                ref[:, j * width : (j + 1) * width] = mm(
-                    pick, normed_ref[2 * j + (at & 1)]
-                ).astype(BF16)
-        else:
-            for q in range(groups):
-                ref[:, q * width : (q + 1) * width] = mm(pick, normed_ref[q]).astype(BF16)
+    for i, ref in enumerate(refs[:-3]):
+        pick = chosen(rank_ref, mark_ref, peer(half, i, at), ref.shape[0])
+        for j in range(groups // 2):
+            cut = slice(j * width, (j + 1) * width)
+            ref[:, cut] = mm(pick, normed_ref[2 * (at // 2) + j]).astype(BF16)
+
+
+def spread_near_body(near, normed_ref, rank_ref, mark_ref, *outs):
+    at = lax.axis_index("tp")
+    groups, _, width = normed_ref.shape
+    for ref, k in zip(outs, near + (0,)):
+        pick = chosen(rank_ref, mark_ref, k, ref.shape[0])
+        for j in range(groups // 2 if k else groups):
+            cut = slice(j * width, (j + 1) * width)
+            ref[:, cut] = mm(pick, normed_ref[2 * j + (at & 1) if k else j]).astype(BF16)
+
+
+def chosen(rank_ref, mark_ref, k, cap):
+    e = lax.axis_index("ep") ^ k
+    slot = lax.broadcasted_iota(jnp.int32, (cap, rank_ref.shape[1]), 0).astype(F32)
+    good = (rank_ref[pl.ds(e, 1), :] == slot) & (mark_ref[pl.ds(e, 1), :] > 0.5)
+    return jnp.where(good, 1.0, 0.0).astype(BF16)
 
 
 def places_body(order, experts, routes_ref, weight_ref, first_ref, second_ref, column_ref, row_ref):
@@ -253,9 +268,10 @@
 def expert_body(plan, cap, wg_ref, wu_ref, wd_ref, *refs):
     mine_ref, other_ref, x_ref, acc_ref = refs[-4:]
     at = lax.axis_index("tp")
-    width = mine_ref.shape[1] // 2
+    width = x_ref.shape[1] // 4
     for (block, count, piece), ref in zip(plan, refs[:-4]):
-        rows = slice(block * cap, (block + count) * cap)
+        first = block(at) * cap
+        rows = pl.ds(first if isinstance(first, int) else pl.multiple_of(first, cap), count * cap)
         for j, quarter in enumerate(piece(at)):
             lane = pl.multiple_of(quarter * width, width)
             x_ref[rows, pl.ds(lane, width)] = ref[0 : count * cap, j * width : (j + 1) * width]
@@ -268,19 +284,15 @@
         up = mm(x, wu_ref[0, :, c : c + chunk])
         parts.append((gate * jax.nn.sigmoid(gate) * up).astype(BF16))
     acc_ref[...] = mm(jnp.concatenate(parts, axis=1), wd_ref[0]).astype(BF16)
-    for j in range(2):
-        cut = slice(j * width, (j + 1) * width)
-        lane = pl.multiple_of((2 * j + (at & 1)) * width, width)
-        mine_ref[:, cut] = acc_ref[:, pl.ds(lane, width)]
-        lane = pl.multiple_of((2 * j + 1 - (at & 1)) * width, width)
-        other_ref[:, cut] = acc_ref[:, pl.ds(lane, width)]
+    for ref, block in ((mine_ref, at & 1), (other_ref, 1 - (at & 1))):
+        ref[...] = acc_ref[pl.ds(pl.multiple_of(block * cap, cap), cap), :]
 
 
 def expert_call(wg, wu, wd, pieces, plan, blocks, cap):
     depth, hidden = wg.shape[1:]
     width = wd.shape[2]
     rows = blocks * cap
-    half = ((rows, width // 2), BF16)
+    half = ((cap, width), BF16)
     return call(
         functools.partial(expert_body, plan, cap),
         [half, half],
@@ -305,26 +317,28 @@
         out_ref[i * rows : (i + 1) * rows, :] = ref[0:rows, :]
 
 
-def add_body(keep_ref, got_ref, *refs):
-    outs = refs[-2:]
-    rows = keep_ref.shape[0] // 2
-    if len(refs) == 3:
-        outs[0][rows:, :] = refs[0][...]
-    for i, ref in enumerate(outs):
-        cut = slice(i * rows, (i + 1) * rows)
-        ref[0:rows, :] = (keep_ref[cut, :].astype(F32) + got_ref[cut, :].astype(F32)).astype(BF16)
-
-
-def combine_body(column_ref, first_ref, second_ref, *refs):
+def add_body(keep_ref, got_ref, out_ref):
+    out_ref[...] = (keep_ref[...].astype(F32) + got_ref[...].astype(F32)).astype(BF16)
+
+
+def combine_body(start, column_ref, first_ref, second_ref, *refs):
     out_ref, all_ref = refs[-2:]
-    cap = all_ref.shape[0] // (len(refs) - 2)
-    for i, ref in enumerate(refs[:-2]):
-        all_ref[i * cap : (i + 1) * cap, :] = ref[0:cap, :]
+    earlier = refs[:-2][len(refs) - 2 - (len(refs) - 2) % 2 :]
+    blocks = refs[: (len(refs) - 2) // 2 * 2]
+    core = lax.axis_index("tp") & 1
+    cap, width = blocks[0].shape[0], out_ref.shape[1]
+    cut = pl.ds(pl.multiple_of(core * width, width), width)
+    for i in range(0, len(blocks), 2):
+        for ref, side in ((blocks[i], core), (blocks[i + 1], 1 - core)):
+            rows = pl.ds(pl.multiple_of((i + side) * cap, cap), cap)
+            all_ref[rows, :] = ref[:, cut]
     weight = column_ref[:, TOP_K : 2 * TOP_K]
     back = all_ref[...]
-    out_ref[...] = (
-        weight[:, 0:1] * mm(first_ref[...], back) + weight[:, 1:2] * mm(second_ref[...], back)
-    ).astype(BF16)
+    total = weight[:, 0:1] * mm(first_ref[:, start * cap : start * cap + back.shape[0]], back)
+    total += weight[:, 1:2] * mm(second_ref[:, start * cap : start * cap + back.shape[0]], back)
+    for ref in earlier:
+        total += ref[...]
+    out_ref[...] = total.astype(out_ref.dtype)
 
 
 def carried_in(own, place):
@@ -399,25 +413,26 @@
     head_gain = head_gain.reshape(1, -1)
     half = experts // 2
     near = tuple(range(1, half))
-    far = tuple(range(half, experts))
     block = lambda n: ((cap, n), BF16)
     padded = -(-experts // ROWS) * ROWS
 
     if direct:
-        sent = call(
-            functools.partial(spread_body, near, far),
-            [block(slice_width)] * len(far) + [block(depth // 2)] * len(near) + [block(depth)],
+        marks = ((padded, count), F32)
+        *sent, normed, rank, mark = call(
+            functools.partial(spread_body, half),
+            [block(depth // 2)] * (half // 2)
+            + [((groups, count, slice_width), BF16), marks, marks],
             in_hbm(routes.T, moe_input, moe_gain.reshape(1, -1)),
             LONG,
-            scratch=[
-                pltpu.VMEM((groups, count, slice_width), BF16),
-                pltpu.VMEM((padded, count), F32),
-                pltpu.VMEM((padded, count), F32),
-            ],
         )
-        own_rows = sent[-1]
-        far_in = {k: swap(a, "ep", experts, k) for k, a in zip(far, sent)}
-        near_out = dict(zip(near, sent[len(far) :]))
+        far_in = [send(a, half, i) for i, a in enumerate(sent)]
+        *near_rows, own_rows = call(
+            functools.partial(spread_near_body, near),
+            [block(depth // 2)] * len(near) + [block(depth)],
+            [normed, rank, mark],
+            0,
+        )
+        near_out = dict(zip(near, near_rows))
         near_in = {}
 
     state_shape = ((size + ROWS, width), BF16)
@@ -450,54 +465,56 @@
             if k not in near_in:
                 near_in[k] = swap(near_out[k], "ep", experts, k)
 
-    def gathered(keys):
-        if 0 in keys:
+    own_half = lambda at: (at & 1, 2 + (at & 1))
+    other_half = lambda at: (1 - (at & 1), 3 - (at & 1))
+    everything = lambda at: tuple(range(groups))
+    own_plane = lambda at: (at // 2 * 2, at // 2 * 2 + 1)
+    other_plane = lambda at: (2 - at // 2 * 2, 3 - at // 2 * 2)
+    zero, one = (lambda at: 0), (lambda at: 1)
+    own_core, other_core = (lambda at: at & 1), (lambda at: 1 - (at & 1))
+
+    def gathered(i):
+        if i == 0:
             here = near_in[1]
             pieces = [own_rows, here, swap(here, "tp", groups, 1)]
-            return pieces, [(0, 1, everything), (1, 1, own_half), (1, 1, other_half)]
-        wide = keys[0] in near
-        source = near_in if wide else far_in
-        here = call(
-            pack_body,
-            [((2 * cap, depth // 2 if wide else slice_width), BF16)],
-            [source[k] for k in keys],
-            0,
-        )[0]
-        pieces = [here, swap(here, "tp", groups, 1)]
-        if wide:
-            return pieces, [(0, 2, own_half), (0, 2, other_half)]
+            return pieces, [(zero, 1, everything), (one, 1, own_half), (one, 1, other_half)]
+        if i < half // 2:
+            here = call(
+                pack_body, [((2 * cap, depth // 2), BF16)], [near_in[2 * i], near_in[2 * i + 1]], 0
+            )[0]
+            pieces = [here, swap(here, "tp", groups, 1)]
+            return pieces, [(zero, 2, own_half), (zero, 2, other_half)]
+        here = far_in[i - half // 2]
         there = swap(here, "tp", groups, 2)
-        pieces += [there, swap(there, "tp", groups, 1)]
-        return pieces, [(0, 2, only(mask)) for mask in (0, 1, 2, 3)]
-
-    own_half = lambda at: (at & 1, 2 + (at & 1))
-    other_half = lambda at: (1 - (at & 1), 3 - (at & 1))
-    only = lambda mask: (lambda at: (at ^ mask,))
-    everything = lambda at: tuple(range(groups))
+        pieces = [here, there]
+        pieces += [swap(here, "tp", groups, 1), swap(there, "tp", groups, 1)]
+        return pieces, [
+            (own_core, 1, own_plane),
+            (own_core, 1, other_plane),
+            (other_core, 1, own_plane),
+            (other_core, 1, other_plane),
+        ]
 
     if direct:
         weights = (w_exp_gate, w_exp_up, w_exp_down)
-        returned = {}
-        for i in range(experts // 2):
-            keys = (2 * i, 2 * i + 1)
-            rows = 2 * cap
-            pieces, plan = gathered(keys)
+        returned, order = [], []
+        for i in (0, *range(half // 2, half), *range(1, half // 2)):
+            pieces, plan = gathered(i)
             mine, other = expert_call(*weights, pieces, plan, 2, cap)
             got = swap(other, "tp", groups, 1)
-            quarter = ((rows, slice_width), BF16)
-            keep, send = call(halve_body, [quarter, quarter], [mine, got], 0)
-            back = swap(send, "tp", groups, 2)
-            with_state = half in keys
-            done = call(
-                add_body,
-                [((cap + size + ROWS, width), BF16) if with_state else block(slice_width)]
-                + [block(slice_width)],
-                [keep, back] + ([total] if with_state else []),
-                0,
-            )
-            for k, a in zip(keys, done):
-                returned[k] = swap(a, "ep", experts, k) if k else a
-        got = returned[half]
+            plane = block(depth // 2)
+            keep, give = call(halve_body, [plane, plane], [mine, got], 0)
+            back = swap(give, "tp", groups, 2)
+            done = call(add_body, [plane], [keep, back], 0)[0]
+            if i < half // 2:
+                order += [2 * i, 2 * i + 1]
+                home = send_near(done, experts, i)
+            else:
+                order += [peer(half, i - half // 2, core) for core in range(2)]
+                home = send(done, half, i - half // 2)
+            returned += [home, swap(home, "tp", groups, 1)]
+        pairs = [(i, i ^ half) for i in range(experts) if not i & half]
+        got = lax.ppermute(total, "ep", pairs)
         before = before[0]
         bit = half
     else:
@@ -519,6 +536,7 @@
             [((length, w_mix_out.shape[1]), BF16)],
             [w_mix_out.reshape(groups, width, -1)] + pieces,
             2 * length * groups * width * w_mix_out.shape[1],
+            near=True,
         )[0]
     else:
         mixed = jnp.dot(
@@ -531,7 +549,6 @@
         )
         return (mixed, moe_out)
 
-    order = (0,) + near + far
     first, second, column = call(
         functools.partial(places_body, order, padded),
         [((count, experts * cap), BF16)] * TOP_K + [((count, 8), F32)],
@@ -539,12 +556,20 @@
         2 * count * count * padded,
         scratch=[pltpu.VMEM((8, count), F32)],
     )
+    seats = [column, first, second]
+    part = call(
+        functools.partial(combine_body, 0),
+        [((count, slice_width), F32)],
+        seats + returned[:-2],
+        4 * count * experts * cap * slice_width,
+        scratch=[pltpu.VMEM(((experts - 2) * cap, slice_width), BF16)],
+    )
     moe_out = call(
-        combine_body,
+        functools.partial(combine_body, experts - 2),
         [((count, slice_width), BF16)],
-        [column, first, second] + [returned[k] for k in order],
-        4 * count * experts * cap * slice_width,
-        scratch=[pltpu.VMEM((experts * cap, slice_width), BF16)],
+        seats + returned[-2:] + list(part),
+        4 * count * 2 * cap * slice_width,
+        scratch=[pltpu.VMEM((2 * cap, slice_width), BF16)],
     )[0]
     return (mixed, moe_out)
 

time: 98.9 us -> 94.4 us (0.954)
  waiting for transfers between devices: 54 us -> 35.7 us
  starting transfers between devices: 25.7 us -> 39 us
    ppermute x33 -> x26, waiting for transfers between devices: 54 us -> 17.3 us  [swap(): return lax.ppermute(array, axis, [(i, i ^ bit) for i in range(size)])]
    ppermute x0 -> x7, waiting for transfers between devices: none -> 18.5 us  [the longest x4 16.4 us: send(): return lax.ppermute(array, ('ep', 'tp'), pairs)]
    ppermute x0 -> x7, starting transfers between devices: none -> 15.9 us  [the longest x4 11 us: send(): return lax.ppermute(array, ('ep', 'tp'), pairs)]
    ppermute x33 -> x26, starting transfers between devices: 25.7 us -> 23.1 us  [swap(): return lax.ppermute(array, axis, [(i, i ^ bit) for i in range(size)])]
  transfers between devices with their start and end apart: 33 -> 33, of which waited for: 17 -> 9; matrix products, arithmetic and copies ran while one was open for 0% -> 1% of each run, Pallas kernels for 14% -> 15%
where the time goes in v2:
time: 94.4 us; the launch traced here: 94.2 us
  starting transfers between devices  39 us (41%)
  waiting for transfers between devices  35.7 us (38%)
  Pallas kernels  17.8 us (19%)
  between operations  1 us (1%)
    ppermute x26, starting transfers between devices, swap(): return lax.ppermute(array, axis, [(i, i ^ bit) for i in range(size)])  23.1 us
    pallas_call x23, Pallas kernels, call(): pl.pallas_call(body, out_shape=tuple((pltpu.VMEM(s, d) if near else jax.S...  17.8 us
    ppermute x26, waiting for transfers between devices, swap(): return lax.ppermute(array, axis, [(i, i ^ bit) for i in range(size)])  17.3 us
    ppermute x4, waiting for transfers between devices, send(): return lax.ppermute(array, ('ep', 'tp'), pairs)  16.4 us
    ppermute x4, starting transfers between devices, send(): return lax.ppermute(array, ('ep', 'tp'), pairs)  11 us
    ppermute x1, starting transfers between devices, body(): got = lax.ppermute(total, 'ep', pairs)  4.16 us
  transfers between devices with their start and end apart: 33, of which 9 were waited for; matrix products, arithmetic and copies ran while one was open for 1% of the time, Pallas kernels for 15%

profile of v2, /device:TPU:0, one launch (start us, length us, event | category | flops | bytes accessed | tf_op | source)
XLA Modules:
  0.0 94.2 jit_solution(6974149280298810744)
XLA Ops:
  0.7 2.2 %shard_map.158 = (bf16[80,1024]{1,0:T(8,128)(2,1)S(1)}, bf16[80,1024]{1,0:T(8,128)(2,1)S(1)}, bf16[4,256,512]{2,1,0:T(8,128)(2,1)S(1)}, f32[8,256]{1,0:T(8,128)S(1)}, f32[8,256]{1,0:T(8,128)S(1)}) custom-call(s32[2,256]{1,0:T(2,128)} %bitcast.8, bf16[256,2048]{1,0:T(8,128)(2,1)} %x_ref.2, f32[1,2048]{1,0:T(1,128)} %bitcast.14), custom_call_target="tpu_custom_call" | custom-call | flops 20000000000 | bytes 1048576 | tf_op jit(solution)/shard_map/pallas_call | solution.py:39
  2.9 4.1 %collective-permute-start.17 = (bf16[80,1024]{1,0:T(8,128)(2,1)S(1)}, bf16[80,1024]{1,0:T(8,128)(2,1)S(1)}, u32[]{:S(2)}, u32[]{:S(2)}) collective-permute-start(bf16[80,1024]{1,0:T(8,128)(2,1)S(1)} %get-tuple-element.62), channel_id=1, source_target_pairs={{0,16},{1,25},{2,18},{3,27},{4,20},{5,29},{6,22},{7,31},{8,24},{9,... | collective-permute-start | bytes 491528 | tf_op jit(solution)/shard_map/ppermute | solution.py:57
  7.0 0.6 shard_map.159
  7.6 0.0 copy-start
  7.6 0.0 copy-start.1
  7.7 0.0 copy-start.2
  7.7 1.4 %shard_map.160 = (bf16[152,1024]{1,0:T(8,128)(2,1)S(1)}, bf16[256,512]{1,0:T(8,128)(2,1)S(1)}, f32[256,512]{1,0:T(8,128)S(1)}) custom-call(bf16[256,512]{1,0:T(8,128)(2,1)S(1)} %copy-done.8, bf16[256,512]{1,0:T(8,128)(2,1)S(1)} %copy-done.9, bf16[256,512]{1,0:T(8,128)(2,1)S(1)} %copy-done.10, f32[4,256]{1,0:T(4,128)S(1)} %bitcast.12, f32[1,512]{1,0:T(1,128)S(1)} %bitcast.13, ...), custom_call_target="tpu_custom_call" | custom-call | flops 20000000000 | bytes 1048576 | tf_op jit(solution)/shard_map/pallas_call | solution.py:39
  9.1 1.6 %collective-permute-start = (bf16[152,1024]{1,0:T(8,128)(2,1)S(1)}, bf16[152,1024]{1,0:T(8,128)(2,1)S(1)}, u32[]{:S(2)}, u32[]{:S(2)}) collective-permute-start(bf16[152,1024]{1,0:T(8,128)(2,1)S(1)} %get-tuple-element.43.refs_0_), channel_id=1, source_target_pairs={{0,4},{4,0},{8,12},{12,8},{16,20},{20,16},{24,28},{28,24},{1,5},{5... | collective-permute-start | bytes 933896 | tf_op jit(solution)/shard_map/ppermute | solution.py:51
  10.7 0.0 collective-permute-start.25
  10.7 8.4 %collective-permute-done.17.refs_0_ = bf16[80,1024]{1,0:T(8,128)(2,1)S(1)} collective-permute-done((bf16[80,1024]{1,0:T(8,128)(2,1)S(1)}, bf16[80,1024]{1,0:T(8,128)(2,1)S(1)}, u32[]{:S(2)}, u32[]{:S(2)}) %collective-permute-start.17) | collective-permute-done | bytes 163872 | tf_op jit(solution)/shard_map/ppermute | solution.py:57
  19.1 1.8 %collective-permute-start.18 = (bf16[80,1024]{1,0:T(8,128)(2,1)S(1)}, bf16[80,1024]{1,0:T(8,128)(2,1)S(1)}, u32[]{:S(2)}, u32[]{:S(2)}) collective-permute-start(bf16[80,1024]{1,0:T(8,128)(2,1)S(1)} %collective-permute-done.17.refs_0_), channel_id=1, source_target_pairs={{0,2},{1,3},{2,0},{3,1},{4,6},{5,7},{6,4},{7,5},{8,10},{9,11},{10,... | collective-permute-start | bytes 491528 | tf_op jit(solution)/shard_map/ppermute | solution.py:51
  20.9 2.0 %collective-permute-done.25.refs_0_ = bf16[80,1024]{1,0:T(8,128)(2,1)S(1)} collective-permute-done((bf16[80,1024]{1,0:T(8,128)(2,1)S(1)}, bf16[80,1024]{1,0:T(8,128)(2,1)S(1)}, u32[]{:S(2)}, u32[]{:S(2)}) %collective-permute-start.25) | collective-permute-done | bytes 163872 | tf_op jit(solution)/shard_map/ppermute | solution.py:57
  22.8 1.5 %collective-permute-start.26 = (bf16[80,1024]{1,0:T(8,128)(2,1)S(1)}, bf16[80,1024]{1,0:T(8,128)(2,1)S(1)}, u32[]{:S(2)}, u32[]{:S(2)}) collective-permute-start(bf16[80,1024]{1,0:T(8,128)(2,1)S(1)} %collective-permute-done.25.refs_0_), channel_id=1, source_target_pairs={{0,2},{1,3},{2,0},{3,1},{4,6},{5,7},{6,4},{7,5},{8,10},{9,11},{10,... | collective-permute-start | bytes 491528 | tf_op jit(solution)/shard_map/ppermute | solution.py:51
  24.4 0.9 collective-permute-done.18.refs_1_
  25.3 0.0 collective-permute-done.refs_1_
  25.3 0.1 shard_map.161
  25.4 0.3 collective-permute-start.1
  25.7 2.9 %collective-permute-start.6 = (bf16[80,1024]{1,0:T(8,128)(2,1)S(1)}, bf16[80,1024]{1,0:T(8,128)(2,1)S(1)}, u32[]{:S(2)}, u32[]{:S(2)}) collective-permute-start(bf16[80,1024]{1,0:T(8,128)(2,1)S(1)} %get-tuple-element.52), channel_id=1, source_target_pairs={{0,12},{4,8},{8,4},{12,0},{16,28},{20,24},{24,20},{28,16},{1,13},{... | collective-permute-start | bytes 491528 | tf_op jit(solution)/shard_map/ppermute | solution.py:51
  28.6 0.5 collective-permute-start.12
  29.1 0.1 collective-permute-start.28
  29.1 2.3 %shard_map.173 = (bf16[80,2048]{1,0:T(8,128)(2,1)S(1)}, bf16[80,2048]{1,0:T(8,128)(2,1)S(1)}) custom-call(bf16[1,2048,1024]{2,1,0:T(8,128)(2,1)S(1)} %copy-done, bf16[1,2048,1024]{2,1,0:T(8,128)(2,1)S(1)} %copy-done.1, bf16[1,1024,2048]{2,1,0:T(8,128)(2,1)S(1)} %copy-done.2, bf16[80,1024]{1,0:T(8,128)(2,1)S(1)} %collective-permute-done.17.refs_0_, ...), custom_call_target="tpu_custom_call" | custom-call | flops 2013265920 | bytes 1048576 | tf_op jit(solution)/shard_map/pallas_call | solution.py:39
  31.5 8.3 %collective-permute-done.6.refs_1_ = bf16[80,1024]{1,0:T(8,128)(2,1)S(1)} collective-permute-done((bf16[80,1024]{1,0:T(8,128)(2,1)S(1)}, bf16[80,1024]{1,0:T(8,128)(2,1)S(1)}, u32[]{:S(2)}, u32[]{:S(2)}) %collective-permute-start.6) | collective-permute-done | bytes 163872 | tf_op jit(solution)/shard_map/ppermute | solution.py:51
  39.8 0.6 collective-permute-start.7
  40.4 2.3 %shard_map.176 = (bf16[80,2048]{1,0:T(8,128)(2,1)S(1)}, bf16[80,2048]{1,0:T(8,128)(2,1)S(1)}) custom-call(bf16[1,2048,1024]{2,1,0:T(8,128)(2,1)S(1)} %copy-done, bf16[1,2048,1024]{2,1,0:T(8,128)(2,1)S(1)} %copy-done.1, bf16[1,1024,2048]{2,1,0:T(8,128)(2,1)S(1)} %copy-done.2, bf16[80,1024]{1,0:T(8,128)(2,1)S(1)} %collective-permute-done.25.refs_0_, ...), custom_call_target="tpu_custom_call" | custom-call | flops 2013265920 | bytes 1048576 | tf_op jit(solution)/shard_map/pallas_call | solution.py:39
  42.8 0.1 collective-permute-start.29
  42.9 2.4 %shard_map.170 = (bf16[80,2048]{1,0:T(8,128)(2,1)S(1)}, bf16[80,2048]{1,0:T(8,128)(2,1)S(1)}) custom-call(bf16[1,2048,1024]{2,1,0:T(8,128)(2,1)S(1)} %copy-done, bf16[1,2048,1024]{2,1,0:T(8,128)(2,1)S(1)} %copy-done.1, bf16[1,1024,2048]{2,1,0:T(8,128)(2,1)S(1)} %copy-done.2, bf16[80,2048]{1,0:T(8,128)(2,1)S(1)} %get-tuple-element.57.refs_0_, ...), custom_call_target="tpu_custom_call" | custom-call | flops 2013265920 | bytes 1048576 | tf_op jit(solution)/shard_map/pallas_call | solution.py:39
  45.2 0.0 copy-start.4
  45.3 0.0 copy-start.7
  45.3 0.5 collective-permute-start.13
  45.8 2.6 %shard_map.167 = (bf16[80,2048]{1,0:T(8,128)(2,1)S(1)}, bf16[80,2048]{1,0:T(8,128)(2,1)S(1)}) custom-call(bf16[1,2048,1024]{2,1,0:T(8,128)(2,1)S(1)} %copy-done, bf16[1,2048,1024]{2,1,0:T(8,128)(2,1)S(1)} %copy-done.1, bf16[1,1024,2048]{2,1,0:T(8,128)(2,1)S(1)} %copy-done.2, bf16[160,1024]{1,0:T(8,128)(2,1)S(1)} %shard_map.166.refs_0_, ...), custom_call_target="tpu_custom_call" | custom-call | flops 2013265920 | bytes 1048576 | tf_op jit(solution)/shard_map/pallas_call | solution.py:39
  48.4 0.0 copy-start.5
  48.4 0.0 copy-start.6
  48.4 0.0 copy-start.3
  48.4 0.1 collective-permute-start.8
  48.5 0.1 shard_map.162
  48.7 4.2 %collective-permute-start.2 = (bf16[136,512]{1,0:T(8,128)(2,1)S(1)}, bf16[136,512]{1,0:T(8,128)(2,1)S(1)}, u32[]{:S(2)}, u32[]{:S(2)}) collective-permute-start(bf16[136,512]{1,0:T(8,128)(2,1)S(1)} %get-tuple-element.48), channel_id=1, source_target_pairs={{0,16},{4,20},{8,24},{12,28},{1,17},{5,21},{9,25},{13,29},{2,18},{... | collective-permute-start | bytes 417800 | tf_op jit(solution)/shard_map/ppermute | solution.py:517
  52.8 0.1 shard_map.174
  52.9 2.6 %collective-permute-start.22 = (bf16[80,1024]{1,0:T(8,128)(2,1)S(1)}, bf16[80,1024]{1,0:T(8,128)(2,1)S(1)}, u32[]{:S(2)}, u32[]{:S(2)}) collective-permute-start(bf16[80,1024]{1,0:T(8,128)(2,1)S(1)} %get-tuple-element.66), channel_id=1, source_target_pairs={{0,2},{1,3},{2,0},{3,1},{4,6},{5,7},{6,4},{7,5},{8,10},{9,11},{10,... | collective-permute-start | bytes 491528 | tf_op jit(solution)/shard_map/ppermute | solution.py:51
  55.5 0.8 collective-permute-done.2.rec_ref
  56.3 0.4 shard_map.163.refs_0_
  56.7 2.6 %collective-permute-start.3 = (bf16[256,512]{1,0:T(8,128)(2,1)S(1)}, bf16[256,512]{1,0:T(8,128)(2,1)S(1)}, u32[]{:S(2)}, u32[]{:S(2)}) collective-permute-start(bf16[256,512]{1,0:T(8,128)(2,1)S(1)} %shard_map.163.refs_0_), channel_id=1, source_target_pairs={{0,2},{1,3},{2,0},{3,1},{4,6},{5,7},{6,4},{7,5},{8,10},{9,11},{10,... | collective-permute-start | bytes 786440 | tf_op jit(solution)/shard_map/ppermute | solution.py:51
  59.3 0.1 shard_map.177
  59.4 0.2 collective-permute-start.30
  59.6 0.1 shard_map.171
  59.7 2.0 %collective-permute-start.14 = (bf16[80,1024]{1,0:T(8,128)(2,1)S(1)}, bf16[80,1024]{1,0:T(8,128)(2,1)S(1)}, u32[]{:S(2)}, u32[]{:S(2)}) collective-permute-start(bf16[80,1024]{1,0:T(8,128)(2,1)S(1)} %get-tuple-element.61), channel_id=1, source_target_pairs={{0,2},{1,3},{2,0},{3,1},{4,6},{5,7},{6,4},{7,5},{8,10},{9,11},{10,... | collective-permute-start | bytes 491528 | tf_op jit(solution)/shard_map/ppermute | solution.py:51
  61.6 0.1 shard_map.168
  61.7 0.3 collective-permute-start.9
  62.1 7.9 %collective-permute-done.30.got_ref = bf16[80,1024]{1,0:T(8,128)(2,1)S(1)} collective-permute-done((bf16[80,1024]{1,0:T(8,128)(2,1)S(1)}, bf16[80,1024]{1,0:T(8,128)(2,1)S(1)}, u32[]{:S(2)}, u32[]{:S(2)}) %collective-permute-start.30) | collective-permute-done | bytes 163872 | tf_op jit(solution)/shard_map/ppermute | solution.py:51
  70.0 3.4 %collective-permute-start.23 = (bf16[80,1024]{1,0:T(8,128)(2,1)S(1)}, bf16[80,1024]{1,0:T(8,128)(2,1)S(1)}, u32[]{:S(2)}, u32[]{:S(2)}) collective-permute-start(bf16[80,1024]{1,0:T(8,128)(2,1)S(1)} %shard_map.175), channel_id=1, source_target_pairs={{0,16},{1,25},{2,18},{3,27},{4,20},{5,29},{6,22},{7,31},{8,24},{9,... | collective-permute-start | bytes 491528 | tf_op jit(solution)/shard_map/ppermute | solution.py:57
  73.4 0.0 collective-permute-done.14.got_ref
  73.5 3.4 %collective-permute-start.31 = (bf16[80,1024]{1,0:T(8,128)(2,1)S(1)}, bf16[80,1024]{1,0:T(8,128)(2,1)S(1)}, u32[]{:S(2)}, u32[]{:S(2)}) collective-permute-start(bf16[80,1024]{1,0:T(8,128)(2,1)S(1)} %shard_map.178), channel_id=1, source_target_pairs={{0,20},{1,29},{2,22},{3,31},{4,16},{5,25},{6,18},{7,27},{8,28},{9,... | collective-permute-start | bytes 491528 | tf_op jit(solution)/shard_map/ppermute | solution.py:57
  76.9 0.7 collective-permute-start.15
  77.6 4.9 %collective-permute-start.5 = (bf16[256,512]{1,0:T(8,128)(2,1)S(1)}, bf16[256,512]{1,0:T(8,128)(2,1)S(1)}, u32[]{:S(2)}, u32[]{:S(2)}) collective-permute-start(bf16[256,512]{1,0:T(8,128)(2,1)S(1)} %collective-permute-done.3.refs_1_), channel_id=1, source_target_pairs={{0,1},{1,0},{2,3},{3,2},{4,5},{5,4},{6,7},{7,6},{8,9},{9,8},{10,11... | collective-permute-start | bytes 786440 | tf_op jit(solution)/shard_map/ppermute | solution.py:51
  82.6 0.1 collective-permute-start.10
  82.6 2.6 %collective-permute-done.23.refs_2_ = bf16[80,1024]{1,0:T(8,128)(2,1)S(1)} collective-permute-done((bf16[80,1024]{1,0:T(8,128)(2,1)S(1)}, bf16[80,1024]{1,0:T(8,128)(2,1)S(1)}, u32[]{:S(2)}, u32[]{:S(2)}) %collective-permute-start.23) | collective-permute-done | bytes 163872 | tf_op jit(solution)/shard_map/ppermute | solution.py:57
  85.2 3.5 %collective-permute-done.31.refs_4_ = bf16[80,1024]{1,0:T(8,128)(2,1)S(1)} collective-permute-done((bf16[80,1024]{1,0:T(8,128)(2,1)S(1)}, bf16[80,1024]{1,0:T(8,128)(2,1)S(1)}, u32[]{:S(2)}, u32[]{:S(2)}) %collective-permute-start.31) | collective-permute-done | bytes 163872 | tf_op jit(solution)/shard_map/ppermute | solution.py:57
  88.7 0.5 collective-permute-start.16
  89.2 1.3 %collective-permute-done.10.refs_0_ = bf16[80,1024]{1,0:T(8,128)(2,1)S(1)} collective-permute-done((bf16[80,1024]{1,0:T(8,128)(2,1)S(1)}, bf16[80,1024]{1,0:T(8,128)(2,1)S(1)}, u32[]{:S(2)}, u32[]{:S(2)}) %collective-permute-start.10) | collective-permute-done | bytes 163872 | tf_op jit(solution)/shard_map/ppermute | solution.py:62
  90.5 0.2 collective-permute-start.11
  90.7 0.5 shard_map.165
  91.2 0.7 shard_map.164
  92.0 0.7 copy.17
  92.7 0.5 shard_map.179.refs_2_
  93.2 1.1 %shard_map.180 = bf16[256,512]{1,0:T(8,128)(2,1)} custom-call(f32[256,8]{1,0:T(8,128)S(1)} %get-tuple-element.49.column_ref, bf16[256,640]{1,0:T(8,128)(2,1)S(1)} %get-tuple-element.50.first_ref, bf16[256,640]{1,0:T(8,128)(2,1)S(1)} %get-tuple-element.51.second_ref, bf16[80,1024]{1,0:T(8,128)(2,1)S(1)} %collective-permute-done.10.refs_0_, ...), custom_call_target="tpu_custom_call" | custom-call | flops 83886080 | bytes 1048576 | tf_op jit(solution)/shard_map/pallas_call | solution.py:39
  (52 shorter events, 0.3 us)
Async XLA Ops:
  0.6 7.0 %copy-start.8 = (bf16[256,512]{1,0:T(8,128)(2,1)S(1)}, bf16[256,512]{1,0:T(8,128)(2,1)}, u32[]{:S(2)}) copy-start(bf16[256,512]{1,0:T(8,128)(2,1)} %q_ref.1) | copy-start | bytes 786436
  0.6 7.0 %copy-start.9 = (bf16[256,512]{1,0:T(8,128)(2,1)S(1)}, bf16[256,512]{1,0:T(8,128)(2,1)}, u32[]{:S(2)}) copy-start(bf16[256,512]{1,0:T(8,128)(2,1)} %x_ref.3) | copy-start | bytes 786436
  0.7 7.0 %copy-start.10 = (bf16[256,512]{1,0:T(8,128)(2,1)S(1)}, bf16[256,512]{1,0:T(8,128)(2,1)}, u32[]{:S(2)}) copy-start(bf16[256,512]{1,0:T(8,128)(2,1)} %v_ref.1) | copy-start | bytes 786436
  0.7 7.0 %copy-start.11 = (f32[256,4]{0,1:T(4,128)S(1)}, f32[256,4]{0,1:T(4,128)}, u32[]{:S(2)}) copy-start(f32[256,4]{0,1:T(4,128)} %param.19) | copy-start | bytes 12292
  0.7 7.0 %copy-start.12 = (f32[512]{0:T(512)S(1)}, f32[512]{0:T(512)}, u32[]{:S(2)}) copy-start(f32[512]{0:T(512)} %param.20) | copy-start | bytes 6148
  2.9 16.2 %collective-permute-start.17 = (bf16[80,1024]{1,0:T(8,128)(2,1)S(1)}, bf16[80,1024]{1,0:T(8,128)(2,1)S(1)}, u32[]{:S(2)}, u32[]{:S(2)}) collective-permute-start(bf16[80,1024]{1,0:T(8,128)(2,1)S(1)} %get-tuple-element.62), channel_id=1, source_target_pairs={{0,16},{1,25},{2,18},{3,27},{4,20},{5,29},{6,22},{7,31},{8,24},{9,... | collective-permute-start | bytes 491528 | tf_op jit(solution)/shard_map/ppermute | solution.py:57
  7.6 21.5 %copy-start = (bf16[1,2048,1024]{2,1,0:T(8,128)(2,1)S(1)}, bf16[1,2048,1024]{2,1,0:T(8,128)(2,1)}, u32[]{:S(2)}) copy-start(bf16[1,2048,1024]{2,1,0:T(8,128)(2,1)} %wg_ref.7) | copy-start | bytes 12582916
  7.6 21.5 %copy-start.1 = (bf16[1,2048,1024]{2,1,0:T(8,128)(2,1)S(1)}, bf16[1,2048,1024]{2,1,0:T(8,128)(2,1)}, u32[]{:S(2)}) copy-start(bf16[1,2048,1024]{2,1,0:T(8,128)(2,1)} %wu_ref.7) | copy-start | bytes 12582916
  7.7 21.5 %copy-start.2 = (bf16[1,1024,2048]{2,1,0:T(8,128)(2,1)S(1)}, bf16[1,1024,2048]{2,1,0:T(8,128)(2,1)}, u32[]{:S(2)}) copy-start(bf16[1,1024,2048]{2,1,0:T(8,128)(2,1)} %wd_ref.7) | copy-start | bytes 12582916
  9.1 16.2 %collective-permute-start = (bf16[152,1024]{1,0:T(8,128)(2,1)S(1)}, bf16[152,1024]{1,0:T(8,128)(2,1)S(1)}, u32[]{:S(2)}, u32[]{:S(2)}) collective-permute-start(bf16[152,1024]{1,0:T(8,128)(2,1)S(1)} %get-tuple-element.43.refs_0_), channel_id=1, source_target_pairs={{0,4},{4,0},{8,12},{12,8},{16,20},{20,16},{24,28},{28,24},{1,5},{5... | collective-permute-start | bytes 933896 | tf_op jit(solution)/shard_map/ppermute | solution.py:51
  10.7 12.2 %collective-permute-start.25 = (bf16[80,1024]{1,0:T(8,128)(2,1)S(1)}, bf16[80,1024]{1,0:T(8,128)(2,1)S(1)}, u32[]{:S(2)}, u32[]{:S(2)}) collective-permute-start(bf16[80,1024]{1,0:T(8,128)(2,1)S(1)} %get-tuple-element.67), channel_id=1, source_target_pairs={{0,20},{1,29},{2,22},{3,31},{4,16},{5,25},{6,18},{7,27},{8,28},{9,... | collective-permute-start | bytes 491528 | tf_op jit(solution)/shard_map/ppermute | solution.py:57
  19.1 6.2 %collective-permute-start.18 = (bf16[80,1024]{1,0:T(8,128)(2,1)S(1)}, bf16[80,1024]{1,0:T(8,128)(2,1)S(1)}, u32[]{:S(2)}, u32[]{:S(2)}) collective-permute-start(bf16[80,1024]{1,0:T(8,128)(2,1)S(1)} %collective-permute-done.17.refs_0_), channel_id=1, source_target_pairs={{0,2},{1,3},{2,0},{3,1},{4,6},{5,7},{6,4},{7,5},{8,10},{9,11},{10,... | collective-permute-start | bytes 491528 | tf_op jit(solution)/shard_map/ppermute | solution.py:51
  20.9 7.7 %collective-permute-start.19 = (bf16[80,1024]{1,0:T(8,128)(2,1)S(1)}, bf16[80,1024]{1,0:T(8,128)(2,1)S(1)}, u32[]{:S(2)}, u32[]{:S(2)}) collective-permute-start(bf16[80,1024]{1,0:T(8,128)(2,1)S(1)} %collective-permute-done.17.refs_0_), channel_id=1, source_target_pairs={{0,1},{1,0},{2,3},{3,2},{4,5},{5,4},{6,7},{7,6},{8,9},{9,8},{10,11... | collective-permute-start | bytes 491528 | tf_op jit(solution)/shard_map/ppermute | solution.py:51
  22.8 5.7 %collective-permute-start.26 = (bf16[80,1024]{1,0:T(8,128)(2,1)S(1)}, bf16[80,1024]{1,0:T(8,128)(2,1)S(1)}, u32[]{:S(2)}, u32[]{:S(2)}) collective-permute-start(bf16[80,1024]{1,0:T(8,128)(2,1)S(1)} %collective-permute-done.25.refs_0_), channel_id=1, source_target_pairs={{0,2},{1,3},{2,0},{3,1},{4,6},{5,7},{6,4},{7,5},{8,10},{9,11},{10,... | collective-permute-start | bytes 491528 | tf_op jit(solution)/shard_map/ppermute | solution.py:51
  25.3 3.8 %collective-permute-start.20 = (bf16[80,1024]{1,0:T(8,128)(2,1)S(1)}, bf16[80,1024]{1,0:T(8,128)(2,1)S(1)}, u32[]{:S(2)}, u32[]{:S(2)}) collective-permute-start(bf16[80,1024]{1,0:T(8,128)(2,1)S(1)} %collective-permute-done.18.refs_1_), channel_id=1, source_target_pairs={{0,1},{1,0},{2,3},{3,2},{4,5},{5,4},{6,7},{7,6},{8,9},{9,8},{10,11... | collective-permute-start | bytes 491528 | tf_op jit(solution)/shard_map/ppermute | solution.py:51
  25.4 14.4 %collective-permute-start.1 = (bf16[152,1024]{1,0:T(8,128)(2,1)S(1)}, bf16[152,1024]{1,0:T(8,128)(2,1)S(1)}, u32[]{:S(2)}, u32[]{:S(2)}) collective-permute-start(bf16[152,1024]{1,0:T(8,128)(2,1)S(1)} %get-tuple-element.45.refs_0_), channel_id=1, source_target_pairs={{0,8},{4,12},{8,0},{12,4},{16,24},{20,28},{24,16},{28,20},{1,9},{5... | collective-permute-start | bytes 933896 | tf_op jit(solution)/shard_map/ppermute | solution.py:51
  25.7 14.1 %collective-permute-start.6 = (bf16[80,1024]{1,0:T(8,128)(2,1)S(1)}, bf16[80,1024]{1,0:T(8,128)(2,1)S(1)}, u32[]{:S(2)}, u32[]{:S(2)}) collective-permute-start(bf16[80,1024]{1,0:T(8,128)(2,1)S(1)} %get-tuple-element.52), channel_id=1, source_target_pairs={{0,12},{4,8},{8,4},{12,0},{16,28},{20,24},{24,20},{28,16},{1,13},{... | collective-permute-start | bytes 491528 | tf_op jit(solution)/shard_map/ppermute | solution.py:51
  28.5 11.9 %collective-permute-start.27 = (bf16[80,1024]{1,0:T(8,128)(2,1)S(1)}, bf16[80,1024]{1,0:T(8,128)(2,1)S(1)}, u32[]{:S(2)}, u32[]{:S(2)}) collective-permute-start(bf16[80,1024]{1,0:T(8,128)(2,1)S(1)} %collective-permute-done.25.refs_0_), channel_id=1, source_target_pairs={{0,1},{1,0},{2,3},{3,2},{4,5},{5,4},{6,7},{7,6},{8,9},{9,8},{10,11... | collective-permute-start | bytes 491528 | tf_op jit(solution)/shard_map/ppermute | solution.py:51
  28.6 14.3 %collective-permute-start.12 = (bf16[152,1024]{1,0:T(8,128)(2,1)S(1)}, bf16[152,1024]{1,0:T(8,128)(2,1)S(1)}, u32[]{:S(2)}, u32[]{:S(2)}) collective-permute-start(bf16[152,1024]{1,0:T(8,128)(2,1)S(1)} %collective-permute-done.refs_1_), channel_id=1, source_target_pairs={{0,1},{1,0},{2,3},{3,2},{4,5},{5,4},{6,7},{7,6},{8,9},{9,8},{10,11... | collective-permute-start | bytes 933896 | tf_op jit(solution)/shard_map/ppermute | solution.py:51
  29.1 11.3 %collective-permute-start.28 = (bf16[80,1024]{1,0:T(8,128)(2,1)S(1)}, bf16[80,1024]{1,0:T(8,128)(2,1)S(1)}, u32[]{:S(2)}, u32[]{:S(2)}) collective-permute-start(bf16[80,1024]{1,0:T(8,128)(2,1)S(1)} %collective-permute-done.26.refs_1_), channel_id=1, source_target_pairs={{0,1},{1,0},{2,3},{3,2},{4,5},{5,4},{6,7},{7,6},{8,9},{9,8},{10,11... | collective-permute-start | bytes 491528 | tf_op jit(solution)/shard_map/ppermute | solution.py:51
  39.8 13.0 %collective-permute-start.21 = (bf16[80,2048]{1,0:T(8,128)(2,1)S(1)}, bf16[80,2048]{1,0:T(8,128)(2,1)S(1)}, u32[]{:S(2)}, u32[]{:S(2)}) collective-permute-start(bf16[80,2048]{1,0:T(8,128)(2,1)S(1)} %get-tuple-element.64), channel_id=1, source_target_pairs={{0,1},{1,0},{2,3},{3,2},{4,5},{5,4},{6,7},{7,6},{8,9},{9,8},{10,11... | collective-permute-start | bytes 983048 | tf_op jit(solution)/shard_map/ppermute | solution.py:51
  39.8 6.0 %collective-permute-start.7 = (bf16[160,1024]{1,0:T(8,128)(2,1)S(1)}, bf16[160,1024]{1,0:T(8,128)(2,1)S(1)}, u32[]{:S(2)}, u32[]{:S(2)}) collective-permute-start(bf16[160,1024]{1,0:T(8,128)(2,1)S(1)} %shard_map.166.refs_0_), channel_id=1, source_target_pairs={{0,1},{1,0},{2,3},{3,2},{4,5},{5,4},{6,7},{7,6},{8,9},{9,8},{10,11... | collective-permute-start | bytes 983048 | tf_op jit(solution)/shard_map/ppermute | solution.py:51
  42.8 16.5 %collective-permute-start.29 = (bf16[80,2048]{1,0:T(8,128)(2,1)S(1)}, bf16[80,2048]{1,0:T(8,128)(2,1)S(1)}, u32[]{:S(2)}, u32[]{:S(2)}) collective-permute-start(bf16[80,2048]{1,0:T(8,128)(2,1)S(1)} %get-tuple-element.69), channel_id=1, source_target_pairs={{0,1},{1,0},{2,3},{3,2},{4,5},{5,4},{6,7},{7,6},{8,9},{9,8},{10,11... | collective-permute-start | bytes 983048 | tf_op jit(solution)/shard_map/ppermute | solution.py:51
  45.2 11.1 %copy-start.4 = (bf16[256,512]{1,0:T(8,128)(2,1)S(1)}, bf16[256,512]{1,0:T(8,128)(2,1)}, u32[]{:S(2)}) copy-start(bf16[256,512]{1,0:T(8,128)(2,1)} %gate_ref.1) | copy-start | bytes 786436
  45.3 11.1 %copy-start.7 = (f32[128]{0:T(128)S(1)}, f32[128]{0:T(128)}, u32[]{:S(2)}) copy-start(f32[128]{0:T(128)} %param.21) | copy-start | bytes 1540
  45.3 14.1 %collective-permute-start.13 = (bf16[80,2048]{1,0:T(8,128)(2,1)S(1)}, bf16[80,2048]{1,0:T(8,128)(2,1)S(1)}, u32[]{:S(2)}, u32[]{:S(2)}) collective-permute-start(bf16[80,2048]{1,0:T(8,128)(2,1)S(1)} %get-tuple-element.59), channel_id=1, source_target_pairs={{0,1},{1,0},{2,3},{3,2},{4,5},{5,4},{6,7},{7,6},{8,9},{9,8},{10,11... | collective-permute-start | bytes 983048 | tf_op jit(solution)/shard_map/ppermute | solution.py:51
  48.4 42.3 %copy-start.5 = (s32[256,2]{0,1:T(2,128)S(1)}, s32[256,2]{0,1:T(2,128)}, u32[]{:S(2)}) copy-start(s32[256,2]{0,1:T(2,128)} %param.25) | copy-start | bytes 6148
  48.4 42.3 %copy-start.6 = (f32[256,2]{0,1:T(2,128)S(1)}, f32[256,2]{0,1:T(2,128)}, u32[]{:S(2)}) copy-start(f32[256,2]{0,1:T(2,128)} %param.26) | copy-start | bytes 6148
  48.4 42.8 %copy-start.3 = (bf16[2048,512]{1,0:T(8,128)(2,1)S(1)}, bf16[2048,512]{1,0:T(8,128)(2,1)}, u32[]{:S(2)}) copy-start(bf16[2048,512]{1,0:T(8,128)(2,1)} %param.22) | copy-start | bytes 6291460
  48.4 11.2 %collective-permute-start.8 = (bf16[80,2048]{1,0:T(8,128)(2,1)S(1)}, bf16[80,2048]{1,0:T(8,128)(2,1)S(1)}, u32[]{:S(2)}, u32[]{:S(2)}) collective-permute-start(bf16[80,2048]{1,0:T(8,128)(2,1)S(1)} %get-tuple-element.54), channel_id=1, source_target_pairs={{0,1},{1,0},{2,3},{3,2},{4,5},{5,4},{6,7},{7,6},{8,9},{9,8},{10,11... | collective-permute-start | bytes 983048 | tf_op jit(solution)/shard_map/ppermute | solution.py:51
  48.7 7.6 %collective-permute-start.2 = (bf16[136,512]{1,0:T(8,128)(2,1)S(1)}, bf16[136,512]{1,0:T(8,128)(2,1)S(1)}, u32[]{:S(2)}, u32[]{:S(2)}) collective-permute-start(bf16[136,512]{1,0:T(8,128)(2,1)S(1)} %get-tuple-element.48), channel_id=1, source_target_pairs={{0,16},{4,20},{8,24},{12,28},{1,17},{5,21},{9,25},{13,29},{2,18},{... | collective-permute-start | bytes 417800 | tf_op jit(solution)/shard_map/ppermute | solution.py:517
  52.9 8.8 %collective-permute-start.22 = (bf16[80,1024]{1,0:T(8,128)(2,1)S(1)}, bf16[80,1024]{1,0:T(8,128)(2,1)S(1)}, u32[]{:S(2)}, u32[]{:S(2)}) collective-permute-start(bf16[80,1024]{1,0:T(8,128)(2,1)S(1)} %get-tuple-element.66), channel_id=1, source_target_pairs={{0,2},{1,3},{2,0},{3,1},{4,6},{5,7},{6,4},{7,5},{8,10},{9,11},{10,... | collective-permute-start | bytes 491528 | tf_op jit(solution)/shard_map/ppermute | solution.py:51
  56.7 20.2 %collective-permute-start.3 = (bf16[256,512]{1,0:T(8,128)(2,1)S(1)}, bf16[256,512]{1,0:T(8,128)(2,1)S(1)}, u32[]{:S(2)}, u32[]{:S(2)}) collective-permute-start(bf16[256,512]{1,0:T(8,128)(2,1)S(1)} %shard_map.163.refs_0_), channel_id=1, source_target_pairs={{0,2},{1,3},{2,0},{3,1},{4,6},{5,7},{6,4},{7,5},{8,10},{9,11},{10,... | collective-permute-start | bytes 786440 | tf_op jit(solution)/shard_map/ppermute | solution.py:51
  59.3 23.2 %collective-permute-start.4 = (bf16[256,512]{1,0:T(8,128)(2,1)S(1)}, bf16[256,512]{1,0:T(8,128)(2,1)S(1)}, u32[]{:S(2)}, u32[]{:S(2)}) collective-permute-start(bf16[256,512]{1,0:T(8,128)(2,1)S(1)} %shard_map.163.refs_0_), channel_id=1, source_target_pairs={{0,1},{1,0},{2,3},{3,2},{4,5},{5,4},{6,7},{7,6},{8,9},{9,8},{10,11... | collective-permute-start | bytes 786440 | tf_op jit(solution)/shard_map/ppermute | solution.py:51
  59.4 10.6 %collective-permute-start.30 = (bf16[80,1024]{1,0:T(8,128)(2,1)S(1)}, bf16[80,1024]{1,0:T(8,128)(2,1)S(1)}, u32[]{:S(2)}, u32[]{:S(2)}) collective-permute-start(bf16[80,1024]{1,0:T(8,128)(2,1)S(1)} %get-tuple-element.71), channel_id=1, source_target_pairs={{0,2},{1,3},{2,0},{3,1},{4,6},{5,7},{6,4},{7,5},{8,10},{9,11},{10,... | collective-permute-start | bytes 491528 | tf_op jit(solution)/shard_map/ppermute | solution.py:51
  59.7 13.8 %collective-permute-start.14 = (bf16[80,1024]{1,0:T(8,128)(2,1)S(1)}, bf16[80,1024]{1,0:T(8,128)(2,1)S(1)}, u32[]{:S(2)}, u32[]{:S(2)}) collective-permute-start(bf16[80,1024]{1,0:T(8,128)(2,1)S(1)} %get-tuple-element.61), channel_id=1, source_target_pairs={{0,2},{1,3},{2,0},{3,1},{4,6},{5,7},{6,4},{7,5},{8,10},{9,11},{10,... | collective-permute-start | bytes 491528 | tf_op jit(solution)/shard_map/ppermute | solution.py:51
  61.7 15.9 %collective-permute-start.9 = (bf16[80,1024]{1,0:T(8,128)(2,1)S(1)}, bf16[80,1024]{1,0:T(8,128)(2,1)S(1)}, u32[]{:S(2)}, u32[]{:S(2)}) collective-permute-start(bf16[80,1024]{1,0:T(8,128)(2,1)S(1)} %get-tuple-element.56), channel_id=1, source_target_pairs={{0,2},{1,3},{2,0},{3,1},{4,6},{5,7},{6,4},{7,5},{8,10},{9,11},{10,... | collective-permute-start | bytes 491528 | tf_op jit(solution)/shard_map/ppermute | solution.py:51
  70.0 15.2 %collective-permute-start.23 = (bf16[80,1024]{1,0:T(8,128)(2,1)S(1)}, bf16[80,1024]{1,0:T(8,128)(2,1)S(1)}, u32[]{:S(2)}, u32[]{:S(2)}) collective-permute-start(bf16[80,1024]{1,0:T(8,128)(2,1)S(1)} %shard_map.175), channel_id=1, source_target_pairs={{0,16},{1,25},{2,18},{3,27},{4,20},{5,29},{6,22},{7,31},{8,24},{9,... | collective-permute-start | bytes 491528 | tf_op jit(solution)/shard_map/ppermute | solution.py:57
  73.5 15.2 %collective-permute-start.31 = (bf16[80,1024]{1,0:T(8,128)(2,1)S(1)}, bf16[80,1024]{1,0:T(8,128)(2,1)S(1)}, u32[]{:S(2)}, u32[]{:S(2)}) collective-permute-start(bf16[80,1024]{1,0:T(8,128)(2,1)S(1)} %shard_map.178), channel_id=1, source_target_pairs={{0,20},{1,29},{2,22},{3,31},{4,16},{5,25},{6,18},{7,27},{8,28},{9,... | collective-permute-start | bytes 491528 | tf_op jit(solution)/shard_map/ppermute | solution.py:57
  76.9 11.8 %collective-permute-start.15 = (bf16[80,1024]{1,0:T(8,128)(2,1)S(1)}, bf16[80,1024]{1,0:T(8,128)(2,1)S(1)}, u32[]{:S(2)}, u32[]{:S(2)}) collective-permute-start(bf16[80,1024]{1,0:T(8,128)(2,1)S(1)} %shard_map.172), channel_id=1, source_target_pairs={{0,0},{1,5},{2,2},{3,7},{4,4},{5,1},{6,6},{7,3},{8,8},{9,13},{10,1... | collective-permute-start | bytes 491528 | tf_op jit(solution)/shard_map/ppermute | solution.py:62
  77.6 13.6 %collective-permute-start.5 = (bf16[256,512]{1,0:T(8,128)(2,1)S(1)}, bf16[256,512]{1,0:T(8,128)(2,1)S(1)}, u32[]{:S(2)}, u32[]{:S(2)}) collective-permute-start(bf16[256,512]{1,0:T(8,128)(2,1)S(1)} %collective-permute-done.3.refs_1_), channel_id=1, source_target_pairs={{0,1},{1,0},{2,3},{3,2},{4,5},{5,4},{6,7},{7,6},{8,9},{9,8},{10,11... | collective-permute-start | bytes 786440 | tf_op jit(solution)/shard_map/ppermute | solution.py:51
  82.6 8.0 %collective-permute-start.10 = (bf16[80,1024]{1,0:T(8,128)(2,1)S(1)}, bf16[80,1024]{1,0:T(8,128)(2,1)S(1)}, u32[]{:S(2)}, u32[]{:S(2)}) collective-permute-start(bf16[80,1024]{1,0:T(8,128)(2,1)S(1)} %shard_map.169), channel_id=1, source_target_pairs={{0,8},{1,13},{2,10},{3,15},{4,12},{5,9},{6,14},{7,11},{8,0},{9,5},... | collective-permute-start | bytes 491528 | tf_op jit(solution)/shard_map/ppermute | solution.py:62
  85.2 7.5 %collective-permute-start.24 = (bf16[80,1024]{1,0:T(8,128)(2,1)S(1)}, bf16[80,1024]{1,0:T(8,128)(2,1)S(1)}, u32[]{:S(2)}, u32[]{:S(2)}) collective-permute-start(bf16[80,1024]{1,0:T(8,128)(2,1)S(1)} %collective-permute-done.23.refs_2_), channel_id=1, source_target_pairs={{0,1},{1,0},{2,3},{3,2},{4,5},{5,4},{6,7},{7,6},{8,9},{9,8},{10,11... | collective-permute-start | bytes 491528 | tf_op jit(solution)/shard_map/ppermute | solution.py:51
  88.7 4.0 %collective-permute-start.32 = (bf16[80,1024]{1,0:T(8,128)(2,1)S(1)}, bf16[80,1024]{1,0:T(8,128)(2,1)S(1)}, u32[]{:S(2)}, u32[]{:S(2)}) collective-permute-start(bf16[80,1024]{1,0:T(8,128)(2,1)S(1)} %collective-permute-done.31.refs_4_), channel_id=1, source_target_pairs={{0,1},{1,0},{2,3},{3,2},{4,5},{5,4},{6,7},{7,6},{8,9},{9,8},{10,11... | collective-permute-start | bytes 491528 | tf_op jit(solution)/shard_map/ppermute | solution.py:51
  88.7 4.0 %collective-permute-start.16 = (bf16[80,1024]{1,0:T(8,128)(2,1)S(1)}, bf16[80,1024]{1,0:T(8,128)(2,1)S(1)}, u32[]{:S(2)}, u32[]{:S(2)}) collective-permute-start(bf16[80,1024]{1,0:T(8,128)(2,1)S(1)} %collective-permute-done.15.refs_0_), channel_id=1, source_target_pairs={{0,1},{1,0},{2,3},{3,2},{4,5},{5,4},{6,7},{7,6},{8,9},{9,8},{10,11... | collective-permute-start | bytes 491528 | tf_op jit(solution)/shard_map/ppermute | solution.py:51
  90.5 2.7 %collective-permute-start.11 = (bf16[80,1024]{1,0:T(8,128)(2,1)S(1)}, bf16[80,1024]{1,0:T(8,128)(2,1)S(1)}, u32[]{:S(2)}, u32[]{:S(2)}) collective-permute-start(bf16[80,1024]{1,0:T(8,128)(2,1)S(1)} %collective-permute-done.10.refs_0_), channel_id=1, source_target_pairs={{0,1},{1,0},{2,3},{3,2},{4,5},{5,4},{6,7},{7,6},{8,9},{9,8},{10,11... | collective-permute-start | bytes 491528 | tf_op jit(solution)/shard_map/ppermute | solution.py:51
